TPU v7x, 32 devices: a whole 2x2x4 slice. The times are simulated.
32 devices in a mesh: dp: 4 (over y, x), kv: 4 (over z), tp: 2 (over core).
Axes of the slice: x: 2, y: 2, z: 4, core: 2. Of those that a mesh axis runs over, the one named last changes fastest.
Arguments:
- tokens: bfloat16 [32, 4096], P('dp', ('kv', 'tp')), may hold values from -7 to 7
- mix_gain: float32 [4096], replicated, may hold values from 0.1 to 1.9
- query_weight: bfloat16 [16, 128, 4096], P('tp', 'kv'), may hold values from -0.09375 to 0.09375
- forget_weight: bfloat16 [16, 128, 4096], P('tp', 'kv'), may hold values from -0.09375 to 0.09375
- value_weight: bfloat16 [16, 128, 4096], P('tp', 'kv'), may hold values from -0.09375 to 0.09375
- gate_weight: bfloat16 [16, 128, 4096], P('tp', 'kv'), may hold values from -0.09375 to 0.09375
- lower_bound: float32 [16, 128], P('tp'), may hold values from 0.02 to 0.9
- recurrent_state: float32 [32, 16, 128, 128], P(('dp', 'kv'), 'tp'), may hold values from -3 to 3
- head_gain: float32 [16, 128], P('tp'), may hold values from 0.1 to 1.9
- out_weight: bfloat16 [16, 128, 4096], P(None, None, ('kv', 'tp')), may hold values from -0.125 to 0.125
- mlp_gain: float32 [4096], replicated, may hold values from 0.1 to 1.9
- up_weight: bfloat16 [4096, 16384], P(None, ('kv', 'tp')), may hold values from -0.09375 to 0.09375
- down_weight: bfloat16 [16384, 4096], P(('kv', 'tp')), may hold values from -0.0625 to 0.0625
Outputs:
- layer_output: bfloat16 [32, 4096], P('dp', ('kv', 'tp'))
- next_state: float32 [32, 16, 128, 128], P(('dp', 'kv'), 'tp')
All inputs are finite; a program needn't handle non-finite values.
Results may differ from a plain program's by a relative error of at most 0.0072.
Values may be sent and summed in bfloat16 or wider, within the bound.
No kernel may reach another device: no remote copies, remote signals or barrier semaphores. Data moves between devices by JAX's collectives and lax.ppermute only.
A program may use at most 128 MiB of HBM per device.

v0:
```python
import jax
import jax.numpy as jnp
from jax import lax
from jax.sharding import PartitionSpec as P

epsilon = 1e-06


def normed_rows(row_block, gain_vector):
    whole_rows = lax.all_gather(row_block, ("kv", "tp"), axis=1, tiled=True).astype(jnp.float32)
    inv_root = lax.rsqrt(jnp.mean(whole_rows * whole_rows, axis=1, keepdims=True) + epsilon)
    result_rows = (whole_rows * inv_root * gain_vector).astype(jnp.bfloat16)
    return result_rows


def local(
    tokens,
    mix_gain,
    query_weight,
    forget_weight,
    value_weight,
    gate_weight,
    lower_bound,
    recurrent_state,
    head_gain,
    out_weight,
    mlp_gain,
    up_weight,
    down_weight,
):
    normed = normed_rows(tokens, mix_gain)
    local_heads, local_chan, width = query_weight.shape
    stacked = jnp.stack((query_weight, forget_weight, value_weight, gate_weight), axis=0).reshape(
        -1, width
    )
    product = lax.dot_general(
        normed, stacked, (((1,), (1,)), ((), ())), preferred_element_type=jnp.float32
    ).astype(jnp.bfloat16)
    product = product.reshape(normed.shape[0], 4, local_heads, local_chan)
    pre_query, pre_forget, value_rows, pre_gate = (
        lax.all_to_all(product[:, 0], "kv", split_axis=0, concat_axis=2, tiled=True),
        lax.all_to_all(product[:, 1], "kv", split_axis=0, concat_axis=2, tiled=True),
        lax.all_to_all(product[:, 2], "kv", split_axis=0, concat_axis=2, tiled=True),
        lax.all_to_all(product[:, 3], "kv", split_axis=0, concat_axis=2, tiled=True),
    )
    log_forget = jnp.logaddexp(
        jnp.log(lower_bound),
        jnp.log1p(-lower_bound) + jax.nn.log_sigmoid(pre_forget.astype(jnp.float32)),
    )
    key_rows = -jnp.expm1(log_forget)
    next_state = (
        jnp.exp(log_forget)[:, :, :, None] * recurrent_state
        + key_rows[:, :, :, None] * value_rows.astype(jnp.float32)[:, :, None, :]
    )
    query_act = jax.nn.silu(pre_query.astype(jnp.float32))
    readout = jnp.einsum("bhk,bhkv->bhv", query_act, next_state, precision=lax.Precision.HIGHEST)
    inv_head = lax.rsqrt(jnp.mean(readout * readout, axis=2, keepdims=True) + epsilon)
    mixed_heads = (
        readout * inv_head * head_gain * jax.nn.silu(pre_gate.astype(jnp.float32))
    ).astype(jnp.bfloat16)
    all_heads = lax.all_gather(mixed_heads, "tp", axis=1, tiled=True)
    flat_mixed = all_heads.reshape(all_heads.shape[0], -1)
    out_matrix = out_weight.reshape(-1, out_weight.shape[2])
    projected = jnp.dot(
        lax.all_gather(flat_mixed, "kv", axis=0, tiled=True),
        out_matrix,
        preferred_element_type=jnp.float32,
    )
    residual = lax.optimization_barrier(
        (tokens.astype(jnp.float32) + projected).astype(jnp.bfloat16)
    )
    normed_mlp = normed_rows(residual, mlp_gain)
    hidden = jnp.square(
        jax.nn.relu(jnp.dot(normed_mlp, up_weight, preferred_element_type=jnp.float32))
    ).astype(jnp.bfloat16)
    summed = lax.psum_scatter(
        jnp.dot(hidden, down_weight, preferred_element_type=jnp.float32),
        ("kv", "tp"),
        scatter_dimension=1,
        tiled=True,
    )
    layer_output = (residual.astype(jnp.float32) + summed).astype(jnp.bfloat16)
    return (layer_output, next_state)


def solution(mesh):
    placed = (
        P("dp", ("kv", "tp")),
        P(),
        P("tp", "kv", None),
        P("tp", "kv", None),
        P("tp", "kv", None),
        P("tp", "kv", None),
        P("tp", None),
        P(("dp", "kv"), "tp", None, None),
        P("tp", None),
        P(None, None, ("kv", "tp")),
        P(),
        P(None, ("kv", "tp")),
        P(("kv", "tp"), None),
    )
    return jax.shard_map(
        local,
        mesh=mesh,
        in_specs=placed,
        out_specs=(P("dp", ("kv", "tp")), P(("dp", "kv"), "tp", None, None)),
        check_vma=False,
    )
```

profile of v0, /device:TPU:0, one launch (start us, length us, event | category | flops | bytes accessed | tf_op | source)
XLA Modules:
  0.0 148.9 jit_solution(8380039019351915380)
XLA Ops:
  7.2 16.0 %all_gather.12 = bf16[8,4096]{1,0:T(8,128)(2,1)S(1)} all-gather(bf16[8,512]{1,0:T(8,128)(2,1)} %param.13), channel_id=1, replica_groups=mesh['dp'=4,'kv'=4,'tp'=2] {'kv','tp'}, dimensions={1}, use_global_device_ids=true | all-gather | bytes 73728 | tf_op jit(solution)/shard_map/all_gather | solution.py:10
  23.4 4.4 %pad_maximum_fusion = bf16[4,8,32,4096]{3,2,1,0:T(8,128)(2,1)S(1)} fusion(bf16[1,8,32,4096]{3,2,1,0:T(8,128)(2,1)} %bitcast.47, bf16[1,8,32,4096]{3,2,1,0:T(8,128)(2,1)} %bitcast.48, bf16[1,8,32,4096]{3,2,1,0:T(8,128)(2,1)} %bitcast.49, bf16[1,8,32,4096]{3,2,1,0:T(8,128)(2,1)} %bitcast.50), kind=kLoop, calls=%fused_computation | loop fusion | flops 12582912 | bytes 16777216 | tf_op jit(solution)/shard_map/stack | solution.py:33
  27.8 2.3 %convolution_convert_fusion = bf16[8,1024]{1,0:T(8,128)(2,1)S(1)} fusion(bf16[1024,4096]{1,0:T(8,128)(2,1)S(1)} %bitcast.46, bf16[8,4096]{1,0:T(8,128)(2,1)S(1)} %all_gather.12, f32[4096]{0:T(1024)S(1)} %copy-done.3, f32[8]{0:T(128)S(1)} %add_rsqrt_fusion.2), kind=kOutput, calls=%fused_computation.4 | convolution fusion | flops 67248128 | bytes 8486944 | tf_op jit(solution)/shard_map/dot_general | solution.py:36
  30.2 0.7 reshape.119
  30.9 4.6 %all-to-all-start.1 = ((bf16[4,2,256]{2,1,0:T(2,128)(2,1)}), bf16[4,2,256]{2,1,0:T(2,128)(2,1)S(1)}, u32[]{:S(2)}, u32[]{:S(2)}) async-start(bf16[4,2,256]{2,1,0:T(2,128)(2,1)} %reshape.119), calls=%async_computation.1 | async-start | bytes 8192 | tf_op jit(solution)/shard_map/all_to_all | solution.py:42
  35.6 0.7 reshape.117
  36.2 0.7 reshape.115
  36.9 0.7 reshape.113
  37.6 3.5 %all-to-all-done.1 = bf16[4,2,256]{2,1,0:T(2,128)(2,1)S(1)} async-done(((bf16[4,2,256]{2,1,0:T(2,128)(2,1)}), bf16[4,2,256]{2,1,0:T(2,128)(2,1)S(1)}, u32[]{:S(2)}, u32[]{:S(2)}) %all-to-all-start.1) | async-done | bytes 4128 | tf_op jit(solution)/shard_map/all_to_all | solution.py:42
  41.1 3.2 %all-to-all-start.2 = ((bf16[4,2,256]{2,1,0:T(2,128)(2,1)}), bf16[4,2,256]{2,1,0:T(2,128)(2,1)S(1)}, u32[]{:S(2)}, u32[]{:S(2)}) async-start(bf16[4,2,256]{2,1,0:T(2,128)(2,1)} %reshape.117), calls=%async_computation.2 | async-start | bytes 8192 | tf_op jit(solution)/shard_map/all_to_all | solution.py:43
  44.4 5.4 %all-to-all-done.2 = bf16[4,2,256]{2,1,0:T(2,128)(2,1)S(1)} async-done(((bf16[4,2,256]{2,1,0:T(2,128)(2,1)}), bf16[4,2,256]{2,1,0:T(2,128)(2,1)S(1)}, u32[]{:S(2)}, u32[]{:S(2)}) %all-to-all-start.2) | async-done | bytes 4128 | tf_op jit(solution)/shard_map/all_to_all | solution.py:43
  49.9 3.2 %all-to-all-start = ((bf16[4,2,256]{2,1,0:T(2,128)(2,1)}), bf16[4,2,256]{2,1,0:T(2,128)(2,1)S(1)}, u32[]{:S(2)}, u32[]{:S(2)}) async-start(bf16[4,2,256]{2,1,0:T(2,128)(2,1)} %reshape.115), calls=%async_computation | async-start | bytes 8192 | tf_op jit(solution)/shard_map/all_to_all | solution.py:41
  53.4 5.2 %all-to-all-done = bf16[4,2,256]{2,1,0:T(2,128)(2,1)S(1)} async-done(((bf16[4,2,256]{2,1,0:T(2,128)(2,1)}), bf16[4,2,256]{2,1,0:T(2,128)(2,1)S(1)}, u32[]{:S(2)}, u32[]{:S(2)}) %all-to-all-start) | async-done | bytes 4128 | tf_op jit(solution)/shard_map/all_to_all | solution.py:41
  58.7 3.2 %all-to-all-start.3 = ((bf16[4,2,256]{2,1,0:T(2,128)(2,1)}), bf16[4,2,256]{2,1,0:T(2,128)(2,1)S(1)}, u32[]{:S(2)}, u32[]{:S(2)}) async-start(bf16[4,2,256]{2,1,0:T(2,128)(2,1)} %reshape.113), calls=%async_computation.3 | async-start | bytes 8192 | tf_op jit(solution)/shard_map/all_to_all | solution.py:44
  62.3 1.8 %multiply_add_fusion = f32[2,8,128,128]{3,2,1,0:T(8,128)S(1)} fusion(f32[2,8,128,128]{3,2,1,0:T(8,128)} %param.20, f32[2,8,128]{2,1,0:T(8,128)S(1)} %reshape.103, f32[2,8,128]{2,1,0:T(8,128)S(1)} %get-tuple-element.7, f32[2,8,128]{2,1,0:T(8,128)S(1)} %get-tuple-element.6), kind=kLoop, calls=%fused_computation.7 | loop fusion | flops 786432 | bytes 2121728 | tf_op jit(solution)/shard_map/add | solution.py:52
  64.1 1.0 fusion.25
  65.2 2.3 %all-to-all-done.3 = bf16[4,2,256]{2,1,0:T(2,128)(2,1)S(1)} async-done(((bf16[4,2,256]{2,1,0:T(2,128)(2,1)}), bf16[4,2,256]{2,1,0:T(2,128)(2,1)S(1)}, u32[]{:S(2)}, u32[]{:S(2)}) %all-to-all-start.3) | async-done | bytes 4128 | tf_op jit(solution)/shard_map/all_to_all | solution.py:44
  67.8 1.8 %all_gather.13 = bf16[2,16,128]{2,1,0:T(8,128)(2,1)S(1)} all-gather(bf16[2,8,128]{2,1,0:T(8,128)(2,1)S(1)} %multiply_convert_fusion), channel_id=1, replica_groups=mesh['dp'=4,'kv'=4,'tp'=2] {'tp'}, dimensions={1}, use_global_device_ids=true | all-gather | bytes 12288 | tf_op jit(solution)/shard_map/all_gather | solution.py:61
  69.6 13.1 %all-gather = bf16[4,2,2048]{2,1,0:T(2,128)(2,1)S(1)} all-gather(bf16[1,2,2048]{2,1,0:T(2,128)(2,1)S(1)} %reshape.108), channel_id=1, replica_groups=mesh['dp'=4,'kv'=4,'tp'=2] {'kv'}, dimensions={0}, use_global_device_ids=true | all-gather | bytes 40960 | tf_op jit(solution)/shard_map/all_gather | solution.py:65
  82.8 0.4 fusion.2
  83.2 14.0 %all_gather.15 = bf16[8,4096]{1,0:T(8,128)(2,1)S(1)} all-gather(bf16[8,512]{1,0:T(8,128)(2,1)S(1)} %fusion.2), channel_id=1, replica_groups=mesh['dp'=4,'kv'=4,'tp'=2] {'kv','tp'}, dimensions={1}, use_global_device_ids=true | all-gather | bytes 73728 | tf_op jit(solution)/shard_map/all_gather | solution.py:10
  97.3 13.5 %fusion.3 = f32[8,4096]{1,0:T(8,128)} fusion(bf16[2048,4096]{1,0:T(8,128)(2,1)} %param.25, bf16[4096,2048]{1,0:T(8,128)(2,1)} %param.24, bf16[8,4096]{1,0:T(8,128)(2,1)S(1)} %all_gather.15, f32[4096]{0:T(1024)S(1)} %copy-done.4, f32[8]{0:T(128)S(1)} %add_rsqrt_fusion.1), kind=kOutput, calls=%fused_computation.8 | convolution fusion | flops 268615680 | bytes 33767456 | tf_op jit(solution)/shard_map/dot_general | solution.py:77
  110.9 29.9 %reduce-scatter.2.cloned.1.call-done = f32[8,512]{1,0:T(8,128)} async-done(((f32[8,4096]{1,0:T(8,128)}), f32[8,512]{1,0:T(8,128)}) %reduce-scatter.2.cloned.1.call-update) | async-done | bytes 16400 | tf_op jit(solution)/shard_map/reduce_scatter | solution.py:76
  140.7 1.3 add_convert_fusion
  (46 shorter events, 1.6 us)
Async XLA Ops:
  7.2 75.6 %copy-start = (bf16[16,128,512]{2,1,0:T(8,128)(2,1)S(1)}, bf16[16,128,512]{2,1,0:T(8,128)(2,1)}, u32[]{:S(2)}) copy-start(bf16[16,128,512]{2,1,0:T(8,128)(2,1)} %param.22) | copy-start | bytes 6291460
  23.4 4.4 %copy-start.3 = (f32[4096]{0:T(1024)S(1)}, f32[4096]{0:T(1024)}, u32[]{:S(2)}) copy-start(f32[4096]{0:T(1024)} %param.14) | copy-start | bytes 49156
  27.7 7.8 %copy-start.5 = (f32[8,128]{1,0:T(8,128)S(1)}, f32[8,128]{1,0:T(8,128)}, u32[]{:S(2)}) copy-start(f32[8,128]{1,0:T(8,128)} %param.19) | copy-start | bytes 12292
  27.8 39.9 %copy-start.6 = (f32[8,128]{1,0:T(8,128)S(1)}, f32[8,128]{1,0:T(8,128)}, u32[]{:S(2)}) copy-start(f32[8,128]{1,0:T(8,128)} %param.21) | copy-start | bytes 12292
  27.8 55.0 %copy-start.2 = (bf16[8,512]{1,0:T(8,128)(2,1)S(1)}, bf16[8,512]{1,0:T(8,128)(2,1)}, u32[]{:S(2)}) copy-start(bf16[8,512]{1,0:T(8,128)(2,1)} %param.13) | copy-start | bytes 24580
  27.8 69.5 %copy-start.4 = (f32[4096]{0:T(1024)S(1)}, f32[4096]{0:T(1024)}, u32[]{:S(2)}) copy-start(f32[4096]{0:T(1024)} %param.23) | copy-start | bytes 49156
  30.9 10.2 %all-to-all-start.1 = ((bf16[4,2,256]{2,1,0:T(2,128)(2,1)}), bf16[4,2,256]{2,1,0:T(2,128)(2,1)S(1)}, u32[]{:S(2)}, u32[]{:S(2)}) async-start(bf16[4,2,256]{2,1,0:T(2,128)(2,1)} %reshape.119), calls=%async_computation.1 | async-start | bytes 8192 | tf_op jit(solution)/shard_map/all_to_all | solution.py:42
  41.1 8.8 %all-to-all-start.2 = ((bf16[4,2,256]{2,1,0:T(2,128)(2,1)}), bf16[4,2,256]{2,1,0:T(2,128)(2,1)S(1)}, u32[]{:S(2)}, u32[]{:S(2)}) async-start(bf16[4,2,256]{2,1,0:T(2,128)(2,1)} %reshape.117), calls=%async_computation.2 | async-start | bytes 8192 | tf_op jit(solution)/shard_map/all_to_all | solution.py:43
  49.9 8.8 %all-to-all-start = ((bf16[4,2,256]{2,1,0:T(2,128)(2,1)}), bf16[4,2,256]{2,1,0:T(2,128)(2,1)S(1)}, u32[]{:S(2)}, u32[]{:S(2)}) async-start(bf16[4,2,256]{2,1,0:T(2,128)(2,1)} %reshape.115), calls=%async_computation | async-start | bytes 8192 | tf_op jit(solution)/shard_map/all_to_all | solution.py:41
  58.7 8.8 %all-to-all-start.3 = ((bf16[4,2,256]{2,1,0:T(2,128)(2,1)}), bf16[4,2,256]{2,1,0:T(2,128)(2,1)S(1)}, u32[]{:S(2)}, u32[]{:S(2)}) async-start(bf16[4,2,256]{2,1,0:T(2,128)(2,1)} %reshape.113), calls=%async_computation.3 | async-start | bytes 8192 | tf_op jit(solution)/shard_map/all_to_all | solution.py:44
  61.9 78.8 %reduce-scatter.2.cloned.1.call-start = ((), (), s32[]{:S(2)}) async-start(), calls=%async_computation.5 | async-start | bytes 147456 | tf_op jit(solution)/shard_map/reduce_scatter | solution.py:76
  64.1 46.7 %copy-start.1 = (f32[2,8,128,128]{3,2,1,0:T(8,128)}, f32[2,8,128,128]{3,2,1,0:T(8,128)S(1)}, u32[]{:S(2)}) copy-start(f32[2,8,128,128]{3,2,1,0:T(8,128)S(1)} %multiply_add_fusion) | copy-start | bytes 3145732
Sparse Core Ops, SparseCore 0:
  111.0 29.6 reduce-scatter.1
where the time goes:
time: 149 us
  waiting for transfers between devices  46.4 us (31%)
  blocking collectives  45 us (30%)
  matrix products  17.1 us (11%)
  starting transfers between devices  14.4 us (10%)
  between operations  14.2 us (10%)
  other arithmetic  8.09 us (5%)
  local copies, waits for them, and re-layouts  3.68 us (2%)
    all_gather x2, blocking collectives, normed_rows(): lax.all_gather(row_block, ('kv', 'tp'), axis=1, tiled=True)  30 us
    reduce_scatter x1, waiting for transfers between devices, local(): lax.psum_scatter(jnp.dot(hidden, down_weight, preferred_element_type=jnp....  29.9 us
    dot_general x1, matrix products, local(): jnp.dot(hidden, down_weight, preferred_element_type=jnp.float32)  13.5 us
    all_gather x1, blocking collectives, local(): lax.all_gather(flat_mixed, 'kv', axis=0, tiled=True)  13.1 us
    all_to_all x1, waiting for transfers between devices, local(): lax.all_to_all(product[:, 2], 'kv', split_axis=0, concat_axis=2, tiled=True)  5.45 us
    all_to_all x1, waiting for transfers between devices, local(): lax.all_to_all(product[:, 0], 'kv', split_axis=0, concat_axis=2, tiled=True)  5.25 us
    all_to_all x1, starting transfers between devices, local(): lax.all_to_all(product[:, 1], 'kv', split_axis=0, concat_axis=2, tiled=True)  4.64 us
    another operation x1, other arithmetic, local(): jnp.stack((query_weight, forget_weight, value_weight, gate_weight), axis=0)  4.36 us
  transfers between devices with their start and end apart: 5, of which 5 were waited for; matrix products, arithmetic and copies ran while one was open for 4% of the time, Pallas kernels for 0%

commit v1 on v0

v1 whole, which is shorter than its diff:
```python
import jax
import jax.numpy as jnp
from jax import lax
from jax.sharding import PartitionSpec as P

epsilon = 1e-06
group = ("kv", "tp")


def gather_blocks(block, members):
    copies = lax.optimization_barrier(jnp.broadcast_to(block[None], (members,) + block.shape))
    return lax.all_to_all(copies, group, split_axis=0, concat_axis=0, tiled=True)


def whole_rows(row_block, members):
    pieces = gather_blocks(row_block, members)
    return jnp.swapaxes(pieces, 0, 1).reshape(row_block.shape[0], -1)


def normed_rows(rows, gain_vector):
    rows = rows.astype(jnp.float32)
    inv_root = lax.rsqrt(jnp.mean(rows * rows, axis=1, keepdims=True) + epsilon)
    return (rows * inv_root * gain_vector).astype(jnp.bfloat16)


def local(
    kv,
    tp,
    tokens,
    mix_gain,
    query_weight,
    forget_weight,
    value_weight,
    gate_weight,
    lower_bound,
    recurrent_state,
    head_gain,
    out_weight,
    mlp_gain,
    up_weight,
    down_weight,
):
    members = kv * tp
    normed = normed_rows(whole_rows(tokens, members), mix_gain)
    local_heads, local_chan, width = query_weight.shape
    rows = normed.shape[0]
    own_rows = rows // kv
    products = [
        lax.dot_general(
            normed,
            weight.reshape(-1, width),
            (((1,), (1,)), ((), ())),
            preferred_element_type=jnp.float32,
        ).astype(jnp.bfloat16)
        for weight in (query_weight, forget_weight, value_weight, gate_weight)
    ]
    product = jnp.stack(products, axis=1).reshape(kv, own_rows * 4 * local_heads, local_chan)
    exchanged = lax.all_to_all(product, "kv", split_axis=0, concat_axis=0, tiled=True)
    channels = jnp.moveaxis(exchanged.reshape(kv, own_rows, 4, local_heads, local_chan), 0, 3)
    channels = channels.reshape(own_rows, 4, local_heads, kv * local_chan).astype(jnp.float32)
    pre_query, pre_forget, value_rows, pre_gate = (channels[:, i] for i in range(4))
    log_forget = jnp.logaddexp(
        jnp.log(lower_bound),
        jnp.log1p(-lower_bound) + jax.nn.log_sigmoid(pre_forget),
    )
    key_rows = -jnp.expm1(log_forget)
    next_state = (
        jnp.exp(log_forget)[:, :, :, None] * recurrent_state
        + key_rows[:, :, :, None] * value_rows[:, :, None, :]
    )
    query_act = jax.nn.silu(pre_query)
    readout = jnp.einsum("bhk,bhkv->bhv", query_act, next_state, precision=lax.Precision.HIGHEST)
    inv_head = lax.rsqrt(jnp.mean(readout * readout, axis=2, keepdims=True) + epsilon)
    mixed_heads = (readout * inv_head * head_gain * jax.nn.silu(pre_gate)).astype(jnp.bfloat16)
    mixed = gather_blocks(mixed_heads.reshape(own_rows, -1), members)
    mixed = jnp.swapaxes(mixed.reshape(kv, tp, own_rows, -1), 1, 2).reshape(rows, -1)
    out_matrix = out_weight.reshape(-1, out_weight.shape[2])
    projected = jnp.dot(mixed, out_matrix, preferred_element_type=jnp.float32)
    residual = lax.optimization_barrier(
        (tokens.astype(jnp.float32) + projected).astype(jnp.bfloat16)
    )
    normed_mlp = normed_rows(whole_rows(residual, members), mlp_gain)
    hidden = jnp.square(
        jax.nn.relu(jnp.dot(normed_mlp, up_weight, preferred_element_type=jnp.float32))
    ).astype(jnp.bfloat16)
    partial = jnp.dot(hidden, down_weight, preferred_element_type=jnp.float32)
    partial = jnp.swapaxes(partial.reshape(rows, members, -1), 0, 1)
    summed = lax.all_to_all(partial, group, split_axis=0, concat_axis=0, tiled=True).sum(axis=0)
    layer_output = (residual.astype(jnp.float32) + summed).astype(jnp.bfloat16)
    return (layer_output, next_state)


def solution(mesh):
    placed = (
        P("dp", ("kv", "tp")),
        P(),
        P("tp", "kv", None),
        P("tp", "kv", None),
        P("tp", "kv", None),
        P("tp", "kv", None),
        P("tp", None),
        P(("dp", "kv"), "tp", None, None),
        P("tp", None),
        P(None, None, ("kv", "tp")),
        P(),
        P(None, ("kv", "tp")),
        P(("kv", "tp"), None),
    )

    def body(*arrays):
        return local(mesh.shape["kv"], mesh.shape["tp"], *arrays)

    return jax.shard_map(
        body,
        mesh=mesh,
        in_specs=placed,
        out_specs=(P("dp", ("kv", "tp")), P(("dp", "kv"), "tp", None, None)),
        check_vma=False,
    )
```

time: 149 us -> 73 us (0.49)
  waiting for transfers between devices: 46.4 us -> 10.7 us
  blocking collectives: 45 us -> 25.6 us
  between operations: 14.2 us -> 0.86 us
  other arithmetic: 8.09 us -> 3.13 us
  starting transfers between devices: 14.4 us -> 9.61 us
  matrix products: 17.1 us -> 18.6 us
    all_gather x4 -> x0, blocking collectives: 45 us -> none  [the longest x2 30 us: normed_rows(): lax.all_gather(row_block, ('kv', 'tp'), axis=1, tiled=True)]
    reduce_scatter x1 -> x0, waiting for transfers between devices: 29.9 us -> none  [local(): lax.psum_scatter(jnp.dot(hidden, down_weight, preferred_element_type=jnp....]
    all_to_all x0 -> x3, blocking collectives: none -> 25.6 us  [the longest x2 16.4 us: gather_blocks(): lax.all_to_all(copies, group, split_axis=0, concat_axis=0, tiled=True)]
    all_to_all x4 -> x2, waiting for transfers between devices: 16.5 us -> 10.7 us  [the longest x1 5.55 us: local(): lax.all_to_all(product, 'kv', split_axis=0, concat_axis=0, tiled=True)]
    all_to_all x4 -> x2, starting transfers between devices: 14.4 us -> 9.61 us  [the longest x1 6.35 us: gather_blocks(): lax.all_to_all(copies, group, split_axis=0, concat_axis=0, tiled=True)]
    another operation x1, other arithmetic: 4.36 us -> 0.02 us  [local(): jnp.stack(products, axis=1)]
    unnamed x24 -> x22, local copies, waits for them, and re-layouts: 3.14 us -> 1.21 us
    broadcast_in_dim x0 -> x3, local copies, waits for them, and re-layouts: none -> 1.51 us  [gather_blocks(): jnp.broadcast_to(block[None], (members,) + block.shape)]
  transfers between devices with their start and end apart: 5 -> 2, of which waited for: 5 -> 2; matrix products, arithmetic and copies ran while one was open for 4% -> 1% of each run, Pallas kernels for 0% -> 0%
where the time goes in v1:
time: 73 us; the launch traced here: 72.4 us
  blocking collectives  25.6 us (35%)
  matrix products  18.6 us (25%)
  waiting for transfers between devices  10.7 us (15%)
  starting transfers between devices  9.61 us (13%)
  local copies, waits for them, and re-layouts  3.99 us (5%)
  other arithmetic  3.13 us (4%)
  between operations  0.86 us (1%)
    all_to_all x2, blocking collectives, gather_blocks(): lax.all_to_all(copies, group, split_axis=0, concat_axis=0, tiled=True)  16.4 us
    dot_general x1, matrix products, local(): partial = jnp.dot(hidden, down_weight, preferred_element_type=jnp.float32)  12.9 us
    all_to_all x1, blocking collectives, local(): lax.all_to_all(partial, group, split_axis=0, concat_axis=0, tiled=True)  9.14 us
    all_to_all x1, starting transfers between devices, gather_blocks(): lax.all_to_all(copies, group, split_axis=0, concat_axis=0, tiled=True)  6.35 us
    all_to_all x1, waiting for transfers between devices, local(): lax.all_to_all(product, 'kv', split_axis=0, concat_axis=0, tiled=True)  5.55 us
    all_to_all x1, waiting for transfers between devices, gather_blocks(): lax.all_to_all(copies, group, split_axis=0, concat_axis=0, tiled=True)  5.2 us
    dot_general x4, matrix products, local(): lax.dot_general(normed, weight.reshape(-1, width), (((1,), (1,)), ((), ()...  4.34 us
    all_to_all x1, starting transfers between devices, local(): lax.all_to_all(product, 'kv', split_axis=0, concat_axis=0, tiled=True)  3.25 us
  transfers between devices with their start and end apart: 2, of which 2 were waited for; matrix products, arithmetic and copies ran while one was open for 1% of the time, Pallas kernels for 0%

profile of v1, /device:TPU:0, one launch (start us, length us, event | category | flops | bytes accessed | tf_op | source)
XLA Modules:
  0.0 72.4 jit_solution(3648265302916928768)
XLA Ops:
  0.6 1.5 %broadcast_in_dim.8 = bf16[8,8,512]{2,1,0:T(8,128)(2,1)} broadcast(bf16[8,512]{1,0:T(8,128)(2,1)} %param.13), dimensions={1,2} | broadcast | bytes 73728 | tf_op jit(solution)/shard_map/broadcast_in_dim | solution.py:11
  2.1 6.4 %all-to-all-start = ((bf16[8,8,512]{2,1,0:T(8,128)(2,1)}), bf16[8,8,512]{2,1,0:T(8,128)(2,1)S(1)}, u32[]{:S(2)}, u32[]{:S(2)}) async-start(bf16[8,8,512]{2,1,0:T(8,128)(2,1)} %broadcast_in_dim.8), calls=%async_computation | async-start | bytes 131072 | tf_op jit(solution)/shard_map/all_to_all | solution.py:12
  8.5 0.7 mul.109
  9.2 5.2 %all-to-all-done = bf16[8,8,512]{2,1,0:T(8,128)(2,1)S(1)} async-done(((bf16[8,8,512]{2,1,0:T(8,128)(2,1)}), bf16[8,8,512]{2,1,0:T(8,128)(2,1)S(1)}, u32[]{:S(2)}, u32[]{:S(2)}) %all-to-all-start) | async-done | bytes 65568 | tf_op jit(solution)/shard_map/all_to_all | solution.py:12
  14.4 0.1 fusion.8
  14.7 2.4 %fusion.6 = bf16[8,1,256]{2,0,1:T(8,128)(2,1)S(1)} fusion(bf16[8,4096]{1,0:T(8,128)(2,1)S(1)} %bitcast.84, bf16[256,4096]{1,0:T(8,128)(2,1)} %bitcast.80), kind=kOutput, calls=%fused_computation.12 | convolution fusion | flops 16779264 | bytes 2166784 | tf_op jit(solution)/shard_map/dot_general | solution.py:49
  17.1 0.7 fusion.5
  17.7 0.7 fusion.4
  18.4 0.3 copy-done.4
  18.7 0.6 fusion.3
  19.6 0.7 reshape.161
  20.3 3.3 %all-to-all-start.1 = ((bf16[4,2,1024]{2,1,0:T(2,128)(2,1)}), bf16[4,2,1024]{2,1,0:T(2,128)(2,1)S(1)}, u32[]{:S(2)}, u32[]{:S(2)}) async-start(bf16[4,2,1024]{2,1,0:T(2,128)(2,1)} %reshape.161), calls=%async_computation.1 | async-start | bytes 32768 | tf_op jit(solution)/shard_map/all_to_all | solution.py:58
  23.6 5.6 %all-to-all-done.1 = bf16[4,2,1024]{2,1,0:T(2,128)(2,1)S(1)} async-done(((bf16[4,2,1024]{2,1,0:T(2,128)(2,1)}), bf16[4,2,1024]{2,1,0:T(2,128)(2,1)S(1)}, u32[]{:S(2)}, u32[]{:S(2)}) %all-to-all-start.1) | async-done | bytes 16416 | tf_op jit(solution)/shard_map/all_to_all | solution.py:58
  29.3 0.1 copy.28
  29.5 0.1 reshape.156
  29.7 1.8 %multiply_add_fusion = f32[2,8,128,128]{3,2,1,0:T(8,128)S(1)} fusion(f32[2,8,128,128]{3,2,1,0:T(8,128)} %param.20, f32[2,8,128]{2,1,0:T(8,128)S(1)} %slice_bitcast_fusion.1, f32[2,8,128]{2,1,0:T(8,128)S(1)} %exponential-minus-one_negate_fusion, f32[2,8,128]{2,1,0:T(8,128)S(1)} %get-tuple-element.2), kind=kLoop, calls=%fused_computation.13 | loop fusion | flops 786432 | bytes 2121728 | tf_op jit(solution)/shard_map/add | solution.py:68
  31.6 1.0 %fusion.23 = f32[2,8,1,128]{3,2,1,0:T(1,128)S(1)} fusion(f32[2,8,128,1]{2,3,1,0:T(1,128)S(1)} %bitcast.98, f32[2,8,128,128]{3,2,1,0:T(8,128)S(1)} %multiply_add_fusion), kind=kOutput, calls=%fused_computation.50 | convolution fusion | flops 3145728 | bytes 1064960 | tf_op jit(solution)/shard_map/bhk,bhkv->bhv/dot_general | solution.py:72
  32.8 8.1 %all_to_all.25 = bf16[8,2,1024]{2,1,0:T(2,128)(2,1)S(1)} all-to-all(bf16[8,2,1024]{2,1,0:T(2,128)(2,1)S(1)} %broadcast_in_dim.10), channel_id=1, replica_groups=mesh['dp'=4,'kv'=4,'tp'=2] {'kv','tp'}, dimensions={0} | all-to-all | bytes 65536 | tf_op jit(solution)/shard_map/all_to_all | solution.py:12
  40.9 0.4 fusion.2
  41.3 8.3 %all_to_all.26 = bf16[8,8,512]{2,1,0:T(8,128)(2,1)S(1)} all-to-all(bf16[8,8,512]{2,1,0:T(8,128)(2,1)S(1)} %broadcast_in_dim.11), channel_id=1, replica_groups=mesh['dp'=4,'kv'=4,'tp'=2] {'kv','tp'}, dimensions={0} | all-to-all | bytes 131072 | tf_op jit(solution)/shard_map/all_to_all | solution.py:12
  49.6 0.1 multiply_reduce_fusion
  49.8 12.9 %fusion.7 = f32[8,4096]{1,0:T(8,128)S(1)} fusion(bf16[2048,4096]{1,0:T(8,128)(2,1)} %param.25, bf16[4096,2048]{1,0:T(8,128)(2,1)} %param.24, f32[8,4096]{1,0:T(8,128)S(1)} %bitcast.88, f32[4096]{0:T(1024)S(1)} %copy-done.6, f32[8]{0:T(128)S(1)} %add_rsqrt_fusion.1), kind=kOutput, calls=%fused_computation.14 | convolution fusion | flops 268582912 | bytes 33832992 | tf_op jit(solution)/shard_map/dot_general | solution.py:86
  62.7 9.1 %all_to_all.27 = f32[8,8,512]{2,1,0:T(8,128)S(1)} all-to-all(f32[8,8,512]{2,1,0:T(8,128)S(1)} %bitcast.89), channel_id=1, replica_groups=mesh['dp'=4,'kv'=4,'tp'=2] {'kv','tp'}, dimensions={0} | all-to-all | bytes 262144 | tf_op jit(solution)/shard_map/all_to_all | solution.py:88
  71.8 0.6 add_convert_fusion
  (41 shorter events, 0.9 us)
Async XLA Ops:
  0.6 40.3 %copy-start = (bf16[16,128,512]{2,1,0:T(8,128)(2,1)S(1)}, bf16[16,128,512]{2,1,0:T(8,128)(2,1)}, u32[]{:S(2)}) copy-start(bf16[16,128,512]{2,1,0:T(8,128)(2,1)} %param.22) | copy-start | bytes 6291460
  2.1 12.3 %all-to-all-start = ((bf16[8,8,512]{2,1,0:T(8,128)(2,1)}), bf16[8,8,512]{2,1,0:T(8,128)(2,1)S(1)}, u32[]{:S(2)}, u32[]{:S(2)}) async-start(bf16[8,8,512]{2,1,0:T(8,128)(2,1)} %broadcast_in_dim.8), calls=%async_computation | async-start | bytes 131072 | tf_op jit(solution)/shard_map/all_to_all | solution.py:12
  14.4 2.7 %copy-start.2 = (bf16[8,32,4096]{2,1,0:T(8,128)(2,1)S(1)}, bf16[8,32,4096]{2,1,0:T(8,128)(2,1)}, u32[]{:S(2)}) copy-start(bf16[8,32,4096]{2,1,0:T(8,128)(2,1)} %param.17) | copy-start | bytes 6291460
  14.7 3.1 %copy-start.3 = (bf16[8,32,4096]{2,1,0:T(8,128)(2,1)S(1)}, bf16[8,32,4096]{2,1,0:T(8,128)(2,1)}, u32[]{:S(2)}) copy-start(bf16[8,32,4096]{2,1,0:T(8,128)(2,1)} %param.16) | copy-start | bytes 6291460
  17.1 1.7 %copy-start.4 = (bf16[8,32,4096]{2,1,0:T(8,128)(2,1)S(1)}, bf16[8,32,4096]{2,1,0:T(8,128)(2,1)}, u32[]{:S(2)}) copy-start(bf16[8,32,4096]{2,1,0:T(8,128)(2,1)} %param.15) | copy-start | bytes 6291460
  17.7 5.9 %copy-start.7 = (f32[8,128]{1,0:T(8,128)S(1)}, f32[8,128]{1,0:T(8,128)}, u32[]{:S(2)}) copy-start(f32[8,128]{1,0:T(8,128)} %param.19) | copy-start | bytes 12292
  19.6 13.0 %copy-start.8 = (f32[8,128]{1,0:T(8,128)S(1)}, f32[8,128]{1,0:T(8,128)}, u32[]{:S(2)}) copy-start(f32[8,128]{1,0:T(8,128)} %param.21) | copy-start | bytes 12292
  20.3 8.8 %all-to-all-start.1 = ((bf16[4,2,1024]{2,1,0:T(2,128)(2,1)}), bf16[4,2,1024]{2,1,0:T(2,128)(2,1)S(1)}, u32[]{:S(2)}, u32[]{:S(2)}) async-start(bf16[4,2,1024]{2,1,0:T(2,128)(2,1)} %reshape.161), calls=%async_computation.1 | async-start | bytes 32768 | tf_op jit(solution)/shard_map/all_to_all | solution.py:58
  29.4 11.6 %copy-start.5 = (bf16[8,512]{1,0:T(8,128)(2,1)S(1)}, bf16[8,512]{1,0:T(8,128)(2,1)}, u32[]{:S(2)}) copy-start(bf16[8,512]{1,0:T(8,128)(2,1)} %param.13) | copy-start | bytes 24580
  31.5 31.2 %copy-start.1 = (f32[2,8,128,128]{3,2,1,0:T(8,128)}, f32[2,8,128,128]{3,2,1,0:T(8,128)S(1)}, u32[]{:S(2)}) copy-start(f32[2,8,128,128]{3,2,1,0:T(8,128)S(1)} %multiply_add_fusion) | copy-start | bytes 3145732
  31.5 18.3 %copy-start.6 = (f32[4096]{0:T(1024)S(1)}, f32[4096]{0:T(1024)}, u32[]{:S(2)}) copy-start(f32[4096]{0:T(1024)} %param.23) | copy-start | bytes 49156

commit v2 on v1

--- a/solution.py
+++ b/solution.py
@@ -1,6 +1,10 @@
+import functools
+
 import jax
 import jax.numpy as jnp
 from jax import lax
+from jax.experimental import pallas as pl
+from jax.experimental.pallas import tpu as pltpu
 from jax.sharding import PartitionSpec as P
 
 epsilon = 1e-06
@@ -90,6 +94,231 @@
     return (layer_output, next_state)
 
 
+whole = pl.BlockSpec(memory_space=pltpu.VMEM)
+
+
+def call(body, outs, arrays, flops, moved, limit):
+    return pl.pallas_call(
+        body,
+        out_shape=outs,
+        in_specs=[whole] * len(arrays),
+        out_specs=jax.tree.map(lambda _: whole, outs),
+        compiler_params=pltpu.CompilerParams(vmem_limit_bytes=limit),
+        cost_estimate=pl.CostEstimate(flops=flops, bytes_accessed=moved, transcendentals=0),
+    )(*arrays)
+
+
+def spread_kernel(block_ref, copies_ref):
+    for dest in range(copies_ref.shape[0]):
+        copies_ref[dest] = block_ref[...]
+
+
+def normed_pieces(pieces_ref, gain_ref):
+    rows = jnp.concatenate([pieces_ref[i] for i in range(pieces_ref.shape[0])], axis=1)
+    rows = rows.astype(jnp.float32)
+    inv_root = lax.rsqrt(jnp.mean(rows * rows, axis=1, keepdims=True) + epsilon)
+    return (rows * inv_root * gain_ref[...]).astype(jnp.bfloat16)
+
+
+def project_kernel(pieces_ref, gain_ref, query_ref, forget_ref, value_ref, gate_ref, sent_ref):
+    normed = normed_pieces(pieces_ref, gain_ref)
+    rows = normed.shape[0]
+    heads, chan, _ = query_ref.shape
+    lanes = 4 * chan
+    for head in range(0, heads, 2):
+        weight = jnp.concatenate(
+            [
+                ref[one]
+                for one in (head, head + 1)
+                for ref in (query_ref, forget_ref, value_ref, gate_ref)
+            ],
+            axis=0,
+        )
+        product = lax.dot_general(
+            normed, weight, (((1,), (1,)), ((), ())), preferred_element_type=jnp.float32
+        )
+        product = product.astype(jnp.bfloat16).astype(jnp.float32)
+        sent_ref[pl.ds(head, rows, stride=heads), :] = product[:, :lanes]
+        sent_ref[pl.ds(head + 1, rows, stride=heads), :] = product[:, lanes:]
+
+
+def sigmoid(x):
+    return 1.0 / (1.0 + jnp.exp(-x))
+
+
+def state_kernel(got_ref, bound_ref, state_ref, gain_ref, next_ref, copies_ref):
+    sources, pairs, _ = got_ref.shape
+    own_rows, heads, keys, values = state_ref.shape
+    chan = keys // sources
+
+    def channels(kind):
+        return jnp.concatenate(
+            [got_ref[i][:, kind * chan : (kind + 1) * chan] for i in range(sources)], axis=1
+        )
+
+    pre_query, pre_forget, value_rows, pre_gate = (channels(kind) for kind in range(4))
+    bound = jnp.concatenate([bound_ref[...]] * own_rows, axis=0)
+    gain = jnp.concatenate([gain_ref[...]] * own_rows, axis=0)
+    forget = jnp.transpose(bound + (1.0 - bound) * sigmoid(pre_forget))
+    key_cols = jnp.transpose((1.0 - bound) * sigmoid(-pre_forget))
+    query = jnp.transpose(pre_query * sigmoid(pre_query))
+    readouts = []
+    for row in range(own_rows):
+        for head in range(heads):
+            pair = row * heads + head
+            one = slice(pair, pair + 1)
+            state = forget[:, one] * state_ref[row, head] + key_cols[:, one] * value_rows[one]
+            next_ref[row, head] = state
+            readouts.append(jnp.sum(query[:, one] * state, axis=0, keepdims=True))
+    readout = jnp.concatenate(readouts, axis=0)
+    inv_head = lax.rsqrt(jnp.mean(readout * readout, axis=1, keepdims=True) + epsilon)
+    mixed = readout * inv_head * gain * (pre_gate * sigmoid(pre_gate))
+    mixed = mixed.astype(jnp.bfloat16).astype(jnp.float32)
+    for dest in range(copies_ref.shape[0]):
+        copies_ref[dest] = mixed
+
+
+def out_kernel(kv, tp, heads, tokens_ref, mixed_ref, weight_ref, copies_ref, residual_ref):
+    pairs, rows = mixed_ref.shape[0] // (kv * tp), tokens_ref.shape[0]
+    own_rows = pairs // heads
+    blocks = []
+    for part in range(tp):
+        for head in range(heads):
+            blocks.append(
+                jnp.concatenate(
+                    [
+                        mixed_ref[pl.ds(part * pairs + row * heads + head, kv, stride=tp * pairs), :]
+                        for row in range(own_rows)
+                    ],
+                    axis=0,
+                )
+            )
+    mixed = jnp.concatenate(blocks, axis=1).astype(jnp.bfloat16)
+    width = weight_ref.shape[2]
+    weight = weight_ref[...].reshape(-1, width)
+    projected = jnp.dot(mixed, weight, preferred_element_type=jnp.float32)
+    ordered = [
+        projected[row * kv + i : row * kv + i + 1] for i in range(kv) for row in range(own_rows)
+    ]
+    projected = jnp.concatenate(ordered, axis=0)
+    residual = (tokens_ref[...].astype(jnp.float32) + projected).astype(jnp.bfloat16)
+    residual_ref[...] = residual
+    for dest in range(copies_ref.shape[0]):
+        copies_ref[dest] = residual
+
+
+def mixer_kernel(pieces_ref, gain_ref, up_ref, down_ref, partial_ref):
+    members, _, width = partial_ref.shape
+    normed = normed_pieces(pieces_ref, gain_ref)
+    hidden = jnp.dot(normed, up_ref[...], preferred_element_type=jnp.float32)
+    hidden = jnp.square(jnp.maximum(hidden, 0.0)).astype(jnp.bfloat16)
+    for dest in range(members):
+        partial_ref[dest] = jnp.dot(
+            hidden,
+            down_ref[:, dest * width : (dest + 1) * width],
+            preferred_element_type=jnp.float32,
+        )
+
+
+def last_kernel(residual_ref, partial_ref, output_ref):
+    total = partial_ref[0]
+    for source in range(1, partial_ref.shape[0]):
+        total = total + partial_ref[source]
+    output_ref[...] = (residual_ref[...].astype(jnp.float32) + total).astype(jnp.bfloat16)
+
+
+MIB = 1 << 20
+
+
+def tiled_local(
+    kv,
+    tp,
+    tokens,
+    mix_gain,
+    query_weight,
+    forget_weight,
+    value_weight,
+    gate_weight,
+    lower_bound,
+    recurrent_state,
+    head_gain,
+    out_weight,
+    mlp_gain,
+    up_weight,
+    down_weight,
+):
+    members = kv * tp
+    rows, width = tokens.shape
+    heads, chan, model = query_weight.shape
+    own_rows, _, keys, values = recurrent_state.shape
+    pairs = own_rows * heads
+    shape = jax.ShapeDtypeStruct
+    exchange = functools.partial(lax.all_to_all, split_axis=0, concat_axis=0, tiled=True)
+
+    copies = call(
+        spread_kernel, shape((members, rows, width), jnp.bfloat16), (tokens,), COST[0], 0, MIB
+    )
+    pieces = exchange(copies, group)
+    sent = call(
+        project_kernel,
+        shape((rows * heads, 4 * chan), jnp.float32),
+        (
+            pieces,
+            mix_gain.reshape(1, -1),
+            query_weight,
+            forget_weight,
+            value_weight,
+            gate_weight,
+        ),
+        COST[1],
+        0,
+        4 * MIB,
+    )
+    got = exchange(sent.reshape(kv, pairs, 4 * chan), "kv")
+    next_state, copies = call(
+        state_kernel,
+        (
+            shape(recurrent_state.shape, jnp.float32),
+            shape((members, pairs, values), jnp.float32),
+        ),
+        (got, lower_bound, recurrent_state, head_gain),
+        COST[2],
+        0,
+        4 * MIB,
+    )
+    mixed = exchange(copies, group)
+    copies, residual = call(
+        functools.partial(out_kernel, kv, tp, heads),
+        (shape((members, rows, width), jnp.bfloat16), shape((rows, width), jnp.bfloat16)),
+        (tokens, mixed.reshape(members * pairs, values), out_weight),
+        COST[3],
+        0,
+        4 * MIB,
+    )
+    pieces = exchange(copies, group)
+    partial = call(
+        mixer_kernel,
+        shape((members, rows, width), jnp.float32),
+        (pieces, mlp_gain.reshape(1, -1), up_weight, down_weight),
+        COST[4],
+        0,
+        4 * MIB,
+    )
+    partial = exchange(partial, group)
+    layer_output = call(
+        last_kernel, shape((rows, width), jnp.bfloat16), (residual, partial), COST[5], 0, MIB
+    )
+    return (layer_output, next_state)
+
+
+COST = (10**11, 10**11, 10**11, 10**6, 10**6, 10**6)
+
+
+def tiles(tokens, query_weight):
+    rows, width = tokens.shape
+    return rows % 8 == 0 and width % 128 == 0 and query_weight.shape[1] % 32 == 0
+
+
 def solution(mesh):
     placed = (
         P("dp", ("kv", "tp")),
@@ -108,7 +337,8 @@
     )
 
     def body(*arrays):
-        return local(mesh.shape["kv"], mesh.shape["tp"], *arrays)
+        run = tiled_local if tiles(arrays[0], arrays[2]) else local
+        return run(mesh.shape["kv"], mesh.shape["tp"], *arrays)
 
     return jax.shard_map(
         body,

time: 73 us -> 59.1 us (0.81)
  blocking collectives: 25.6 us -> 47.1 us
  matrix products: 18.6 us -> 0 us
  waiting for transfers between devices: 10.7 us -> 0 us
  Pallas kernels: 0 us -> 9.97 us
  starting transfers between devices: 9.61 us -> 0 us
  local copies, waits for them, and re-layouts: 3.99 us -> 0.79 us
  other arithmetic: 3.13 us -> 0.01 us
    all_to_all x3 -> x5, blocking collectives: 25.6 us -> 47.1 us  [the longest x2 20.6 us: tiled_local(): pieces = exchange(copies, group)]
    dot_general x7 -> x0, matrix products: 18.6 us -> none  [the longest x1 12.9 us: local(): partial = jnp.dot(hidden, down_weight, preferred_element_type=jnp.float32)]
    all_to_all x2 -> x0, waiting for transfers between devices: 10.7 us -> none  [the longest x1 5.55 us: local(): lax.all_to_all(product, 'kv', split_axis=0, concat_axis=0, tiled=True)]
    pallas_call x0 -> x6, Pallas kernels: none -> 9.97 us  [call(): pl.pallas_call(body, out_shape=outs, in_specs=[whole] * len(arrays), out_...]
    all_to_all x2 -> x0, starting transfers between devices: 9.61 us -> none  [the longest x1 6.35 us: gather_blocks(): lax.all_to_all(copies, group, split_axis=0, concat_axis=0, tiled=True)]
    add x1 -> x0, other arithmetic: 1.83 us -> none  [local(): jnp.exp(log_forget)[:, :, :, None] * recurrent_state]
    broadcast_in_dim x3 -> x0, local copies, waits for them, and re-layouts: 1.51 us -> none  [gather_blocks(): jnp.broadcast_to(block[None], (members,) + block.shape)]
  transfers between devices with their start and end apart: 2 -> 0, of which waited for: 2 -> 0; matrix products, arithmetic and copies ran while one was open for 1% -> 0% of each run, Pallas kernels for 0% -> 0%
where the time goes in v2:
time: 59.1 us; the launch traced here: 58.7 us
  blocking collectives  47.1 us (80%)
  Pallas kernels  9.97 us (17%)
  between operations  0.85 us (1%)
  local copies, waits for them, and re-layouts  0.79 us (1%)
    all_to_all x2, blocking collectives, tiled_local(): pieces = exchange(copies, group)  20.6 us
    pallas_call x6, Pallas kernels, call(): pl.pallas_call(body, out_shape=outs, in_specs=[whole] * len(arrays), out_...  9.97 us
    all_to_all x1, blocking collectives, tiled_local(): partial = exchange(partial, group)  9.14 us
    all_to_all x1, blocking collectives, tiled_local(): mixed = exchange(copies, group)  8.81 us
    all_to_all x1, blocking collectives, tiled_local(): got = exchange(sent.reshape(kv, pairs, 4 * chan), 'kv')  8.55 us

profile of v2, /device:TPU:0, one launch (start us, length us, event | category | flops | bytes accessed | tf_op | source)
XLA Modules:
  0.0 58.7 jit_solution(4380742619919215191)
XLA Ops:
  0.6 0.0 copy-start.2
  0.6 0.7 %copy-done.2 = bf16[8,512]{1,0:T(8,128)(2,1)S(1)} copy-done((bf16[8,512]{1,0:T(8,128)(2,1)S(1)}, bf16[8,512]{1,0:T(8,128)(2,1)}, u32[]{:S(2)}) %copy-start.2) | copy-done | bytes 8216
  1.3 0.0 copy-start.9
  1.4 12.3 %all_to_all.25.pieces_ref = bf16[8,8,512]{2,1,0:T(8,128)(2,1)S(1)} all-to-all(bf16[8,8,512]{2,1,0:T(8,128)(2,1)S(1)} %shard_map.140), channel_id=1, replica_groups=mesh['dp'=4,'kv'=4,'tp'=2] {'kv','tp'}, dimensions={0} | all-to-all | bytes 131072 | tf_op jit(solution)/shard_map/all_to_all | solution.py:261
  13.7 0.0 copy-start.8
  13.7 0.0 copy-start.10
  13.8 0.0 copy-start.11
  13.8 2.3 %shard_map.141 = f32[64,128]{1,0:T(8,128)S(1)} custom-call(bf16[8,8,512]{2,1,0:T(8,128)(2,1)S(1)} %all_to_all.25.pieces_ref, f32[1,4096]{1,0:T(1,128)S(1)} %bitcast.11, bf16[8,32,4096]{2,1,0:T(8,128)(2,1)S(1)} %copy-done.4, bf16[8,32,4096]{2,1,0:T(8,128)(2,1)S(1)} %copy-done.5, bf16[8,32,4096]{2,1,0:T(8,128)(2,1)S(1)} %copy-done.6, ...), custom_call_target="tpu_custom_call" | custom-call | flops 99999997952 | tf_op jit(solution)/shard_map/pallas_call | solution.py:101
  16.1 8.5 %all_to_all.26.got_ref = f32[4,16,128]{2,1,0:T(8,128)S(1)} all-to-all(f32[4,16,128]{2,1,0:T(8,128)S(1)} %bitcast.9), channel_id=1, replica_groups=mesh['dp'=4,'kv'=4,'tp'=2] {'kv'}, dimensions={0} | all-to-all | bytes 65536 | tf_op jit(solution)/shard_map/all_to_all | solution.py:277
  24.6 0.0 copy-start
  24.7 0.0 copy-start.3
  24.7 0.0 slice-start.1
  24.7 0.0 slice-start.2
  24.7 0.0 slice-start.3
  24.7 0.0 slice-start.5
  24.7 0.0 slice-start.6
  24.7 0.0 slice-start.7
  24.7 2.1 %shard_map.142 = (f32[2,8,128,128]{3,2,1,0:T(8,128)}, f32[8,16,128]{2,1,0:T(8,128)S(1)}) custom-call(f32[4,16,128]{2,1,0:T(8,128)S(1)} %all_to_all.26.got_ref, f32[8,128]{1,0:T(8,128)S(1)} %copy-done.10, f32[2,8,128,128]{3,2,1,0:T(8,128)S(1)} %copy-done.8, f32[8,128]{1,0:T(8,128)S(1)} %copy-done.11), custom_call_target="tpu_custom_call" | custom-call | flops 99999997952 | tf_op jit(solution)/shard_map/pallas_call | solution.py:101
  26.9 8.8 %all_to_all.27 = f32[8,16,128]{2,1,0:T(8,128)S(1)} all-to-all(f32[8,16,128]{2,1,0:T(8,128)S(1)} %get-tuple-element.6), channel_id=1, replica_groups=mesh['dp'=4,'kv'=4,'tp'=2] {'kv','tp'}, dimensions={0} | all-to-all | bytes 131072 | tf_op jit(solution)/shard_map/all_to_all | solution.py:289
  35.7 0.4 shard_map.143
  36.1 8.3 %all_to_all.28.pieces_ref = bf16[8,8,512]{2,1,0:T(8,128)(2,1)S(1)} all-to-all(bf16[8,8,512]{2,1,0:T(8,128)(2,1)S(1)} %get-tuple-element.8), channel_id=1, replica_groups=mesh['dp'=4,'kv'=4,'tp'=2] {'kv','tp'}, dimensions={0} | all-to-all | bytes 131072 | tf_op jit(solution)/shard_map/all_to_all | solution.py:298
  44.5 4.5 %shard_map.144 = f32[8,8,512]{2,1,0:T(8,128)S(1)} custom-call(bf16[8,8,512]{2,1,0:T(8,128)(2,1)S(1)} %all_to_all.28.pieces_ref, f32[1,4096]{1,0:T(1,128)S(1)} %bitcast.10, bf16[4096,2048]{1,0:T(8,128)(2,1)S(1)} %bitcast.5, bf16[2048,4096]{1,0:T(8,128)(2,1)S(1)} %bitcast.7), custom_call_target="tpu_custom_call" | custom-call | flops 1000000 | tf_op jit(solution)/shard_map/pallas_call | solution.py:101
  49.0 9.1 %all_to_all.29.partial_ref = f32[8,8,512]{2,1,0:T(8,128)S(1)} all-to-all(f32[8,8,512]{2,1,0:T(8,128)S(1)} %shard_map.144), channel_id=1, replica_groups=mesh['dp'=4,'kv'=4,'tp'=2] {'kv','tp'}, dimensions={0} | all-to-all | bytes 262144 | tf_op jit(solution)/shard_map/all_to_all | solution.py:307
  58.1 0.6 %shard_map.145 = bf16[8,512]{1,0:T(8,128)(2,1)} custom-call(bf16[8,512]{1,0:T(8,128)(2,1)S(1)} %get-tuple-element.7.residual_ref, f32[8,8,512]{2,1,0:T(8,128)S(1)} %all_to_all.29.partial_ref), custom_call_target="tpu_custom_call" | custom-call | flops 1000000 | tf_op jit(solution)/shard_map/pallas_call | solution.py:101
  (29 shorter events, 0.1 us)
Async XLA Ops:
  0.6 0.7 %copy-start.2 = (bf16[8,512]{1,0:T(8,128)(2,1)S(1)}, bf16[8,512]{1,0:T(8,128)(2,1)}, u32[]{:S(2)}) copy-start(bf16[8,512]{1,0:T(8,128)(2,1)} %tokens_ref.1) | copy-start | bytes 24580
  1.3 12.4 %copy-start.4 = (bf16[8,32,4096]{2,1,0:T(8,128)(2,1)S(1)}, bf16[8,32,4096]{2,1,0:T(8,128)(2,1)}, u32[]{:S(2)}) copy-start(bf16[8,32,4096]{2,1,0:T(8,128)(2,1)} %query_ref.1) | copy-start | bytes 6291460
  1.3 12.4 %copy-start.5 = (bf16[8,32,4096]{2,1,0:T(8,128)(2,1)S(1)}, bf16[8,32,4096]{2,1,0:T(8,128)(2,1)}, u32[]{:S(2)}) copy-start(bf16[8,32,4096]{2,1,0:T(8,128)(2,1)} %forget_ref.1) | copy-start | bytes 6291460
  1.3 12.4 %copy-start.6 = (bf16[8,32,4096]{2,1,0:T(8,128)(2,1)S(1)}, bf16[8,32,4096]{2,1,0:T(8,128)(2,1)}, u32[]{:S(2)}) copy-start(bf16[8,32,4096]{2,1,0:T(8,128)(2,1)} %value_ref.1) | copy-start | bytes 6291460
  1.3 12.4 %copy-start.7 = (bf16[8,32,4096]{2,1,0:T(8,128)(2,1)S(1)}, bf16[8,32,4096]{2,1,0:T(8,128)(2,1)}, u32[]{:S(2)}) copy-start(bf16[8,32,4096]{2,1,0:T(8,128)(2,1)} %gate_ref.1) | copy-start | bytes 6291460
  1.3 12.4 %copy-start.9 = (f32[4096]{0:T(1024)S(1)}, f32[4096]{0:T(1024)}, u32[]{:S(2)}) copy-start(f32[4096]{0:T(1024)} %param.14) | copy-start | bytes 49156
  13.7 10.9 %copy-start.8 = (f32[2,8,128,128]{3,2,1,0:T(8,128)S(1)}, f32[2,8,128,128]{3,2,1,0:T(8,128)}, u32[]{:S(2)}) copy-start(f32[2,8,128,128]{3,2,1,0:T(8,128)} %state_ref.1) | copy-start | bytes 3145732
  13.7 10.9 %copy-start.10 = (f32[8,128]{1,0:T(8,128)S(1)}, f32[8,128]{1,0:T(8,128)}, u32[]{:S(2)}) copy-start(f32[8,128]{1,0:T(8,128)} %bound_ref.1) | copy-start | bytes 12292
  13.8 10.9 %copy-start.11 = (f32[8,128]{1,0:T(8,128)S(1)}, f32[8,128]{1,0:T(8,128)}, u32[]{:S(2)}) copy-start(f32[8,128]{1,0:T(8,128)} %gain_ref.1) | copy-start | bytes 12292
  16.1 28.3 %slice-start = ((s8[16777216]{0:T(1024)(128)(4,1)}), s8[4194304]{0:T(1024)(128)(4,1)S(1)}, s32[]{:S(2)}) async-start(s8[16777216]{0:T(1024)(128)(4,1)} %bitcast.4), calls=%async_computation.5 | async-start | bytes 8388608
  16.1 28.3 %slice-start.4 = ((s8[16777216]{0:T(1024)(128)(4,1)}), s8[4194304]{0:T(1024)(128)(4,1)S(1)}, s32[]{:S(2)}) async-start(s8[16777216]{0:T(1024)(128)(4,1)} %bitcast.6), calls=%async_computation.9 | async-start | bytes 8388608
  24.6 11.0 %copy-start = (bf16[16,128,512]{2,1,0:T(8,128)(2,1)S(1)}, bf16[16,128,512]{2,1,0:T(8,128)(2,1)}, u32[]{:S(2)}) copy-start(bf16[16,128,512]{2,1,0:T(8,128)(2,1)} %weight_ref.1) | copy-start | bytes 6291460
  24.7 11.0 %copy-start.3 = (bf16[8,512]{1,0:T(8,128)(2,1)S(1)}, bf16[8,512]{1,0:T(8,128)(2,1)}, u32[]{:S(2)}) copy-start(bf16[8,512]{1,0:T(8,128)(2,1)} %tokens_ref.1) | copy-start | bytes 24580
  24.7 19.7 %slice-start.1 = ((s8[16777216]{0:T(1024)(128)(4,1)}), s8[4194304]{0:T(1024)(128)(4,1)S(1)}, s32[]{:S(2)}) async-start(s8[16777216]{0:T(1024)(128)(4,1)} %bitcast.4), calls=%async_computation.6 | async-start | bytes 8388608
  24.7 19.7 %slice-start.2 = ((s8[16777216]{0:T(1024)(128)(4,1)}), s8[4194304]{0:T(1024)(128)(4,1)S(1)}, s32[]{:S(2)}) async-start(s8[16777216]{0:T(1024)(128)(4,1)} %bitcast.4), calls=%async_computation.7 | async-start | bytes 8388608
  24.7 19.7 %slice-start.3 = ((s8[16777216]{0:T(1024)(128)(4,1)}), s8[4194304]{0:T(1024)(128)(4,1)S(1)}, s32[]{:S(2)}) async-start(s8[16777216]{0:T(1024)(128)(4,1)} %bitcast.4), calls=%async_computation.8 | async-start | bytes 8388608
  24.7 19.7 %slice-start.5 = ((s8[16777216]{0:T(1024)(128)(4,1)}), s8[4194304]{0:T(1024)(128)(4,1)S(1)}, s32[]{:S(2)}) async-start(s8[16777216]{0:T(1024)(128)(4,1)} %bitcast.6), calls=%async_computation.10 | async-start | bytes 8388608
  24.7 19.7 %slice-start.6 = ((s8[16777216]{0:T(1024)(128)(4,1)}), s8[4194304]{0:T(1024)(128)(4,1)S(1)}, s32[]{:S(2)}) async-start(s8[16777216]{0:T(1024)(128)(4,1)} %bitcast.6), calls=%async_computation.11 | async-start | bytes 8388608
  24.7 19.7 %slice-start.7 = ((s8[16777216]{0:T(1024)(128)(4,1)}), s8[4194304]{0:T(1024)(128)(4,1)S(1)}, s32[]{:S(2)}) async-start(s8[16777216]{0:T(1024)(128)(4,1)} %bitcast.6), calls=%async_computation.12 | async-start | bytes 8388608
  26.9 17.6 %copy-start.1 = (f32[4096]{0:T(1024)S(1)}, f32[4096]{0:T(1024)}, u32[]{:S(2)}) copy-start(f32[4096]{0:T(1024)} %param.23) | copy-start | bytes 49156

commit v3 on v2

v3 whole, which is shorter than its diff:
```python
import functools

import jax
import jax.numpy as jnp
from jax import lax
from jax.experimental import pallas as pl
from jax.experimental.pallas import tpu as pltpu
from jax.sharding import PartitionSpec as P


epsilon = 1e-06
group = ("kv", "tp")


def gather_blocks(block, members):
    copies = lax.optimization_barrier(jnp.broadcast_to(block[None], (members,) + block.shape))
    return lax.all_to_all(copies, group, split_axis=0, concat_axis=0, tiled=True)


def whole_rows(row_block, members):
    pieces = gather_blocks(row_block, members)
    return jnp.swapaxes(pieces, 0, 1).reshape(row_block.shape[0], -1)


def normed_rows(rows, gain_vector):
    rows = rows.astype(jnp.float32)
    inv_root = lax.rsqrt(jnp.mean(rows * rows, axis=1, keepdims=True) + epsilon)
    return (rows * inv_root * gain_vector).astype(jnp.bfloat16)


def local(
    kv,
    tp,
    tokens,
    mix_gain,
    query_weight,
    forget_weight,
    value_weight,
    gate_weight,
    lower_bound,
    recurrent_state,
    head_gain,
    out_weight,
    mlp_gain,
    up_weight,
    down_weight,
):
    members = kv * tp
    normed = normed_rows(whole_rows(tokens, members), mix_gain)
    local_heads, local_chan, width = query_weight.shape
    rows = normed.shape[0]
    own_rows = rows // kv
    products = [
        lax.dot_general(
            normed,
            weight.reshape(-1, width),
            (((1,), (1,)), ((), ())),
            preferred_element_type=jnp.float32,
        ).astype(jnp.bfloat16)
        for weight in (query_weight, forget_weight, value_weight, gate_weight)
    ]
    product = jnp.stack(products, axis=1).reshape(kv, own_rows * 4 * local_heads, local_chan)
    exchanged = lax.all_to_all(product, "kv", split_axis=0, concat_axis=0, tiled=True)
    channels = jnp.moveaxis(exchanged.reshape(kv, own_rows, 4, local_heads, local_chan), 0, 3)
    channels = channels.reshape(own_rows, 4, local_heads, kv * local_chan).astype(jnp.float32)
    pre_query, pre_forget, value_rows, pre_gate = (channels[:, i] for i in range(4))
    log_forget = jnp.logaddexp(
        jnp.log(lower_bound),
        jnp.log1p(-lower_bound) + jax.nn.log_sigmoid(pre_forget),
    )
    key_rows = -jnp.expm1(log_forget)
    next_state = (
        jnp.exp(log_forget)[:, :, :, None] * recurrent_state
        + key_rows[:, :, :, None] * value_rows[:, :, None, :]
    )
    query_act = jax.nn.silu(pre_query)
    readout = jnp.einsum("bhk,bhkv->bhv", query_act, next_state, precision=lax.Precision.HIGHEST)
    inv_head = lax.rsqrt(jnp.mean(readout * readout, axis=2, keepdims=True) + epsilon)
    mixed_heads = (readout * inv_head * head_gain * jax.nn.silu(pre_gate)).astype(jnp.bfloat16)
    mixed = gather_blocks(mixed_heads.reshape(own_rows, -1), members)
    mixed = jnp.swapaxes(mixed.reshape(kv, tp, own_rows, -1), 1, 2).reshape(rows, -1)
    out_matrix = out_weight.reshape(-1, out_weight.shape[2])
    projected = jnp.dot(mixed, out_matrix, preferred_element_type=jnp.float32)
    residual = lax.optimization_barrier(
        (tokens.astype(jnp.float32) + projected).astype(jnp.bfloat16)
    )
    normed_mlp = normed_rows(whole_rows(residual, members), mlp_gain)
    hidden = jnp.square(
        jax.nn.relu(jnp.dot(normed_mlp, up_weight, preferred_element_type=jnp.float32))
    ).astype(jnp.bfloat16)
    partial = jnp.dot(hidden, down_weight, preferred_element_type=jnp.float32)
    partial = jnp.swapaxes(partial.reshape(rows, members, -1), 0, 1)
    summed = lax.all_to_all(partial, group, split_axis=0, concat_axis=0, tiled=True).sum(axis=0)
    layer_output = (residual.astype(jnp.float32) + summed).astype(jnp.bfloat16)
    return (layer_output, next_state)


whole = pl.BlockSpec(memory_space=pltpu.VMEM)


def call(body, outs, arrays, flops, limit, scratch=()):
    return pl.pallas_call(
        body,
        out_shape=outs,
        in_specs=[whole] * len(arrays),
        out_specs=jax.tree.map(lambda _: whole, outs),
        scratch_shapes=scratch,
        compiler_params=pltpu.CompilerParams(vmem_limit_bytes=limit),
        cost_estimate=pl.CostEstimate(flops=flops, bytes_accessed=0, transcendentals=0),
    )(*arrays)


def far_step(core):
    return 1 + 2 * core


def placed_blocks(core, near_ref, mid_ref, far_ref, swapped_ref):
    return (
        (0, near_ref),
        (2, mid_ref),
        (far_step(core), far_ref),
        (far_step(1 - core), swapped_ref),
    )


def pair_kernel(own_ref, mate_ref, pair_ref):
    core = lax.axis_index("tp")
    pair_ref[core] = own_ref[...]
    pair_ref[1 - core] = mate_ref[...]


def normed_pieces(pair_refs, gain_ref, rows_ref):
    chip = lax.axis_index("kv")
    cores, _, width = pair_refs[0].shape
    for step, pair_ref in placed_blocks(lax.axis_index("tp"), *pair_refs):
        first = lax.bitwise_xor(chip, step) * (cores * width)
        for core in range(cores):
            place = pl.ds(pl.multiple_of(first + core * width, width), width)
            rows_ref[:, place] = pair_ref[core].astype(jnp.float32)
    rows = rows_ref[...]
    inv_root = lax.rsqrt(jnp.mean(rows * rows, axis=1, keepdims=True) + epsilon)
    return (rows * inv_root * gain_ref[...]).astype(jnp.bfloat16)


def project_kernel(chips, *refs):
    pair_refs, (gain_ref, query_ref, forget_ref, value_ref, gate_ref) = refs[:chips], refs[chips : chips + 5]
    near_ref, mid_ref, far_ref, swap_ref, rows_ref, made_ref = refs[chips + 5 :]
    normed = normed_pieces(pair_refs, gain_ref, rows_ref)
    rows = normed.shape[0]
    heads, chan, _ = query_ref.shape
    lanes = 4 * chan
    for head in range(0, heads, 2):
        weight = jnp.concatenate(
            [
                ref[one]
                for one in (head, head + 1)
                for ref in (query_ref, forget_ref, value_ref, gate_ref)
            ],
            axis=0,
        )
        product = lax.dot_general(
            normed, weight, (((1,), (1,)), ((), ())), preferred_element_type=jnp.float32
        )
        product = product.astype(jnp.bfloat16).astype(jnp.float32)
        made_ref[pl.ds(head, rows, stride=heads), :] = product[:, :lanes]
        made_ref[pl.ds(head + 1, rows, stride=heads), :] = product[:, lanes:]
    chip = lax.axis_index("kv")
    pairs = rows * heads // chips
    for step, sent_ref in placed_blocks(
        lax.axis_index("tp"), near_ref, mid_ref, far_ref, swap_ref
    ):
        first = pl.multiple_of(lax.bitwise_xor(chip, step) * pairs, pairs)
        sent_ref[...] = made_ref[pl.ds(first, pairs), :]


def sigmoid(x):
    return 1.0 / (1.0 + jnp.exp(-x))


def readout_kernel(chips, *refs):
    got_refs, (bound_ref, state_ref, gain_ref) = refs[:chips], refs[chips : chips + 3]
    mixed_ref, key_ref, value_ref, placed_ref = refs[chips + 3 :]
    own_rows, heads, keys, _ = state_ref.shape
    chan = keys // chips
    chip, core = lax.axis_index("kv"), lax.axis_index("tp")
    for step, got_ref in placed_blocks(core, *got_refs):
        block = got_ref[...] if len(got_ref.shape) == 2 else got_ref[core]
        placed_ref[lax.bitwise_xor(chip, step)] = block

    def channels(kind):
        return jnp.concatenate(
            [placed_ref[i][:, kind * chan : (kind + 1) * chan] for i in range(chips)], axis=1
        )

    pre_query, pre_forget, value_rows, pre_gate = (channels(kind) for kind in range(4))
    bound = jnp.concatenate([bound_ref[...]] * own_rows, axis=0)
    gain = jnp.concatenate([gain_ref[...]] * own_rows, axis=0)
    forget = bound + (1.0 - bound) * sigmoid(pre_forget)
    key_rows = (1.0 - bound) * sigmoid(-pre_forget)
    query = pre_query * sigmoid(pre_query)
    new_part = jnp.sum(query * key_rows, axis=1, keepdims=True) * value_rows
    weight = jnp.transpose(query * forget)
    old_parts = []
    for row in range(own_rows):
        for head in range(heads):
            pair = row * heads + head
            old_parts.append(
                jnp.sum(weight[:, pair : pair + 1] * state_ref[row, head], axis=0, keepdims=True)
            )
    readout = jnp.concatenate(old_parts, axis=0) + new_part
    inv_head = lax.rsqrt(jnp.mean(readout * readout, axis=1, keepdims=True) + epsilon)
    mixed = readout * inv_head * gain * (pre_gate * sigmoid(pre_gate))
    mixed_ref[...] = mixed.astype(jnp.bfloat16).astype(jnp.float32)
    key_ref[...] = key_rows
    value_ref[...] = value_rows


def state_kernel(key_ref, value_ref, state_ref, next_ref):
    own_rows, heads, _, _ = state_ref.shape
    key_cols = jnp.transpose(key_ref[...])
    for row in range(own_rows):
        for head in range(heads):
            pair = row * heads + head
            old = state_ref[row, head]
            next_ref[row, head] = old + key_cols[:, pair : pair + 1] * (
                value_ref[pair : pair + 1, :] - old
            )


def stage_kernel(block_ref, staged_ref):
    staged_ref[...] = block_ref[...]


def out_kernel(chips, heads, *refs):
    pair_refs, (tokens_ref, weight_ref, residual_ref, placed_ref) = refs[:chips], refs[chips:]
    cores, pairs, values = pair_refs[0].shape
    own_rows = pairs // heads
    chip = lax.axis_index("kv")
    for step, pair_ref in placed_blocks(lax.axis_index("tp"), *pair_refs):
        first = pl.multiple_of(lax.bitwise_xor(chip, step) * (cores * pairs), cores * pairs)
        placed_ref[pl.ds(first, cores * pairs), :] = pair_ref[...].reshape(-1, values)
    blocks = []
    for core in range(cores):
        for head in range(heads):
            blocks.append(
                jnp.concatenate(
                    [
                        placed_ref[
                            pl.ds(core * pairs + row * heads + head, chips, stride=cores * pairs), :
                        ]
                        for row in range(own_rows)
                    ],
                    axis=0,
                )
            )
    mixed = jnp.concatenate(blocks, axis=1).astype(jnp.bfloat16)
    weight = weight_ref[...].reshape(-1, weight_ref.shape[2])
    projected = jnp.dot(mixed, weight, preferred_element_type=jnp.float32)
    ordered = [
        projected[row * chips + i : row * chips + i + 1]
        for i in range(chips)
        for row in range(own_rows)
    ]
    projected = jnp.concatenate(ordered, axis=0)
    residual_ref[...] = (tokens_ref[...].astype(jnp.float32) + projected).astype(jnp.bfloat16)


def down_part(hidden, down_ref, core, partial_ref):
    width = partial_ref.shape[2]
    chip = lax.axis_index("kv")
    far = lax.bitwise_xor(chip, far_step(core))
    columns = (2 * far, 2 * far + 1, 2 * lax.bitwise_xor(chip, 2) + core, 2 * chip + core)
    for slot, column in enumerate(columns):
        partial_ref[slot] = jnp.dot(
            hidden,
            down_ref[:, pl.ds(pl.multiple_of(column * width, width), width)],
            preferred_element_type=jnp.float32,
        )


def mixer_kernel(chips, *refs):
    pair_refs, (gain_ref, up_ref, down_ref) = refs[:chips], refs[chips : chips + 3]
    hidden_ref, partial_ref, rows_ref = refs[chips + 3 :]
    normed = normed_pieces(pair_refs, gain_ref, rows_ref)
    hidden = jnp.dot(normed, up_ref[...], preferred_element_type=jnp.float32)
    hidden = jnp.square(jnp.maximum(hidden, 0.0)).astype(jnp.bfloat16)
    hidden_ref[...] = hidden
    down_part(hidden, down_ref, 1 - lax.axis_index("tp"), partial_ref)


def own_part_kernel(hidden_ref, down_ref, partial_ref):
    down_part(hidden_ref[...], down_ref, lax.axis_index("tp"), partial_ref)


def chip_sum_kernel(own_ref, mate_ref, far_ref, mid_ref, kept_ref):
    for core in range(2):
        far_ref[core] = (own_ref[core] + mate_ref[core]).astype(jnp.bfloat16)
    mid_ref[...] = (own_ref[2] + mate_ref[2]).astype(jnp.bfloat16)
    kept_ref[...] = own_ref[3] + mate_ref[3]


def last_kernel(residual_ref, kept_ref, mid_ref, far_ref, swapped_ref, state_ref, output_ref):
    del state_ref
    core = lax.axis_index("tp")
    total = kept_ref[...]
    for block in (mid_ref[...], far_ref[core], swapped_ref[core]):
        total = total + block.astype(jnp.float32)
    output_ref[...] = (residual_ref[...].astype(jnp.float32) + total).astype(jnp.bfloat16)


MIB = 1 << 20
COST = (10**11, 10**11, 10**9, 10**9, 10**6, 10**6, 10**9, 10**6, 10**6)


def tiled_local(
    kv,
    tp,
    tokens,
    mix_gain,
    query_weight,
    forget_weight,
    value_weight,
    gate_weight,
    lower_bound,
    recurrent_state,
    head_gain,
    out_weight,
    mlp_gain,
    up_weight,
    down_weight,
):
    rows, width = tokens.shape
    heads, chan, model = query_weight.shape
    own_rows, _, keys, values = recurrent_state.shape
    pairs = own_rows * heads
    shape = jax.ShapeDtypeStruct
    f32, bf16 = jnp.float32, jnp.bfloat16

    def permute(block, steps, swapped=False):
        hops = [
            (k * tp + t, (k ^ steps[t]) * tp + (1 - t if swapped else t))
            for k in range(kv)
            for t in range(tp)
        ]
        return lax.ppermute(block, group, hops)

    def other_core(block):
        return permute(block, (0, 0), True)

    def paired(block, mate, cost):
        return call(pair_kernel, shape((tp,) + block.shape, block.dtype), (block, mate), cost, MIB)

    def crossed(far, mid):
        got_far = permute(far, (1, 3))
        got_mid = permute(mid, (2, 2))
        return got_mid, got_far, permute(got_far, (0, 0), True)

    def gather_pairs(block, staged, cost):
        pair = paired(staged, other_core(block), cost)
        return (pair,) + crossed(pair, pair)

    staged = call(stage_kernel, shape(tokens.shape, bf16), (tokens,), COST[4], MIB)
    near, mid, far, swap = call(
        functools.partial(project_kernel, kv),
        [shape((pairs, 4 * chan), f32)] * kv,
        (
            *gather_pairs(tokens, staged, COST[0]),
            mix_gain.reshape(1, -1),
            query_weight,
            forget_weight,
            value_weight,
            gate_weight,
        ),
        COST[1],
        4 * MIB,
        [pltpu.VMEM((rows, model), f32), pltpu.VMEM((rows * heads, 4 * chan), f32)],
    )
    got = (near,) + crossed(paired(far, other_core(swap), COST[4]), mid)
    mixed, key_rows, value_rows = call(
        functools.partial(readout_kernel, kv),
        [shape((pairs, values), f32), shape((pairs, keys), f32), shape((pairs, values), f32)],
        (*got, lower_bound, recurrent_state, head_gain),
        COST[2],
        4 * MIB,
        [pltpu.VMEM((kv, pairs, 4 * chan), f32)],
    )
    next_state = call(
        state_kernel,
        shape(recurrent_state.shape, f32),
        (key_rows, value_rows, recurrent_state),
        COST[3],
        4 * MIB,
    )
    residual = call(
        functools.partial(out_kernel, kv, heads),
        shape((rows, width), bf16),
        (*gather_pairs(mixed, mixed, COST[4]), staged, out_weight),
        COST[4],
        4 * MIB,
        [pltpu.VMEM((kv * tp * pairs, values), f32)],
    )
    hidden, mate_part = call(
        functools.partial(mixer_kernel, kv),
        [shape((rows, up_weight.shape[1]), bf16), shape((kv, rows, width), f32)],
        (*gather_pairs(residual, residual, COST[4]), mlp_gain.reshape(1, -1), up_weight, down_weight),
        COST[5],
        4 * MIB,
        [pltpu.VMEM((rows, model), f32)],
    )
    own_part = call(
        own_part_kernel, shape((kv, rows, width), f32), (hidden, down_weight), COST[6], 4 * MIB
    )
    far, mid, kept = call(
        chip_sum_kernel,
        [shape((tp, rows, width), bf16), shape((rows, width), bf16), shape((rows, width), f32)],
        (own_part, other_core(mate_part)),
        COST[7],
        MIB,
    )
    sums = crossed(far, mid)
    layer_output = call(
        last_kernel, shape((rows, width), bf16), (residual, kept, *sums, next_state), COST[8], MIB
    )
    return (layer_output, next_state)


def tiles(kv, tp, tokens, query_weight):
    rows, width = tokens.shape
    aligned = rows % 8 == 0 and width % 128 == 0 and query_weight.shape[1] % 32 == 0
    return aligned and tp == 2 and kv == 4


def solution(mesh):
    placed = (
        P("dp", ("kv", "tp")),
        P(),
        P("tp", "kv", None),
        P("tp", "kv", None),
        P("tp", "kv", None),
        P("tp", "kv", None),
        P("tp", None),
        P(("dp", "kv"), "tp", None, None),
        P("tp", None),
        P(None, None, ("kv", "tp")),
        P(),
        P(None, ("kv", "tp")),
        P(("kv", "tp"), None),
    )

    def body(*arrays):
        kv, tp = mesh.shape["kv"], mesh.shape["tp"]
        run = tiled_local if tiles(kv, tp, arrays[0], arrays[2]) else local
        return run(kv, tp, *arrays)

    return jax.shard_map(
        body,
        mesh=mesh,
        in_specs=placed,
        out_specs=(P("dp", ("kv", "tp")), P(("dp", "kv"), "tp", None, None)),
        check_vma=False,
    )
```

time: 59.1 us -> 51.4 us (0.87)
  blocking collectives: 47.1 us -> 0 us
  starting transfers between devices: 0 us -> 21.6 us
  waiting for transfers between devices: 0 us -> 16.5 us
  local copies, waits for them, and re-layouts: 0.79 us -> 2.01 us
    all_to_all x5 -> x0, blocking collectives: 47.1 us -> none  [the longest x2 20.6 us: tiled_local(): pieces = exchange(copies, group)]
    ppermute x0 -> x20, starting transfers between devices: none -> 21.6 us  [permute(): return lax.ppermute(block, group, hops)]
    ppermute x0 -> x20, waiting for transfers between devices: none -> 16.5 us  [permute(): return lax.ppermute(block, group, hops)]
    unnamed x40, local copies, waits for them, and re-layouts: 0.79 us -> 2.01 us
    pallas_call x6 -> x13, Pallas kernels: 9.97 us -> 10.2 us  [call(): pl.pallas_call(body, out_shape=outs, in_specs=[whole] * len(arrays), out_...]
  transfers between devices with their start and end apart: 0 -> 20, of which waited for: 0 -> 12; matrix products, arithmetic and copies ran while one was open for 0% -> 0% of each run, Pallas kernels for 0% -> 5%
where the time goes in v3:
time: 51.4 us; the launch traced here: 51.2 us
  starting transfers between devices  21.6 us (42%)
  waiting for transfers between devices  16.5 us (32%)
  Pallas kernels  10.2 us (20%)
  local copies, waits for them, and re-layouts  2.01 us (4%)
  between operations  0.92 us (2%)
    ppermute x20, starting transfers between devices, permute(): return lax.ppermute(block, group, hops)  21.6 us
    ppermute x20, waiting for transfers between devices, permute(): return lax.ppermute(block, group, hops)  16.5 us
    pallas_call x13, Pallas kernels, call(): pl.pallas_call(body, out_shape=outs, in_specs=[whole] * len(arrays), out_...  10.2 us
    unnamed x40, local copies, waits for them, and re-layouts  2.01 us
  transfers between devices with their start and end apart: 20, of which 12 were waited for; matrix products, arithmetic and copies ran while one was open for 0% of the time, Pallas kernels for 5%

profile of v3, /device:TPU:0, one launch (start us, length us, event | category | flops | bytes accessed | tf_op | source)
XLA Modules:
  0.0 51.2 jit_solution(13044273836933635841)
XLA Ops:
  2.2 2.9 %collective-permute-start.2 = (bf16[2,8,512]{2,1,0:T(8,128)(2,1)S(1)}, bf16[2,8,512]{2,1,0:T(8,128)(2,1)S(1)}, u32[]{:S(2)}, u32[]{:S(2)}) collective-permute-start(bf16[2,8,512]{2,1,0:T(8,128)(2,1)S(1)} %shard_map.141.refs_0_), channel_id=1, source_target_pairs={{0,2},{1,7},{2,0},{3,5},{4,6},{5,3},{6,4},{7,1},{8,10},{9,15},{10,... | collective-permute-start | bytes 49160 | tf_op jit(solution)/shard_map/ppermute | solution.py:345
  5.1 2.6 %collective-permute-start.1 = (bf16[2,8,512]{2,1,0:T(8,128)(2,1)S(1)}, bf16[2,8,512]{2,1,0:T(8,128)(2,1)S(1)}, u32[]{:S(2)}, u32[]{:S(2)}) collective-permute-start(bf16[2,8,512]{2,1,0:T(8,128)(2,1)S(1)} %shard_map.141.refs_0_), channel_id=1, source_target_pairs={{0,4},{1,5},{2,6},{3,7},{4,0},{5,1},{6,2},{7,3},{8,12},{9,13},{10,... | collective-permute-start | bytes 49160 | tf_op jit(solution)/shard_map/ppermute | solution.py:345
  8.2 1.7 %collective-permute-done.1.refs_1_ = bf16[2,8,512]{2,1,0:T(8,128)(2,1)S(1)} collective-permute-done((bf16[2,8,512]{2,1,0:T(8,128)(2,1)S(1)}, bf16[2,8,512]{2,1,0:T(8,128)(2,1)S(1)}, u32[]{:S(2)}, u32[]{:S(2)}) %collective-permute-start.1) | collective-permute-done | bytes 16416 | tf_op jit(solution)/shard_map/ppermute | solution.py:345
  10.0 2.3 %shard_map.142 = (f32[16,128]{1,0:T(8,128)S(1)}, f32[16,128]{1,0:T(8,128)S(1)}, f32[16,128]{1,0:T(8,128)S(1)}, f32[16,128]{1,0:T(8,128)S(1)}) custom-call(bf16[2,8,512]{2,1,0:T(8,128)(2,1)S(1)} %shard_map.141.refs_0_, bf16[2,8,512]{2,1,0:T(8,128)(2,1)S(1)} %collective-permute-done.1.refs_1_, bf16[2,8,512]{2,1,0:T(8,128)(2,1)S(1)} %collective-permute-done.2.refs_2_, ...), custom_call_target="tpu_custom_call" | custom-call | flops 99999997952 | tf_op jit(solution)/shard_map/pallas_call | solution.py:102
  13.9 3.7 %collective-permute-done.6.refs_2_ = f32[2,16,128]{2,1,0:T(8,128)S(1)} collective-permute-done((f32[2,16,128]{2,1,0:T(8,128)S(1)}, f32[2,16,128]{2,1,0:T(8,128)S(1)}, u32[]{:S(2)}, u32[]{:S(2)}) %collective-permute-start.6) | collective-permute-done | bytes 16416 | tf_op jit(solution)/shard_map/ppermute | solution.py:345
  17.7 1.0 %collective-permute-start.7 = (f32[2,16,128]{2,1,0:T(8,128)S(1)}, f32[2,16,128]{2,1,0:T(8,128)S(1)}, u32[]{:S(2)}, u32[]{:S(2)}) collective-permute-start(f32[2,16,128]{2,1,0:T(8,128)S(1)} %collective-permute-done.6.refs_2_), channel_id=1, source_target_pairs={{0,1},{1,0},{2,3},{3,2},{4,5},{5,4},{6,7},{7,6},{8,9},{9,8},{10,11... | collective-permute-start | bytes 49160 | tf_op jit(solution)/shard_map/ppermute | solution.py:345
  18.7 1.2 %collective-permute-start.4 = (f32[16,128]{1,0:T(8,128)S(1)}, f32[16,128]{1,0:T(8,128)S(1)}, u32[]{:S(2)}, u32[]{:S(2)}) collective-permute-start(f32[16,128]{1,0:T(8,128)S(1)} %get-tuple-element.15), channel_id=1, source_target_pairs={{0,4},{1,5},{2,6},{3,7},{4,0},{5,1},{6,2},{7,3},{8,12},{9,13},{10,... | collective-permute-start | bytes 24584 | tf_op jit(solution)/shard_map/ppermute | solution.py:345
  19.9 3.4 %collective-permute-done.4.refs_1_ = f32[16,128]{1,0:T(8,128)S(1)} collective-permute-done((f32[16,128]{1,0:T(8,128)S(1)}, f32[16,128]{1,0:T(8,128)S(1)}, u32[]{:S(2)}, u32[]{:S(2)}) %collective-permute-start.4) | collective-permute-done | bytes 8224 | tf_op jit(solution)/shard_map/ppermute | solution.py:345
  24.1 1.2 %collective-permute-done.8.mate_ref = f32[16,128]{1,0:T(8,128)S(1)} collective-permute-done((f32[16,128]{1,0:T(8,128)S(1)}, f32[16,128]{1,0:T(8,128)S(1)}, u32[]{:S(2)}, u32[]{:S(2)}) %collective-permute-start.8) | collective-permute-done | bytes 8224 | tf_op jit(solution)/shard_map/ppermute | solution.py:345
  25.2 2.9 %collective-permute-start.9 = (f32[2,16,128]{2,1,0:T(8,128)S(1)}, f32[2,16,128]{2,1,0:T(8,128)S(1)}, u32[]{:S(2)}, u32[]{:S(2)}) collective-permute-start(f32[2,16,128]{2,1,0:T(8,128)S(1)} %shard_map.145.refs_0_), channel_id=1, source_target_pairs={{0,4},{1,5},{2,6},{3,7},{4,0},{5,1},{6,2},{7,3},{8,12},{9,13},{10,... | collective-permute-start | bytes 49160 | tf_op jit(solution)/shard_map/ppermute | solution.py:345
  29.0 0.9 %collective-permute-start.11 = (f32[2,16,128]{2,1,0:T(8,128)S(1)}, f32[2,16,128]{2,1,0:T(8,128)S(1)}, u32[]{:S(2)}, u32[]{:S(2)}) collective-permute-start(f32[2,16,128]{2,1,0:T(8,128)S(1)} %collective-permute-done.10.refs_2_), channel_id=1, source_target_pairs={{0,1},{1,0},{2,3},{3,2},{4,5},{5,4},{6,7},{7,6},{8,9},{9,8},{10,11... | collective-permute-start | bytes 49160 | tf_op jit(solution)/shard_map/ppermute | solution.py:345
  32.3 1.2 %collective-permute-start.14 = (bf16[2,8,512]{2,1,0:T(8,128)(2,1)S(1)}, bf16[2,8,512]{2,1,0:T(8,128)(2,1)S(1)}, u32[]{:S(2)}, u32[]{:S(2)}) collective-permute-start(bf16[2,8,512]{2,1,0:T(8,128)(2,1)S(1)} %shard_map.147.refs_0_), channel_id=1, source_target_pairs={{0,2},{1,7},{2,0},{3,5},{4,6},{5,3},{6,4},{7,1},{8,10},{9,15},{10,... | collective-permute-start | bytes 49160 | tf_op jit(solution)/shard_map/ppermute | solution.py:345
  33.5 1.6 %collective-permute-start.13 = (bf16[2,8,512]{2,1,0:T(8,128)(2,1)S(1)}, bf16[2,8,512]{2,1,0:T(8,128)(2,1)S(1)}, u32[]{:S(2)}, u32[]{:S(2)}) collective-permute-start(bf16[2,8,512]{2,1,0:T(8,128)(2,1)S(1)} %shard_map.147.refs_0_), channel_id=1, source_target_pairs={{0,4},{1,5},{2,6},{3,7},{4,0},{5,1},{6,2},{7,3},{8,12},{9,13},{10,... | collective-permute-start | bytes 49160 | tf_op jit(solution)/shard_map/ppermute | solution.py:345
  35.2 0.9 %collective-permute-done.14.refs_2_ = bf16[2,8,512]{2,1,0:T(8,128)(2,1)S(1)} collective-permute-done((bf16[2,8,512]{2,1,0:T(8,128)(2,1)S(1)}, bf16[2,8,512]{2,1,0:T(8,128)(2,1)S(1)}, u32[]{:S(2)}, u32[]{:S(2)}) %collective-permute-start.14) | collective-permute-done | bytes 16416 | tf_op jit(solution)/shard_map/ppermute | solution.py:345
  36.1 1.0 %collective-permute-start.15 = (bf16[2,8,512]{2,1,0:T(8,128)(2,1)S(1)}, bf16[2,8,512]{2,1,0:T(8,128)(2,1)S(1)}, u32[]{:S(2)}, u32[]{:S(2)}) collective-permute-start(bf16[2,8,512]{2,1,0:T(8,128)(2,1)S(1)} %collective-permute-done.14.refs_2_), channel_id=1, source_target_pairs={{0,1},{1,0},{2,3},{3,2},{4,5},{5,4},{6,7},{7,6},{8,9},{9,8},{10,11... | collective-permute-start | bytes 49160 | tf_op jit(solution)/shard_map/ppermute | solution.py:345
  37.1 1.1 %collective-permute-done.13.refs_1_ = bf16[2,8,512]{2,1,0:T(8,128)(2,1)S(1)} collective-permute-done((bf16[2,8,512]{2,1,0:T(8,128)(2,1)S(1)}, bf16[2,8,512]{2,1,0:T(8,128)(2,1)S(1)}, u32[]{:S(2)}, u32[]{:S(2)}) %collective-permute-start.13) | collective-permute-done | bytes 16416 | tf_op jit(solution)/shard_map/ppermute | solution.py:345
  38.3 3.5 %shard_map.148 = (bf16[8,2048]{1,0:T(8,128)(2,1)S(1)}, f32[4,8,512]{2,1,0:T(8,128)S(1)}) custom-call(bf16[2,8,512]{2,1,0:T(8,128)(2,1)S(1)} %shard_map.147.refs_0_, bf16[2,8,512]{2,1,0:T(8,128)(2,1)S(1)} %collective-permute-done.13.refs_1_, bf16[2,8,512]{2,1,0:T(8,128)(2,1)S(1)} %collective-permute-done.14.refs_2_, ...), custom_call_target="tpu_custom_call" | custom-call | flops 1000000 | tf_op jit(solution)/shard_map/pallas_call | solution.py:102
  41.9 1.2 %shard_map.149.own_ref = f32[4,8,512]{2,1,0:T(8,128)S(1)} custom-call(bf16[8,2048]{1,0:T(8,128)(2,1)S(1)} %get-tuple-element.19.hidden_ref, bf16[2048,4096]{1,0:T(8,128)(2,1)S(1)} %bitcast.3), custom_call_target="tpu_custom_call" | custom-call | flops 1000000000 | tf_op jit(solution)/shard_map/pallas_call | solution.py:102
  43.1 0.9 %collective-permute-start.18 = (bf16[2,8,512]{2,1,0:T(8,128)(2,1)S(1)}, bf16[2,8,512]{2,1,0:T(8,128)(2,1)S(1)}, u32[]{:S(2)}, u32[]{:S(2)}) collective-permute-start(bf16[2,8,512]{2,1,0:T(8,128)(2,1)S(1)} %get-tuple-element.23), channel_id=1, source_target_pairs={{0,2},{1,7},{2,0},{3,5},{4,6},{5,3},{6,4},{7,1},{8,10},{9,15},{10,... | collective-permute-start | bytes 49160 | tf_op jit(solution)/shard_map/ppermute | solution.py:345
  44.0 2.0 %collective-permute-start.17 = (bf16[8,512]{1,0:T(8,128)(2,1)S(1)}, bf16[8,512]{1,0:T(8,128)(2,1)S(1)}, u32[]{:S(2)}, u32[]{:S(2)}) collective-permute-start(bf16[8,512]{1,0:T(8,128)(2,1)S(1)} %get-tuple-element.22), channel_id=1, source_target_pairs={{0,4},{1,5},{2,6},{3,7},{4,0},{5,1},{6,2},{7,3},{8,12},{9,13},{10,... | collective-permute-start | bytes 24584 | tf_op jit(solution)/shard_map/ppermute | solution.py:345
  46.0 0.9 %collective-permute-done.18.far_ref = bf16[2,8,512]{2,1,0:T(8,128)(2,1)S(1)} collective-permute-done((bf16[2,8,512]{2,1,0:T(8,128)(2,1)S(1)}, bf16[2,8,512]{2,1,0:T(8,128)(2,1)S(1)}, u32[]{:S(2)}, u32[]{:S(2)}) %collective-permute-start.18) | collective-permute-done | bytes 16416 | tf_op jit(solution)/shard_map/ppermute | solution.py:345
  46.9 1.0 %collective-permute-start.19 = (bf16[2,8,512]{2,1,0:T(8,128)(2,1)S(1)}, bf16[2,8,512]{2,1,0:T(8,128)(2,1)S(1)}, u32[]{:S(2)}, u32[]{:S(2)}) collective-permute-start(bf16[2,8,512]{2,1,0:T(8,128)(2,1)S(1)} %collective-permute-done.18.far_ref), channel_id=1, source_target_pairs={{0,1},{1,0},{2,3},{3,2},{4,5},{5,4},{6,7},{7,6},{8,9},{9,8},{10,11... | collective-permute-start | bytes 49160 | tf_op jit(solution)/shard_map/ppermute | solution.py:345
  47.9 1.4 %shard_map.151.state_ref = f32[2,8,128,128]{3,2,1,0:T(8,128)} custom-call(f32[16,128]{1,0:T(8,128)S(1)} %get-tuple-element.24.key_ref, f32[16,128]{1,0:T(8,128)S(1)} %get-tuple-element.25.value_ref, f32[2,8,128,128]{3,2,1,0:T(8,128)S(1)} %copy-done.8), custom_call_target="tpu_custom_call" | custom-call | flops 1000000000 | tf_op jit(solution)/shard_map/pallas_call | solution.py:102
  49.4 1.2 %copy-done.1 = f32[2,8,128,128]{3,2,1,0:T(8,128)S(1)} copy-done((f32[2,8,128,128]{3,2,1,0:T(8,128)S(1)}, f32[2,8,128,128]{3,2,1,0:T(8,128)}, u32[]{:S(2)}) %copy-start.1) | copy-done | bytes 1048600
  (71 shorter events, 8.5 us)
Async XLA Ops:
  0.6 1.6 %collective-permute-start = (bf16[8,512]{1,0:T(8,128)(2,1)}, bf16[8,512]{1,0:T(8,128)(2,1)S(1)}, u32[]{:S(2)}, u32[]{:S(2)}) collective-permute-start(bf16[8,512]{1,0:T(8,128)(2,1)} %block_ref.1), channel_id=1, source_target_pairs={{0,1},{1,0},{2,3},{3,2},{4,5},{5,4},{6,7},{7,6},{8,9},{9,8},{10,11... | collective-permute-start | bytes 24584 | tf_op jit(solution)/shard_map/ppermute | solution.py:345
  2.2 5.5 %collective-permute-start.2 = (bf16[2,8,512]{2,1,0:T(8,128)(2,1)S(1)}, bf16[2,8,512]{2,1,0:T(8,128)(2,1)S(1)}, u32[]{:S(2)}, u32[]{:S(2)}) collective-permute-start(bf16[2,8,512]{2,1,0:T(8,128)(2,1)S(1)} %shard_map.141.refs_0_), channel_id=1, source_target_pairs={{0,2},{1,7},{2,0},{3,5},{4,6},{5,3},{6,4},{7,1},{8,10},{9,15},{10,... | collective-permute-start | bytes 49160 | tf_op jit(solution)/shard_map/ppermute | solution.py:345
  5.1 4.7 %collective-permute-start.1 = (bf16[2,8,512]{2,1,0:T(8,128)(2,1)S(1)}, bf16[2,8,512]{2,1,0:T(8,128)(2,1)S(1)}, u32[]{:S(2)}, u32[]{:S(2)}) collective-permute-start(bf16[2,8,512]{2,1,0:T(8,128)(2,1)S(1)} %shard_map.141.refs_0_), channel_id=1, source_target_pairs={{0,4},{1,5},{2,6},{3,7},{4,0},{5,1},{6,2},{7,3},{8,12},{9,13},{10,... | collective-permute-start | bytes 49160 | tf_op jit(solution)/shard_map/ppermute | solution.py:345
  7.7 2.2 %collective-permute-start.3 = (bf16[2,8,512]{2,1,0:T(8,128)(2,1)S(1)}, bf16[2,8,512]{2,1,0:T(8,128)(2,1)S(1)}, u32[]{:S(2)}, u32[]{:S(2)}) collective-permute-start(bf16[2,8,512]{2,1,0:T(8,128)(2,1)S(1)} %collective-permute-done.2.refs_2_), channel_id=1, source_target_pairs={{0,1},{1,0},{2,3},{3,2},{4,5},{5,4},{6,7},{7,6},{8,9},{9,8},{10,11... | collective-permute-start | bytes 49160 | tf_op jit(solution)/shard_map/ppermute | solution.py:345
  9.9 28.3 %slice-start = ((s8[16777216]{0:T(1024)(128)(4,1)}), s8[4194304]{0:T(1024)(128)(4,1)S(1)}, s32[]{:S(2)}) async-start(s8[16777216]{0:T(1024)(128)(4,1)} %bitcast.2), calls=%async_computation | async-start | bytes 8388608
  9.9 28.3 %slice-start.4 = ((s8[16777216]{0:T(1024)(128)(4,1)}), s8[4194304]{0:T(1024)(128)(4,1)S(1)}, s32[]{:S(2)}) async-start(s8[16777216]{0:T(1024)(128)(4,1)} %bitcast.4), calls=%async_computation.4 | async-start | bytes 8388608
  10.0 28.2 %slice-start.1 = ((s8[16777216]{0:T(1024)(128)(4,1)}), s8[4194304]{0:T(1024)(128)(4,1)S(1)}, s32[]{:S(2)}) async-start(s8[16777216]{0:T(1024)(128)(4,1)} %bitcast.2), calls=%async_computation.1 | async-start | bytes 8388608
  10.0 28.2 %slice-start.2 = ((s8[16777216]{0:T(1024)(128)(4,1)}), s8[4194304]{0:T(1024)(128)(4,1)S(1)}, s32[]{:S(2)}) async-start(s8[16777216]{0:T(1024)(128)(4,1)} %bitcast.2), calls=%async_computation.2 | async-start | bytes 8388608
  12.4 1.6 %collective-permute-start.5 = (f32[16,128]{1,0:T(8,128)S(1)}, f32[16,128]{1,0:T(8,128)S(1)}, u32[]{:S(2)}, u32[]{:S(2)}) collective-permute-start(f32[16,128]{1,0:T(8,128)S(1)} %get-tuple-element.17), channel_id=1, source_target_pairs={{0,1},{1,0},{2,3},{3,2},{4,5},{5,4},{6,7},{7,6},{8,9},{9,8},{10,11... | collective-permute-start | bytes 24584 | tf_op jit(solution)/shard_map/ppermute | solution.py:345
  13.9 3.7 %collective-permute-start.6 = (f32[2,16,128]{2,1,0:T(8,128)S(1)}, f32[2,16,128]{2,1,0:T(8,128)S(1)}, u32[]{:S(2)}, u32[]{:S(2)}) collective-permute-start(f32[2,16,128]{2,1,0:T(8,128)S(1)} %shard_map.143), channel_id=1, source_target_pairs={{0,2},{1,7},{2,0},{3,5},{4,6},{5,3},{6,4},{7,1},{8,10},{9,15},{10,... | collective-permute-start | bytes 49160 | tf_op jit(solution)/shard_map/ppermute | solution.py:345
  17.7 5.5 %collective-permute-start.7 = (f32[2,16,128]{2,1,0:T(8,128)S(1)}, f32[2,16,128]{2,1,0:T(8,128)S(1)}, u32[]{:S(2)}, u32[]{:S(2)}) collective-permute-start(f32[2,16,128]{2,1,0:T(8,128)S(1)} %collective-permute-done.6.refs_2_), channel_id=1, source_target_pairs={{0,1},{1,0},{2,3},{3,2},{4,5},{5,4},{6,7},{7,6},{8,9},{9,8},{10,11... | collective-permute-start | bytes 49160 | tf_op jit(solution)/shard_map/ppermute | solution.py:345
  18.7 4.5 %collective-permute-start.4 = (f32[16,128]{1,0:T(8,128)S(1)}, f32[16,128]{1,0:T(8,128)S(1)}, u32[]{:S(2)}, u32[]{:S(2)}) collective-permute-start(f32[16,128]{1,0:T(8,128)S(1)} %get-tuple-element.15), channel_id=1, source_target_pairs={{0,4},{1,5},{2,6},{3,7},{4,0},{5,1},{6,2},{7,3},{8,12},{9,13},{10,... | collective-permute-start | bytes 24584 | tf_op jit(solution)/shard_map/ppermute | solution.py:345
  24.0 1.2 %collective-permute-start.8 = (f32[16,128]{1,0:T(8,128)S(1)}, f32[16,128]{1,0:T(8,128)S(1)}, u32[]{:S(2)}, u32[]{:S(2)}) collective-permute-start(f32[16,128]{1,0:T(8,128)S(1)} %get-tuple-element.18.own_ref), channel_id=1, source_target_pairs={{0,1},{1,0},{2,3},{3,2},{4,5},{5,4},{6,7},{7,6},{8,9},{9,8},{10,11... | collective-permute-start | bytes 24584 | tf_op jit(solution)/shard_map/ppermute | solution.py:345
  25.2 3.7 %collective-permute-start.10 = (f32[2,16,128]{2,1,0:T(8,128)S(1)}, f32[2,16,128]{2,1,0:T(8,128)S(1)}, u32[]{:S(2)}, u32[]{:S(2)}) collective-permute-start(f32[2,16,128]{2,1,0:T(8,128)S(1)} %shard_map.145.refs_0_), channel_id=1, source_target_pairs={{0,2},{1,7},{2,0},{3,5},{4,6},{5,3},{6,4},{7,1},{8,10},{9,15},{10,... | collective-permute-start | bytes 49160 | tf_op jit(solution)/shard_map/ppermute | solution.py:345
  25.2 4.6 %collective-permute-start.9 = (f32[2,16,128]{2,1,0:T(8,128)S(1)}, f32[2,16,128]{2,1,0:T(8,128)S(1)}, u32[]{:S(2)}, u32[]{:S(2)}) collective-permute-start(f32[2,16,128]{2,1,0:T(8,128)S(1)} %shard_map.145.refs_0_), channel_id=1, source_target_pairs={{0,4},{1,5},{2,6},{3,7},{4,0},{5,1},{6,2},{7,3},{8,12},{9,13},{10,... | collective-permute-start | bytes 49160 | tf_op jit(solution)/shard_map/ppermute | solution.py:345
  29.0 1.7 %collective-permute-start.11 = (f32[2,16,128]{2,1,0:T(8,128)S(1)}, f32[2,16,128]{2,1,0:T(8,128)S(1)}, u32[]{:S(2)}, u32[]{:S(2)}) collective-permute-start(f32[2,16,128]{2,1,0:T(8,128)S(1)} %collective-permute-done.10.refs_2_), channel_id=1, source_target_pairs={{0,1},{1,0},{2,3},{3,2},{4,5},{5,4},{6,7},{7,6},{8,9},{9,8},{10,11... | collective-permute-start | bytes 49160 | tf_op jit(solution)/shard_map/ppermute | solution.py:345
  31.1 1.2 %collective-permute-start.12 = (bf16[8,512]{1,0:T(8,128)(2,1)S(1)}, bf16[8,512]{1,0:T(8,128)(2,1)S(1)}, u32[]{:S(2)}, u32[]{:S(2)}) collective-permute-start(bf16[8,512]{1,0:T(8,128)(2,1)S(1)} %shard_map.146.own_ref.residual_ref), channel_id=1, source_target_pairs={{0,1},{1,0},{2,3},{3,2},{4,5},{5,4},{6,7},{7,6},{8,9},{9,8},{10,11... | collective-permute-start | bytes 24584 | tf_op jit(solution)/shard_map/ppermute | solution.py:345
  32.3 3.7 %collective-permute-start.14 = (bf16[2,8,512]{2,1,0:T(8,128)(2,1)S(1)}, bf16[2,8,512]{2,1,0:T(8,128)(2,1)S(1)}, u32[]{:S(2)}, u32[]{:S(2)}) collective-permute-start(bf16[2,8,512]{2,1,0:T(8,128)(2,1)S(1)} %shard_map.147.refs_0_), channel_id=1, source_target_pairs={{0,2},{1,7},{2,0},{3,5},{4,6},{5,3},{6,4},{7,1},{8,10},{9,15},{10,... | collective-permute-start | bytes 49160 | tf_op jit(solution)/shard_map/ppermute | solution.py:345
  33.5 4.6 %collective-permute-start.13 = (bf16[2,8,512]{2,1,0:T(8,128)(2,1)S(1)}, bf16[2,8,512]{2,1,0:T(8,128)(2,1)S(1)}, u32[]{:S(2)}, u32[]{:S(2)}) collective-permute-start(bf16[2,8,512]{2,1,0:T(8,128)(2,1)S(1)} %shard_map.147.refs_0_), channel_id=1, source_target_pairs={{0,4},{1,5},{2,6},{3,7},{4,0},{5,1},{6,2},{7,3},{8,12},{9,13},{10,... | collective-permute-start | bytes 49160 | tf_op jit(solution)/shard_map/ppermute | solution.py:345
  36.1 2.1 %collective-permute-start.15 = (bf16[2,8,512]{2,1,0:T(8,128)(2,1)S(1)}, bf16[2,8,512]{2,1,0:T(8,128)(2,1)S(1)}, u32[]{:S(2)}, u32[]{:S(2)}) collective-permute-start(bf16[2,8,512]{2,1,0:T(8,128)(2,1)S(1)} %collective-permute-done.14.refs_2_), channel_id=1, source_target_pairs={{0,1},{1,0},{2,3},{3,2},{4,5},{5,4},{6,7},{7,6},{8,9},{9,8},{10,11... | collective-permute-start | bytes 49160 | tf_op jit(solution)/shard_map/ppermute | solution.py:345
  41.7 1.3 %collective-permute-start.16 = (f32[4,8,512]{2,1,0:T(8,128)S(1)}, f32[4,8,512]{2,1,0:T(8,128)S(1)}, u32[]{:S(2)}, u32[]{:S(2)}) collective-permute-start(f32[4,8,512]{2,1,0:T(8,128)S(1)} %get-tuple-element.20), channel_id=1, source_target_pairs={{0,1},{1,0},{2,3},{3,2},{4,5},{5,4},{6,7},{7,6},{8,9},{9,8},{10,11... | collective-permute-start | bytes 196616 | tf_op jit(solution)/shard_map/ppermute | solution.py:345
  43.1 3.8 %collective-permute-start.18 = (bf16[2,8,512]{2,1,0:T(8,128)(2,1)S(1)}, bf16[2,8,512]{2,1,0:T(8,128)(2,1)S(1)}, u32[]{:S(2)}, u32[]{:S(2)}) collective-permute-start(bf16[2,8,512]{2,1,0:T(8,128)(2,1)S(1)} %get-tuple-element.23), channel_id=1, source_target_pairs={{0,2},{1,7},{2,0},{3,5},{4,6},{5,3},{6,4},{7,1},{8,10},{9,15},{10,... | collective-permute-start | bytes 49160 | tf_op jit(solution)/shard_map/ppermute | solution.py:345
  44.0 5.4 %collective-permute-start.17 = (bf16[8,512]{1,0:T(8,128)(2,1)S(1)}, bf16[8,512]{1,0:T(8,128)(2,1)S(1)}, u32[]{:S(2)}, u32[]{:S(2)}) collective-permute-start(bf16[8,512]{1,0:T(8,128)(2,1)S(1)} %get-tuple-element.22), channel_id=1, source_target_pairs={{0,4},{1,5},{2,6},{3,7},{4,0},{5,1},{6,2},{7,3},{8,12},{9,13},{10,... | collective-permute-start | bytes 24584 | tf_op jit(solution)/shard_map/ppermute | solution.py:345
  46.9 2.5 %collective-permute-start.19 = (bf16[2,8,512]{2,1,0:T(8,128)(2,1)S(1)}, bf16[2,8,512]{2,1,0:T(8,128)(2,1)S(1)}, u32[]{:S(2)}, u32[]{:S(2)}) collective-permute-start(bf16[2,8,512]{2,1,0:T(8,128)(2,1)S(1)} %collective-permute-done.18.far_ref), channel_id=1, source_target_pairs={{0,1},{1,0},{2,3},{3,2},{4,5},{5,4},{6,7},{7,6},{8,9},{9,8},{10,11... | collective-permute-start | bytes 49160 | tf_op jit(solution)/shard_map/ppermute | solution.py:345
  (16 other events, 228.1 us)

commit v4 on v3

--- a/solution.py
+++ b/solution.py
@@ -129,46 +129,78 @@
     pair_ref[1 - core] = mate_ref[...]
 
 
-def normed_pieces(pair_refs, gain_ref, rows_ref):
-    chip = lax.axis_index("kv")
-    cores, _, width = pair_refs[0].shape
-    for step, pair_ref in placed_blocks(lax.axis_index("tp"), *pair_refs):
-        first = lax.bitwise_xor(chip, step) * (cores * width)
-        for core in range(cores):
-            place = pl.ds(pl.multiple_of(first + core * width, width), width)
-            rows_ref[:, place] = pair_ref[core].astype(jnp.float32)
-    rows = rows_ref[...]
-    inv_root = lax.rsqrt(jnp.mean(rows * rows, axis=1, keepdims=True) + epsilon)
-    return (rows * inv_root * gain_ref[...]).astype(jnp.bfloat16)
+def pair_columns(step, width):
+    first = lax.bitwise_xor(lax.axis_index("kv"), step) * width
+    return pl.ds(pl.multiple_of(first, width), width)
+
+
+def flat_pair(pair_ref):
+    return jnp.concatenate([pair_ref[0], pair_ref[1]], axis=1).astype(jnp.float32)
+
+
+def scaled_pair(rows, gain_ref, columns):
+    return (rows * gain_ref[:, columns]).astype(jnp.bfloat16)
+
+
+def head_weight(weight_refs, head, columns):
+    return jnp.concatenate(
+        [ref[one, :, columns] for one in (head, head + 1) for ref in weight_refs], axis=0
+    )
+
+
+def add_projections(steps, gain_ref, weight_refs, start, total_ref):
+    heads, chan, _ = weight_refs[0].shape
+    lanes = 8 * chan
+    blocks = []
+    for step, pair_ref in steps:
+        rows = flat_pair(pair_ref)
+        columns = pair_columns(step, rows.shape[1])
+        blocks.append((scaled_pair(rows, gain_ref, columns), columns))
+    for head in range(0, heads, 2):
+        place = slice(head // 2 * lanes, (head // 2 + 1) * lanes)
+        total = start(place)
+        for scaled, columns in blocks:
+            part = lax.dot_general(
+                scaled,
+                head_weight(weight_refs, head, columns),
+                (((1,), (1,)), ((), ())),
+                preferred_element_type=jnp.float32,
+            )
+            total = part if total is None else total + part
+        total_ref[:, place] = total
+
+
+def early_project_kernel(near_ref, far_ref, gain_ref, *refs):
+    weight_refs, total_ref = refs[:4], refs[4]
+    steps = ((0, near_ref), (far_step(lax.axis_index("tp")), far_ref))
+    add_projections(steps, gain_ref, weight_refs, lambda place: None, total_ref)
+
+
+def inverse_root(pair_refs):
+    squares, width = 0.0, 0
+    for pair_ref in pair_refs:
+        rows = flat_pair(pair_ref)
+        squares = squares + jnp.sum(rows * rows, axis=1, keepdims=True)
+        width += rows.shape[1]
+    return lax.rsqrt(squares / width + epsilon)
 
 
 def project_kernel(chips, *refs):
-    pair_refs, (gain_ref, query_ref, forget_ref, value_ref, gate_ref) = refs[:chips], refs[chips : chips + 5]
-    near_ref, mid_ref, far_ref, swap_ref, rows_ref, made_ref = refs[chips + 5 :]
-    normed = normed_pieces(pair_refs, gain_ref, rows_ref)
-    rows = normed.shape[0]
-    heads, chan, _ = query_ref.shape
-    lanes = 4 * chan
-    for head in range(0, heads, 2):
-        weight = jnp.concatenate(
-            [
-                ref[one]
-                for one in (head, head + 1)
-                for ref in (query_ref, forget_ref, value_ref, gate_ref)
-            ],
-            axis=0,
-        )
-        product = lax.dot_general(
-            normed, weight, (((1,), (1,)), ((), ())), preferred_element_type=jnp.float32
-        )
-        product = product.astype(jnp.bfloat16).astype(jnp.float32)
-        made_ref[pl.ds(head, rows, stride=heads), :] = product[:, :lanes]
-        made_ref[pl.ds(head + 1, rows, stride=heads), :] = product[:, lanes:]
+    pair_refs, (early_ref, gain_ref) = refs[:chips], refs[chips : chips + 2]
+    weight_refs = refs[chips + 2 : chips + 6]
+    near_ref, mid_ref, far_ref, swap_ref, total_ref, made_ref = refs[chips + 6 :]
+    core = lax.axis_index("tp")
+    steps = ((2, pair_refs[1]), (far_step(1 - core), pair_refs[3]))
+    add_projections(steps, gain_ref, weight_refs, lambda place: early_ref[:, place], total_ref)
+    heads, chan, _ = weight_refs[0].shape
+    rows, lanes = total_ref.shape[0], 4 * chan
+    product = total_ref[...] * inverse_root(pair_refs)
+    product = product.astype(jnp.bfloat16).astype(jnp.float32)
+    for head in range(heads):
+        made_ref[pl.ds(head, rows, stride=heads), :] = product[:, head * lanes : (head + 1) * lanes]
     chip = lax.axis_index("kv")
     pairs = rows * heads // chips
-    for step, sent_ref in placed_blocks(
-        lax.axis_index("tp"), near_ref, mid_ref, far_ref, swap_ref
-    ):
+    for step, sent_ref in placed_blocks(core, near_ref, mid_ref, far_ref, swap_ref):
         first = pl.multiple_of(lax.bitwise_xor(chip, step) * pairs, pairs)
         sent_ref[...] = made_ref[pl.ds(first, pairs), :]
 
@@ -215,16 +247,25 @@
     value_ref[...] = value_rows
 
 
-def state_kernel(key_ref, value_ref, state_ref, next_ref):
+def state_kernel(key_ref, value_ref, state_ref, next_ref, made_ref, done_ref):
     own_rows, heads, _, _ = state_ref.shape
     key_cols = jnp.transpose(key_ref[...])
+    copies = []
     for row in range(own_rows):
         for head in range(heads):
             pair = row * heads + head
             old = state_ref[row, head]
-            next_ref[row, head] = old + key_cols[:, pair : pair + 1] * (
+            made_ref[pair] = old + key_cols[:, pair : pair + 1] * (
                 value_ref[pair : pair + 1, :] - old
             )
+            copies.append(
+                pltpu.make_async_copy(made_ref.at[pair], next_ref.at[row, head], done_ref.at[pair])
+            )
+            if pair > 0:
+                copies[pair - 1].start()
+    copies[-1].start()
+    for copy in copies:
+        copy.wait()
 
 
 def stage_kernel(block_ref, staged_ref):
@@ -278,14 +319,33 @@
         )
 
 
+def up_part(steps, gain_ref, up_ref, total):
+    for step, pair_ref in steps:
+        rows = flat_pair(pair_ref)
+        columns = pair_columns(step, rows.shape[1])
+        part = jnp.dot(
+            scaled_pair(rows, gain_ref, columns),
+            up_ref[columns, :],
+            preferred_element_type=jnp.float32,
+        )
+        total = part if total is None else total + part
+    return total
+
+
+def early_up_kernel(near_ref, far_ref, gain_ref, up_ref, early_ref):
+    steps = ((0, near_ref), (far_step(lax.axis_index("tp")), far_ref))
+    early_ref[...] = up_part(steps, gain_ref, up_ref, None)
+
+
 def mixer_kernel(chips, *refs):
-    pair_refs, (gain_ref, up_ref, down_ref) = refs[:chips], refs[chips : chips + 3]
-    hidden_ref, partial_ref, rows_ref = refs[chips + 3 :]
-    normed = normed_pieces(pair_refs, gain_ref, rows_ref)
-    hidden = jnp.dot(normed, up_ref[...], preferred_element_type=jnp.float32)
+    pair_refs, (early_ref, gain_ref, up_ref, down_ref) = refs[:chips], refs[chips : chips + 4]
+    hidden_ref, partial_ref = refs[chips + 4 :]
+    core = lax.axis_index("tp")
+    steps = ((2, pair_refs[1]), (far_step(1 - core), pair_refs[3]))
+    hidden = up_part(steps, gain_ref, up_ref, early_ref[...]) * inverse_root(pair_refs)
     hidden = jnp.square(jnp.maximum(hidden, 0.0)).astype(jnp.bfloat16)
     hidden_ref[...] = hidden
-    down_part(hidden, down_ref, 1 - lax.axis_index("tp"), partial_ref)
+    down_part(hidden, down_ref, 1 - core, partial_ref)
 
 
 def own_part_kernel(hidden_ref, down_ref, partial_ref):
@@ -299,8 +359,7 @@
     kept_ref[...] = own_ref[3] + mate_ref[3]
 
 
-def last_kernel(residual_ref, kept_ref, mid_ref, far_ref, swapped_ref, state_ref, output_ref):
-    del state_ref
+def last_kernel(residual_ref, kept_ref, mid_ref, far_ref, swapped_ref, output_ref):
     core = lax.axis_index("tp")
     total = kept_ref[...]
     for block in (mid_ref[...], far_ref[core], swapped_ref[core]):
@@ -309,7 +368,7 @@
 
 
 MIB = 1 << 20
-COST = (10**11, 10**11, 10**9, 10**9, 10**6, 10**6, 10**9, 10**6, 10**6)
+COST = (10**11, 10**11, 10**9, 10**9, 10**6, 10**6, 10**9, 10**6, 10**6, 10**9, 10**6)
 
 
 def tiled_local(
@@ -330,7 +389,7 @@
     down_weight,
 ):
     rows, width = tokens.shape
-    heads, chan, model = query_weight.shape
+    heads, chan, _ = query_weight.shape
     own_rows, _, keys, values = recurrent_state.shape
     pairs = own_rows * heads
     shape = jax.ShapeDtypeStruct
@@ -360,20 +419,23 @@
         return (pair,) + crossed(pair, pair)
 
     staged = call(stage_kernel, shape(tokens.shape, bf16), (tokens,), COST[4], MIB)
+    pairs_of_rows = gather_pairs(tokens, staged, COST[0])
+    mix_row = mix_gain.reshape(1, -1)
+    projections = (query_weight, forget_weight, value_weight, gate_weight)
+    early = call(
+        early_project_kernel,
+        shape((rows, 4 * heads * chan), f32),
+        (pairs_of_rows[0], pairs_of_rows[2], mix_row, *projections),
+        COST[9],
+        14 * MIB,
+    )
     near, mid, far, swap = call(
         functools.partial(project_kernel, kv),
         [shape((pairs, 4 * chan), f32)] * kv,
-        (
-            *gather_pairs(tokens, staged, COST[0]),
-            mix_gain.reshape(1, -1),
-            query_weight,
-            forget_weight,
-            value_weight,
-            gate_weight,
-        ),
+        (*pairs_of_rows, early, mix_row, *projections),
         COST[1],
-        4 * MIB,
-        [pltpu.VMEM((rows, model), f32), pltpu.VMEM((rows * heads, 4 * chan), f32)],
+        14 * MIB,
+        [pltpu.VMEM((rows, 4 * heads * chan), f32), pltpu.VMEM((rows * heads, 4 * chan), f32)],
     )
     got = (near,) + crossed(paired(far, other_core(swap), COST[4]), mid)
     mixed, key_rows, value_rows = call(
@@ -381,34 +443,44 @@
         [shape((pairs, values), f32), shape((pairs, keys), f32), shape((pairs, values), f32)],
         (*got, lower_bound, recurrent_state, head_gain),
         COST[2],
-        4 * MIB,
+        14 * MIB,
         [pltpu.VMEM((kv, pairs, 4 * chan), f32)],
     )
-    next_state = call(
+    next_state = pl.pallas_call(
         state_kernel,
-        shape(recurrent_state.shape, f32),
-        (key_rows, value_rows, recurrent_state),
-        COST[3],
-        4 * MIB,
-    )
+        out_shape=shape(recurrent_state.shape, f32),
+        in_specs=[whole] * 3,
+        out_specs=pl.BlockSpec(memory_space=pl.ANY),
+        scratch_shapes=[pltpu.VMEM((pairs, keys, values), f32), pltpu.SemaphoreType.DMA((pairs,))],
+        compiler_params=pltpu.CompilerParams(vmem_limit_bytes=6 * MIB),
+        cost_estimate=pl.CostEstimate(flops=COST[3], bytes_accessed=0, transcendentals=0),
+    )(key_rows, value_rows, recurrent_state)
     residual = call(
         functools.partial(out_kernel, kv, heads),
         shape((rows, width), bf16),
-        (*gather_pairs(mixed, mixed, COST[4]), staged, out_weight),
+        (*gather_pairs(mixed, mixed, COST[4]), tokens, out_weight),
         COST[4],
-        4 * MIB,
+        14 * MIB,
         [pltpu.VMEM((kv * tp * pairs, values), f32)],
+    )
+    pairs_of_rows = gather_pairs(residual, residual, COST[4])
+    mlp_row = mlp_gain.reshape(1, -1)
+    early = call(
+        early_up_kernel,
+        shape((rows, up_weight.shape[1]), f32),
+        (pairs_of_rows[0], pairs_of_rows[2], mlp_row, up_weight),
+        COST[10],
+        14 * MIB,
     )
     hidden, mate_part = call(
         functools.partial(mixer_kernel, kv),
         [shape((rows, up_weight.shape[1]), bf16), shape((kv, rows, width), f32)],
-        (*gather_pairs(residual, residual, COST[4]), mlp_gain.reshape(1, -1), up_weight, down_weight),
+        (*pairs_of_rows, early, mlp_row, up_weight, down_weight),
         COST[5],
-        4 * MIB,
-        [pltpu.VMEM((rows, model), f32)],
+        14 * MIB,
     )
     own_part = call(
-        own_part_kernel, shape((kv, rows, width), f32), (hidden, down_weight), COST[6], 4 * MIB
+        own_part_kernel, shape((kv, rows, width), f32), (hidden, down_weight), COST[6], 14 * MIB
     )
     far, mid, kept = call(
         chip_sum_kernel,
@@ -419,7 +491,7 @@
     )
     sums = crossed(far, mid)
     layer_output = call(
-        last_kernel, shape((rows, width), bf16), (residual, kept, *sums, next_state), COST[8], MIB
+        last_kernel, shape((rows, width), bf16), (residual, kept, *sums), COST[8], MIB
     )
     return (layer_output, next_state)
 

time: 51.4 us -> 48 us (0.934)
  waiting for transfers between devices: 16.5 us -> 13.2 us
  local copies, waits for them, and re-layouts: 2.01 us -> 0.81 us
  starting transfers between devices: 21.6 us -> 22.7 us
    ppermute x20, waiting for transfers between devices: 16.5 us -> 13.2 us  [permute(): return lax.ppermute(block, group, hops)]
    pallas_call x13 -> x14, Pallas kernels: 10.2 us -> 8.85 us  [call(): pl.pallas_call(body, out_shape=outs, in_specs=[whole] * len(arrays), out_...]
    pallas_call x0 -> x1, Pallas kernels: none -> 1.31 us  [tiled_local(): pl.pallas_call(state_kernel, out_shape=shape(recurrent_state.shape, f32),...]
    unnamed x40, local copies, waits for them, and re-layouts: 2.01 us -> 0.81 us
    ppermute x20, starting transfers between devices: 21.6 us -> 22.7 us  [permute(): return lax.ppermute(block, group, hops)]
  transfers between devices with their start and end apart: 20 -> 20, of which waited for: 12 -> 12; matrix products, arithmetic and copies ran while one was open for 0% -> 0% of each run, Pallas kernels for 5% -> 10%
where the time goes in v4:
time: 48 us; the launch traced here: 47.8 us
  starting transfers between devices  22.7 us (47%)
  waiting for transfers between devices  13.2 us (28%)
  Pallas kernels  10.2 us (21%)
  between operations  0.91 us (2%)
  local copies, waits for them, and re-layouts  0.81 us (2%)
    ppermute x20, starting transfers between devices, permute(): return lax.ppermute(block, group, hops)  22.7 us
    ppermute x20, waiting for transfers between devices, permute(): return lax.ppermute(block, group, hops)  13.2 us
    pallas_call x14, Pallas kernels, call(): pl.pallas_call(body, out_shape=outs, in_specs=[whole] * len(arrays), out_...  8.85 us
    pallas_call x1, Pallas kernels, tiled_local(): pl.pallas_call(state_kernel, out_shape=shape(recurrent_state.shape, f32),...  1.31 us
  transfers between devices with their start and end apart: 20, of which 12 were waited for; matrix products, arithmetic and copies ran while one was open for 0% of the time, Pallas kernels for 10%

profile of v4, /device:TPU:0, one launch (start us, length us, event | category | flops | bytes accessed | tf_op | source)
XLA Modules:
  0.0 47.8 jit_solution(13897000221221241469)
XLA Ops:
  2.2 2.9 %collective-permute-start.2 = (bf16[2,8,512]{2,1,0:T(8,128)(2,1)S(1)}, bf16[2,8,512]{2,1,0:T(8,128)(2,1)S(1)}, u32[]{:S(2)}, u32[]{:S(2)}) collective-permute-start(bf16[2,8,512]{2,1,0:T(8,128)(2,1)S(1)} %shard_map.141.near_ref.refs_0_), channel_id=1, source_target_pairs={{0,2},{1,7},{2,0},{3,5},{4,6},{5,3},{6,4},{7,1},{8,10},{9,15},{10,... | collective-permute-start | bytes 49160 | tf_op jit(solution)/shard_map/ppermute | solution.py:404
  5.1 2.6 %collective-permute-start.1 = (bf16[2,8,512]{2,1,0:T(8,128)(2,1)S(1)}, bf16[2,8,512]{2,1,0:T(8,128)(2,1)S(1)}, u32[]{:S(2)}, u32[]{:S(2)}) collective-permute-start(bf16[2,8,512]{2,1,0:T(8,128)(2,1)S(1)} %shard_map.141.near_ref.refs_0_), channel_id=1, source_target_pairs={{0,4},{1,5},{2,6},{3,7},{4,0},{5,1},{6,2},{7,3},{8,12},{9,13},{10,... | collective-permute-start | bytes 49160 | tf_op jit(solution)/shard_map/ppermute | solution.py:404
  8.2 1.2 %shard_map.142.refs_4_ = f32[8,1024]{1,0:T(8,128)S(1)} custom-call(bf16[2,8,512]{2,1,0:T(8,128)(2,1)S(1)} %shard_map.141.near_ref.refs_0_, bf16[2,8,512]{2,1,0:T(8,128)(2,1)S(1)} %collective-permute-done.2.far_ref.refs_2_, f32[1,4096]{1,0:T(1,128)S(1)} %bitcast.8, bf16[8,32,4096]{2,1,0:T(8,128)(2,1)S(1)} %copy-done.1, bf16[8,32,4096]{2,1,0:T(8,128)(2,1)S(1)} %copy-done.2, ...), custom_call_target="tpu_custom_call" | custom-call | flops 1000000000 | tf_op jit(solution)/shard_map/pallas_call | solution.py:102
  9.9 1.2 %shard_map.143 = (f32[16,128]{1,0:T(8,128)S(1)}, f32[16,128]{1,0:T(8,128)S(1)}, f32[16,128]{1,0:T(8,128)S(1)}, f32[16,128]{1,0:T(8,128)S(1)}) custom-call(bf16[2,8,512]{2,1,0:T(8,128)(2,1)S(1)} %shard_map.141.near_ref.refs_0_, bf16[2,8,512]{2,1,0:T(8,128)(2,1)S(1)} %collective-permute-done.1.refs_1_, ...), custom_call_target="tpu_custom_call" | custom-call | flops 99999997952 | tf_op jit(solution)/shard_map/pallas_call | solution.py:102
  11.8 0.8 %collective-permute-done.5.mate_ref = f32[16,128]{1,0:T(8,128)S(1)} collective-permute-done((f32[16,128]{1,0:T(8,128)S(1)}, f32[16,128]{1,0:T(8,128)S(1)}, u32[]{:S(2)}, u32[]{:S(2)}) %collective-permute-start.5) | collective-permute-done | bytes 8224 | tf_op jit(solution)/shard_map/ppermute | solution.py:404
  12.9 3.5 %collective-permute-done.6.refs_2_ = f32[2,16,128]{2,1,0:T(8,128)S(1)} collective-permute-done((f32[2,16,128]{2,1,0:T(8,128)S(1)}, f32[2,16,128]{2,1,0:T(8,128)S(1)}, u32[]{:S(2)}, u32[]{:S(2)}) %collective-permute-start.6) | collective-permute-done | bytes 16416 | tf_op jit(solution)/shard_map/ppermute | solution.py:404
  16.4 1.0 %collective-permute-start.7 = (f32[2,16,128]{2,1,0:T(8,128)S(1)}, f32[2,16,128]{2,1,0:T(8,128)S(1)}, u32[]{:S(2)}, u32[]{:S(2)}) collective-permute-start(f32[2,16,128]{2,1,0:T(8,128)S(1)} %collective-permute-done.6.refs_2_), channel_id=1, source_target_pairs={{0,1},{1,0},{2,3},{3,2},{4,5},{5,4},{6,7},{7,6},{8,9},{9,8},{10,11... | collective-permute-start | bytes 49160 | tf_op jit(solution)/shard_map/ppermute | solution.py:404
  17.4 1.2 %collective-permute-start.4 = (f32[16,128]{1,0:T(8,128)S(1)}, f32[16,128]{1,0:T(8,128)S(1)}, u32[]{:S(2)}, u32[]{:S(2)}) collective-permute-start(f32[16,128]{1,0:T(8,128)S(1)} %get-tuple-element.15), channel_id=1, source_target_pairs={{0,4},{1,5},{2,6},{3,7},{4,0},{5,1},{6,2},{7,3},{8,12},{9,13},{10,... | collective-permute-start | bytes 24584 | tf_op jit(solution)/shard_map/ppermute | solution.py:404
  18.6 3.4 %collective-permute-done.4.refs_1_ = f32[16,128]{1,0:T(8,128)S(1)} collective-permute-done((f32[16,128]{1,0:T(8,128)S(1)}, f32[16,128]{1,0:T(8,128)S(1)}, u32[]{:S(2)}, u32[]{:S(2)}) %collective-permute-start.4) | collective-permute-done | bytes 8224 | tf_op jit(solution)/shard_map/ppermute | solution.py:404
  22.8 1.2 %collective-permute-done.8.mate_ref = f32[16,128]{1,0:T(8,128)S(1)} collective-permute-done((f32[16,128]{1,0:T(8,128)S(1)}, f32[16,128]{1,0:T(8,128)S(1)}, u32[]{:S(2)}, u32[]{:S(2)}) %collective-permute-start.8) | collective-permute-done | bytes 8224 | tf_op jit(solution)/shard_map/ppermute | solution.py:404
  24.3 2.9 %collective-permute-start.9 = (f32[2,16,128]{2,1,0:T(8,128)S(1)}, f32[2,16,128]{2,1,0:T(8,128)S(1)}, u32[]{:S(2)}, u32[]{:S(2)}) collective-permute-start(f32[2,16,128]{2,1,0:T(8,128)S(1)} %shard_map.146.refs_0_), channel_id=1, source_target_pairs={{0,4},{1,5},{2,6},{3,7},{4,0},{5,1},{6,2},{7,3},{8,12},{9,13},{10,... | collective-permute-start | bytes 49160 | tf_op jit(solution)/shard_map/ppermute | solution.py:404
  27.7 0.8 %collective-permute-start.11 = (f32[2,16,128]{2,1,0:T(8,128)S(1)}, f32[2,16,128]{2,1,0:T(8,128)S(1)}, u32[]{:S(2)}, u32[]{:S(2)}) collective-permute-start(f32[2,16,128]{2,1,0:T(8,128)S(1)} %collective-permute-done.10.refs_2_), channel_id=1, source_target_pairs={{0,1},{1,0},{2,3},{3,2},{4,5},{5,4},{6,7},{7,6},{8,9},{9,8},{10,11... | collective-permute-start | bytes 49160 | tf_op jit(solution)/shard_map/ppermute | solution.py:404
  29.7 0.8 %collective-permute-start.12 = (bf16[8,512]{1,0:T(8,128)(2,1)S(1)}, bf16[8,512]{1,0:T(8,128)(2,1)S(1)}, u32[]{:S(2)}, u32[]{:S(2)}) collective-permute-start(bf16[8,512]{1,0:T(8,128)(2,1)S(1)} %shard_map.147.own_ref.residual_ref), channel_id=1, source_target_pairs={{0,1},{1,0},{2,3},{3,2},{4,5},{5,4},{6,7},{7,6},{8,9},{9,8},{10,11... | collective-permute-start | bytes 24584 | tf_op jit(solution)/shard_map/ppermute | solution.py:404
  30.5 0.8 %collective-permute-done.12.mate_ref = bf16[8,512]{1,0:T(8,128)(2,1)S(1)} collective-permute-done((bf16[8,512]{1,0:T(8,128)(2,1)S(1)}, bf16[8,512]{1,0:T(8,128)(2,1)S(1)}, u32[]{:S(2)}, u32[]{:S(2)}) %collective-permute-start.12) | collective-permute-done | bytes 8224 | tf_op jit(solution)/shard_map/ppermute | solution.py:404
  31.3 0.9 %collective-permute-start.14 = (bf16[2,8,512]{2,1,0:T(8,128)(2,1)S(1)}, bf16[2,8,512]{2,1,0:T(8,128)(2,1)S(1)}, u32[]{:S(2)}, u32[]{:S(2)}) collective-permute-start(bf16[2,8,512]{2,1,0:T(8,128)(2,1)S(1)} %shard_map.148.near_ref.refs_0_), channel_id=1, source_target_pairs={{0,2},{1,7},{2,0},{3,5},{4,6},{5,3},{6,4},{7,1},{8,10},{9,15},{10,... | collective-permute-start | bytes 49160 | tf_op jit(solution)/shard_map/ppermute | solution.py:404
  32.2 2.1 %collective-permute-start.13 = (bf16[2,8,512]{2,1,0:T(8,128)(2,1)S(1)}, bf16[2,8,512]{2,1,0:T(8,128)(2,1)S(1)}, u32[]{:S(2)}, u32[]{:S(2)}) collective-permute-start(bf16[2,8,512]{2,1,0:T(8,128)(2,1)S(1)} %shard_map.148.near_ref.refs_0_), channel_id=1, source_target_pairs={{0,4},{1,5},{2,6},{3,7},{4,0},{5,1},{6,2},{7,3},{8,12},{9,13},{10,... | collective-permute-start | bytes 49160 | tf_op jit(solution)/shard_map/ppermute | solution.py:404
  35.1 1.0 %collective-permute-start.15 = (bf16[2,8,512]{2,1,0:T(8,128)(2,1)S(1)}, bf16[2,8,512]{2,1,0:T(8,128)(2,1)S(1)}, u32[]{:S(2)}, u32[]{:S(2)}) collective-permute-start(bf16[2,8,512]{2,1,0:T(8,128)(2,1)S(1)} %collective-permute-done.14.far_ref.refs_2_), channel_id=1, source_target_pairs={{0,1},{1,0},{2,3},{3,2},{4,5},{5,4},{6,7},{7,6},{8,9},{9,8},{10,11... | collective-permute-start | bytes 49160 | tf_op jit(solution)/shard_map/ppermute | solution.py:404
  36.1 1.2 %shard_map.149.refs_4_ = f32[8,2048]{1,0:T(8,128)S(1)} custom-call(bf16[2,8,512]{2,1,0:T(8,128)(2,1)S(1)} %shard_map.148.near_ref.refs_0_, bf16[2,8,512]{2,1,0:T(8,128)(2,1)S(1)} %collective-permute-done.14.far_ref.refs_2_, f32[1,4096]{1,0:T(1,128)S(1)} %bitcast.6, bf16[4096,2048]{1,0:T(8,128)(2,1)S(1)} %bitcast.3), custom_call_target="tpu_custom_call" | custom-call | flops 1000000 | tf_op jit(solution)/shard_map/pallas_call | solution.py:102
  37.4 2.3 %shard_map.150 = (bf16[8,2048]{1,0:T(8,128)(2,1)S(1)}, f32[4,8,512]{2,1,0:T(8,128)S(1)}) custom-call(bf16[2,8,512]{2,1,0:T(8,128)(2,1)S(1)} %shard_map.148.near_ref.refs_0_, bf16[2,8,512]{2,1,0:T(8,128)(2,1)S(1)} %collective-permute-done.13.refs_1_, bf16[2,8,512]{2,1,0:T(8,128)(2,1)S(1)} %collective-permute-done.14.far_ref.refs_2_, ...), custom_call_target="tpu_custom_call" | custom-call | flops 1000000 | tf_op jit(solution)/shard_map/pallas_call | solution.py:102
  39.8 1.2 %shard_map.151.own_ref = f32[4,8,512]{2,1,0:T(8,128)S(1)} custom-call(bf16[8,2048]{1,0:T(8,128)(2,1)S(1)} %get-tuple-element.19.hidden_ref, bf16[2048,4096]{1,0:T(8,128)(2,1)S(1)} %bitcast.5), custom_call_target="tpu_custom_call" | custom-call | flops 1000000000 | tf_op jit(solution)/shard_map/pallas_call | solution.py:102
  41.7 2.3 %collective-permute-start.17 = (bf16[8,512]{1,0:T(8,128)(2,1)S(1)}, bf16[8,512]{1,0:T(8,128)(2,1)S(1)}, u32[]{:S(2)}, u32[]{:S(2)}) collective-permute-start(bf16[8,512]{1,0:T(8,128)(2,1)S(1)} %get-tuple-element.22), channel_id=1, source_target_pairs={{0,4},{1,5},{2,6},{3,7},{4,0},{5,1},{6,2},{7,3},{8,12},{9,13},{10,... | collective-permute-start | bytes 24584 | tf_op jit(solution)/shard_map/ppermute | solution.py:404
  44.0 0.8 %collective-permute-done.18.far_ref = bf16[2,8,512]{2,1,0:T(8,128)(2,1)S(1)} collective-permute-done((bf16[2,8,512]{2,1,0:T(8,128)(2,1)S(1)}, bf16[2,8,512]{2,1,0:T(8,128)(2,1)S(1)}, u32[]{:S(2)}, u32[]{:S(2)}) %collective-permute-start.18) | collective-permute-done | bytes 16416 | tf_op jit(solution)/shard_map/ppermute | solution.py:404
  44.8 1.1 %collective-permute-start.19 = (bf16[2,8,512]{2,1,0:T(8,128)(2,1)S(1)}, bf16[2,8,512]{2,1,0:T(8,128)(2,1)S(1)}, u32[]{:S(2)}, u32[]{:S(2)}) collective-permute-start(bf16[2,8,512]{2,1,0:T(8,128)(2,1)S(1)} %collective-permute-done.18.far_ref), channel_id=1, source_target_pairs={{0,1},{1,0},{2,3},{3,2},{4,5},{5,4},{6,7},{7,6},{8,9},{9,8},{10,11... | collective-permute-start | bytes 49160 | tf_op jit(solution)/shard_map/ppermute | solution.py:404
  45.8 1.3 %shard_map.154 = f32[2,8,128,128]{3,2,1,0:T(8,128)} custom-call(f32[16,128]{1,0:T(8,128)S(1)} %get-tuple-element.24.key_ref, f32[16,128]{1,0:T(8,128)S(1)} %get-tuple-element.25.value_ref, f32[2,8,128,128]{3,2,1,0:T(8,128)S(1)} %copy-done.9), custom_call_target="tpu_custom_call" | custom-call | flops 1000000000 | tf_op jit(solution)/shard_map/pallas_call | solution.py:449
  (73 shorter events, 8.4 us)
Async XLA Ops:
  0.6 1.6 %collective-permute-start = (bf16[8,512]{1,0:T(8,128)(2,1)}, bf16[8,512]{1,0:T(8,128)(2,1)S(1)}, u32[]{:S(2)}, u32[]{:S(2)}) collective-permute-start(bf16[8,512]{1,0:T(8,128)(2,1)} %refs_4_.3), channel_id=1, source_target_pairs={{0,1},{1,0},{2,3},{3,2},{4,5},{5,4},{6,7},{7,6},{8,9},{9,8},{10,11... | collective-permute-start | bytes 24584 | tf_op jit(solution)/shard_map/ppermute | solution.py:404
  2.2 5.5 %collective-permute-start.2 = (bf16[2,8,512]{2,1,0:T(8,128)(2,1)S(1)}, bf16[2,8,512]{2,1,0:T(8,128)(2,1)S(1)}, u32[]{:S(2)}, u32[]{:S(2)}) collective-permute-start(bf16[2,8,512]{2,1,0:T(8,128)(2,1)S(1)} %shard_map.141.near_ref.refs_0_), channel_id=1, source_target_pairs={{0,2},{1,7},{2,0},{3,5},{4,6},{5,3},{6,4},{7,1},{8,10},{9,15},{10,... | collective-permute-start | bytes 49160 | tf_op jit(solution)/shard_map/ppermute | solution.py:404
  5.1 4.7 %collective-permute-start.1 = (bf16[2,8,512]{2,1,0:T(8,128)(2,1)S(1)}, bf16[2,8,512]{2,1,0:T(8,128)(2,1)S(1)}, u32[]{:S(2)}, u32[]{:S(2)}) collective-permute-start(bf16[2,8,512]{2,1,0:T(8,128)(2,1)S(1)} %shard_map.141.near_ref.refs_0_), channel_id=1, source_target_pairs={{0,4},{1,5},{2,6},{3,7},{4,0},{5,1},{6,2},{7,3},{8,12},{9,13},{10,... | collective-permute-start | bytes 49160 | tf_op jit(solution)/shard_map/ppermute | solution.py:404
  7.7 2.2 %collective-permute-start.3 = (bf16[2,8,512]{2,1,0:T(8,128)(2,1)S(1)}, bf16[2,8,512]{2,1,0:T(8,128)(2,1)S(1)}, u32[]{:S(2)}, u32[]{:S(2)}) collective-permute-start(bf16[2,8,512]{2,1,0:T(8,128)(2,1)S(1)} %collective-permute-done.2.far_ref.refs_2_), channel_id=1, source_target_pairs={{0,1},{1,0},{2,3},{3,2},{4,5},{5,4},{6,7},{7,6},{8,9},{9,8},{10,11... | collective-permute-start | bytes 49160 | tf_op jit(solution)/shard_map/ppermute | solution.py:404
  8.2 27.9 %slice-start = ((s8[16777216]{0:T(1024)(128)(4,1)}), s8[4194304]{0:T(1024)(128)(4,1)S(1)}, s32[]{:S(2)}) async-start(s8[16777216]{0:T(1024)(128)(4,1)} %bitcast.2), calls=%async_computation | async-start | bytes 8388608
  8.2 29.1 %slice-start.4 = ((s8[16777216]{0:T(1024)(128)(4,1)}), s8[4194304]{0:T(1024)(128)(4,1)S(1)}, s32[]{:S(2)}) async-start(s8[16777216]{0:T(1024)(128)(4,1)} %bitcast.4), calls=%async_computation.4 | async-start | bytes 8388608
  9.5 27.8 %slice-start.5 = ((s8[16777216]{0:T(1024)(128)(4,1)}), s8[4194304]{0:T(1024)(128)(4,1)S(1)}, s32[]{:S(2)}) async-start(s8[16777216]{0:T(1024)(128)(4,1)} %bitcast.4), calls=%async_computation.5 | async-start | bytes 8388608
  9.5 27.8 %slice-start.6 = ((s8[16777216]{0:T(1024)(128)(4,1)}), s8[4194304]{0:T(1024)(128)(4,1)S(1)}, s32[]{:S(2)}) async-start(s8[16777216]{0:T(1024)(128)(4,1)} %bitcast.4), calls=%async_computation.6 | async-start | bytes 8388608
  11.1 1.6 %collective-permute-start.5 = (f32[16,128]{1,0:T(8,128)S(1)}, f32[16,128]{1,0:T(8,128)S(1)}, u32[]{:S(2)}, u32[]{:S(2)}) collective-permute-start(f32[16,128]{1,0:T(8,128)S(1)} %get-tuple-element.17), channel_id=1, source_target_pairs={{0,1},{1,0},{2,3},{3,2},{4,5},{5,4},{6,7},{7,6},{8,9},{9,8},{10,11... | collective-permute-start | bytes 24584 | tf_op jit(solution)/shard_map/ppermute | solution.py:404
  12.7 3.7 %collective-permute-start.6 = (f32[2,16,128]{2,1,0:T(8,128)S(1)}, f32[2,16,128]{2,1,0:T(8,128)S(1)}, u32[]{:S(2)}, u32[]{:S(2)}) collective-permute-start(f32[2,16,128]{2,1,0:T(8,128)S(1)} %shard_map.144), channel_id=1, source_target_pairs={{0,2},{1,7},{2,0},{3,5},{4,6},{5,3},{6,4},{7,1},{8,10},{9,15},{10,... | collective-permute-start | bytes 49160 | tf_op jit(solution)/shard_map/ppermute | solution.py:404
  16.4 5.5 %collective-permute-start.7 = (f32[2,16,128]{2,1,0:T(8,128)S(1)}, f32[2,16,128]{2,1,0:T(8,128)S(1)}, u32[]{:S(2)}, u32[]{:S(2)}) collective-permute-start(f32[2,16,128]{2,1,0:T(8,128)S(1)} %collective-permute-done.6.refs_2_), channel_id=1, source_target_pairs={{0,1},{1,0},{2,3},{3,2},{4,5},{5,4},{6,7},{7,6},{8,9},{9,8},{10,11... | collective-permute-start | bytes 49160 | tf_op jit(solution)/shard_map/ppermute | solution.py:404
  17.4 4.5 %collective-permute-start.4 = (f32[16,128]{1,0:T(8,128)S(1)}, f32[16,128]{1,0:T(8,128)S(1)}, u32[]{:S(2)}, u32[]{:S(2)}) collective-permute-start(f32[16,128]{1,0:T(8,128)S(1)} %get-tuple-element.15), channel_id=1, source_target_pairs={{0,4},{1,5},{2,6},{3,7},{4,0},{5,1},{6,2},{7,3},{8,12},{9,13},{10,... | collective-permute-start | bytes 24584 | tf_op jit(solution)/shard_map/ppermute | solution.py:404
  22.7 1.2 %collective-permute-start.8 = (f32[16,128]{1,0:T(8,128)S(1)}, f32[16,128]{1,0:T(8,128)S(1)}, u32[]{:S(2)}, u32[]{:S(2)}) collective-permute-start(f32[16,128]{1,0:T(8,128)S(1)} %get-tuple-element.18.own_ref), channel_id=1, source_target_pairs={{0,1},{1,0},{2,3},{3,2},{4,5},{5,4},{6,7},{7,6},{8,9},{9,8},{10,11... | collective-permute-start | bytes 24584 | tf_op jit(solution)/shard_map/ppermute | solution.py:404
  23.9 3.7 %collective-permute-start.10 = (f32[2,16,128]{2,1,0:T(8,128)S(1)}, f32[2,16,128]{2,1,0:T(8,128)S(1)}, u32[]{:S(2)}, u32[]{:S(2)}) collective-permute-start(f32[2,16,128]{2,1,0:T(8,128)S(1)} %shard_map.146.refs_0_), channel_id=1, source_target_pairs={{0,2},{1,7},{2,0},{3,5},{4,6},{5,3},{6,4},{7,1},{8,10},{9,15},{10,... | collective-permute-start | bytes 49160 | tf_op jit(solution)/shard_map/ppermute | solution.py:404
  24.3 4.7 %collective-permute-start.9 = (f32[2,16,128]{2,1,0:T(8,128)S(1)}, f32[2,16,128]{2,1,0:T(8,128)S(1)}, u32[]{:S(2)}, u32[]{:S(2)}) collective-permute-start(f32[2,16,128]{2,1,0:T(8,128)S(1)} %shard_map.146.refs_0_), channel_id=1, source_target_pairs={{0,4},{1,5},{2,6},{3,7},{4,0},{5,1},{6,2},{7,3},{8,12},{9,13},{10,... | collective-permute-start | bytes 49160 | tf_op jit(solution)/shard_map/ppermute | solution.py:404
  27.7 1.7 %collective-permute-start.11 = (f32[2,16,128]{2,1,0:T(8,128)S(1)}, f32[2,16,128]{2,1,0:T(8,128)S(1)}, u32[]{:S(2)}, u32[]{:S(2)}) collective-permute-start(f32[2,16,128]{2,1,0:T(8,128)S(1)} %collective-permute-done.10.refs_2_), channel_id=1, source_target_pairs={{0,1},{1,0},{2,3},{3,2},{4,5},{5,4},{6,7},{7,6},{8,9},{9,8},{10,11... | collective-permute-start | bytes 49160 | tf_op jit(solution)/shard_map/ppermute | solution.py:404
  29.7 1.6 %collective-permute-start.12 = (bf16[8,512]{1,0:T(8,128)(2,1)S(1)}, bf16[8,512]{1,0:T(8,128)(2,1)S(1)}, u32[]{:S(2)}, u32[]{:S(2)}) collective-permute-start(bf16[8,512]{1,0:T(8,128)(2,1)S(1)} %shard_map.147.own_ref.residual_ref), channel_id=1, source_target_pairs={{0,1},{1,0},{2,3},{3,2},{4,5},{5,4},{6,7},{7,6},{8,9},{9,8},{10,11... | collective-permute-start | bytes 24584 | tf_op jit(solution)/shard_map/ppermute | solution.py:404
  31.3 3.7 %collective-permute-start.14 = (bf16[2,8,512]{2,1,0:T(8,128)(2,1)S(1)}, bf16[2,8,512]{2,1,0:T(8,128)(2,1)S(1)}, u32[]{:S(2)}, u32[]{:S(2)}) collective-permute-start(bf16[2,8,512]{2,1,0:T(8,128)(2,1)S(1)} %shard_map.148.near_ref.refs_0_), channel_id=1, source_target_pairs={{0,2},{1,7},{2,0},{3,5},{4,6},{5,3},{6,4},{7,1},{8,10},{9,15},{10,... | collective-permute-start | bytes 49160 | tf_op jit(solution)/shard_map/ppermute | solution.py:404
  32.2 5.1 %collective-permute-start.13 = (bf16[2,8,512]{2,1,0:T(8,128)(2,1)S(1)}, bf16[2,8,512]{2,1,0:T(8,128)(2,1)S(1)}, u32[]{:S(2)}, u32[]{:S(2)}) collective-permute-start(bf16[2,8,512]{2,1,0:T(8,128)(2,1)S(1)} %shard_map.148.near_ref.refs_0_), channel_id=1, source_target_pairs={{0,4},{1,5},{2,6},{3,7},{4,0},{5,1},{6,2},{7,3},{8,12},{9,13},{10,... | collective-permute-start | bytes 49160 | tf_op jit(solution)/shard_map/ppermute | solution.py:404
  35.1 2.2 %collective-permute-start.15 = (bf16[2,8,512]{2,1,0:T(8,128)(2,1)S(1)}, bf16[2,8,512]{2,1,0:T(8,128)(2,1)S(1)}, u32[]{:S(2)}, u32[]{:S(2)}) collective-permute-start(bf16[2,8,512]{2,1,0:T(8,128)(2,1)S(1)} %collective-permute-done.14.far_ref.refs_2_), channel_id=1, source_target_pairs={{0,1},{1,0},{2,3},{3,2},{4,5},{5,4},{6,7},{7,6},{8,9},{9,8},{10,11... | collective-permute-start | bytes 49160 | tf_op jit(solution)/shard_map/ppermute | solution.py:404
  39.6 1.3 %collective-permute-start.16 = (f32[4,8,512]{2,1,0:T(8,128)S(1)}, f32[4,8,512]{2,1,0:T(8,128)S(1)}, u32[]{:S(2)}, u32[]{:S(2)}) collective-permute-start(f32[4,8,512]{2,1,0:T(8,128)S(1)} %get-tuple-element.20), channel_id=1, source_target_pairs={{0,1},{1,0},{2,3},{3,2},{4,5},{5,4},{6,7},{7,6},{8,9},{9,8},{10,11... | collective-permute-start | bytes 196616 | tf_op jit(solution)/shard_map/ppermute | solution.py:404
  41.0 3.8 %collective-permute-start.18 = (bf16[2,8,512]{2,1,0:T(8,128)(2,1)S(1)}, bf16[2,8,512]{2,1,0:T(8,128)(2,1)S(1)}, u32[]{:S(2)}, u32[]{:S(2)}) collective-permute-start(bf16[2,8,512]{2,1,0:T(8,128)(2,1)S(1)} %get-tuple-element.23), channel_id=1, source_target_pairs={{0,2},{1,7},{2,0},{3,5},{4,6},{5,3},{6,4},{7,1},{8,10},{9,15},{10,... | collective-permute-start | bytes 49160 | tf_op jit(solution)/shard_map/ppermute | solution.py:404
  41.7 5.5 %collective-permute-start.17 = (bf16[8,512]{1,0:T(8,128)(2,1)S(1)}, bf16[8,512]{1,0:T(8,128)(2,1)S(1)}, u32[]{:S(2)}, u32[]{:S(2)}) collective-permute-start(bf16[8,512]{1,0:T(8,128)(2,1)S(1)} %get-tuple-element.22), channel_id=1, source_target_pairs={{0,4},{1,5},{2,6},{3,7},{4,0},{5,1},{6,2},{7,3},{8,12},{9,13},{10,... | collective-permute-start | bytes 24584 | tf_op jit(solution)/shard_map/ppermute | solution.py:404
  44.8 2.4 %collective-permute-start.19 = (bf16[2,8,512]{2,1,0:T(8,128)(2,1)S(1)}, bf16[2,8,512]{2,1,0:T(8,128)(2,1)S(1)}, u32[]{:S(2)}, u32[]{:S(2)}) collective-permute-start(bf16[2,8,512]{2,1,0:T(8,128)(2,1)S(1)} %collective-permute-done.18.far_ref), channel_id=1, source_target_pairs={{0,1},{1,0},{2,3},{3,2},{4,5},{5,4},{6,7},{7,6},{8,9},{9,8},{10,11... | collective-permute-start | bytes 49160 | tf_op jit(solution)/shard_map/ppermute | solution.py:404
  (16 other events, 227.9 us)

commit v5 on v4

--- a/solution.py
+++ b/solution.py
@@ -138,8 +138,20 @@
     return jnp.concatenate([pair_ref[0], pair_ref[1]], axis=1).astype(jnp.float32)
 
 
-def scaled_pair(rows, gain_ref, columns):
-    return (rows * gain_ref[:, columns]).astype(jnp.bfloat16)
+def split_pair(pair_ref, gain_ref, columns):
+    scaled = flat_pair(pair_ref) * gain_ref[:, columns]
+    high = scaled.astype(jnp.bfloat16)
+    low = (scaled - high.astype(jnp.float32)).astype(jnp.bfloat16)
+    return jnp.concatenate([high, low], axis=0)
+
+
+def normed_pair(pair_ref, gain_ref, columns, inv_root):
+    return (flat_pair(pair_ref) * inv_root * gain_ref[:, columns]).astype(jnp.bfloat16)
+
+
+def joined(product):
+    half = product.shape[0] // 2
+    return product[:half] + product[half:]
 
 
 def head_weight(weight_refs, head, columns):
@@ -148,32 +160,60 @@
     )
 
 
-def add_projections(steps, gain_ref, weight_refs, start, total_ref):
+def project_blocks(blocks, weight_refs, finish):
     heads, chan, _ = weight_refs[0].shape
     lanes = 8 * chan
-    blocks = []
-    for step, pair_ref in steps:
-        rows = flat_pair(pair_ref)
-        columns = pair_columns(step, rows.shape[1])
-        blocks.append((scaled_pair(rows, gain_ref, columns), columns))
     for head in range(0, heads, 2):
-        place = slice(head // 2 * lanes, (head // 2 + 1) * lanes)
-        total = start(place)
-        for scaled, columns in blocks:
+        total = None
+        for rows, columns in blocks:
             part = lax.dot_general(
-                scaled,
+                rows,
                 head_weight(weight_refs, head, columns),
                 (((1,), (1,)), ((), ())),
                 preferred_element_type=jnp.float32,
             )
             total = part if total is None else total + part
+        finish(slice(head // 2 * lanes, (head // 2 + 1) * lanes), total)
+
+
+def near_step():
+    return 0
+
+
+def other_step():
+    return far_step(lax.axis_index("tp"))
+
+
+def late_steps(pair_refs):
+    return ((2, pair_refs[1]), (far_step(1 - lax.axis_index("tp")), pair_refs[3]))
+
+
+def split_blocks(steps, gain_ref):
+    blocks = []
+    for step, pair_ref in steps:
+        columns = pair_columns(step, 2 * pair_ref.shape[2])
+        blocks.append((split_pair(pair_ref, gain_ref, columns), columns))
+    return blocks
+
+
+def normed_blocks(steps, gain_ref, inv_root):
+    blocks = []
+    for step, pair_ref in steps:
+        columns = pair_columns(step, 2 * pair_ref.shape[2])
+        blocks.append((normed_pair(pair_ref, gain_ref, columns, inv_root), columns))
+    return blocks
+
+
+def early_project_kernel(step, pair_ref, gain_ref, *refs):
+    weight_refs, before_refs, total_ref = refs[:4], refs[4:-1], refs[-1]
+
+    def finish(place, total):
+        total = joined(total)
+        for ref in before_refs:
+            total = total + ref[:, place]
         total_ref[:, place] = total
 
-
-def early_project_kernel(near_ref, far_ref, gain_ref, *refs):
-    weight_refs, total_ref = refs[:4], refs[4]
-    steps = ((0, near_ref), (far_step(lax.axis_index("tp")), far_ref))
-    add_projections(steps, gain_ref, weight_refs, lambda place: None, total_ref)
+    project_blocks(split_blocks(((step(), pair_ref),), gain_ref), weight_refs, finish)
 
 
 def inverse_root(pair_refs):
@@ -190,12 +230,15 @@
     weight_refs = refs[chips + 2 : chips + 6]
     near_ref, mid_ref, far_ref, swap_ref, total_ref, made_ref = refs[chips + 6 :]
     core = lax.axis_index("tp")
-    steps = ((2, pair_refs[1]), (far_step(1 - core), pair_refs[3]))
-    add_projections(steps, gain_ref, weight_refs, lambda place: early_ref[:, place], total_ref)
+    inv_root = inverse_root(pair_refs)
+
+    def finish(place, total):
+        total_ref[:, place] = early_ref[:, place] * inv_root + total
+
+    project_blocks(normed_blocks(late_steps(pair_refs), gain_ref, inv_root), weight_refs, finish)
     heads, chan, _ = weight_refs[0].shape
     rows, lanes = total_ref.shape[0], 4 * chan
-    product = total_ref[...] * inverse_root(pair_refs)
-    product = product.astype(jnp.bfloat16).astype(jnp.float32)
+    product = total_ref[...].astype(jnp.bfloat16).astype(jnp.float32)
     for head in range(heads):
         made_ref[pl.ds(head, rows, stride=heads), :] = product[:, head * lanes : (head + 1) * lanes]
     chip = lax.axis_index("kv")
@@ -247,25 +290,22 @@
     value_ref[...] = value_rows
 
 
-def state_kernel(key_ref, value_ref, state_ref, next_ref, made_ref, done_ref):
+def state_kernel(key_ref, value_ref, state_ref, next_ref):
     own_rows, heads, _, _ = state_ref.shape
     key_cols = jnp.transpose(key_ref[...])
-    copies = []
     for row in range(own_rows):
         for head in range(heads):
             pair = row * heads + head
             old = state_ref[row, head]
-            made_ref[pair] = old + key_cols[:, pair : pair + 1] * (
+            next_ref[row, head] = old + key_cols[:, pair : pair + 1] * (
                 value_ref[pair : pair + 1, :] - old
             )
-            copies.append(
-                pltpu.make_async_copy(made_ref.at[pair], next_ref.at[row, head], done_ref.at[pair])
-            )
-            if pair > 0:
-                copies[pair - 1].start()
-    copies[-1].start()
-    for copy in copies:
-        copy.wait()
+
+
+def copy_out_kernel(made_ref, next_ref, done_ref):
+    copy = pltpu.make_async_copy(made_ref, next_ref, done_ref)
+    copy.start()
+    copy.wait()
 
 
 def stage_kernel(block_ref, staged_ref):
@@ -319,33 +359,31 @@
         )
 
 
-def up_part(steps, gain_ref, up_ref, total):
-    for step, pair_ref in steps:
-        rows = flat_pair(pair_ref)
-        columns = pair_columns(step, rows.shape[1])
-        part = jnp.dot(
-            scaled_pair(rows, gain_ref, columns),
-            up_ref[columns, :],
-            preferred_element_type=jnp.float32,
-        )
+def up_blocks(blocks, up_ref):
+    total = None
+    for rows, columns in blocks:
+        part = jnp.dot(rows, up_ref[columns, :], preferred_element_type=jnp.float32)
         total = part if total is None else total + part
     return total
 
 
-def early_up_kernel(near_ref, far_ref, gain_ref, up_ref, early_ref):
-    steps = ((0, near_ref), (far_step(lax.axis_index("tp")), far_ref))
-    early_ref[...] = up_part(steps, gain_ref, up_ref, None)
+def early_up_kernel(step, pair_ref, gain_ref, up_ref, down_ref, *refs):
+    del down_ref
+    total = joined(up_blocks(split_blocks(((step(), pair_ref),), gain_ref), up_ref))
+    for ref in refs[:-1]:
+        total = total + ref[...]
+    refs[-1][...] = total
 
 
 def mixer_kernel(chips, *refs):
     pair_refs, (early_ref, gain_ref, up_ref, down_ref) = refs[:chips], refs[chips : chips + 4]
     hidden_ref, partial_ref = refs[chips + 4 :]
-    core = lax.axis_index("tp")
-    steps = ((2, pair_refs[1]), (far_step(1 - core), pair_refs[3]))
-    hidden = up_part(steps, gain_ref, up_ref, early_ref[...]) * inverse_root(pair_refs)
+    inv_root = inverse_root(pair_refs)
+    late = up_blocks(normed_blocks(late_steps(pair_refs), gain_ref, inv_root), up_ref)
+    hidden = early_ref[...] * inv_root + late
     hidden = jnp.square(jnp.maximum(hidden, 0.0)).astype(jnp.bfloat16)
     hidden_ref[...] = hidden
-    down_part(hidden, down_ref, 1 - core, partial_ref)
+    down_part(hidden, down_ref, 1 - lax.axis_index("tp"), partial_ref)
 
 
 def own_part_kernel(hidden_ref, down_ref, partial_ref):
@@ -418,16 +456,25 @@
         pair = paired(staged, other_core(block), cost)
         return (pair,) + crossed(pair, pair)
 
+    def early_parts(kernel, got, operands, columns, cost):
+        total = ()
+        for place, step in ((0, near_step), (2, other_step)):
+            part = call(
+                functools.partial(kernel, step),
+                shape((rows, columns), f32),
+                (got[place], *operands, *total),
+                cost,
+                14 * MIB,
+            )
+            total = (part,)
+        return total[0]
+
     staged = call(stage_kernel, shape(tokens.shape, bf16), (tokens,), COST[4], MIB)
     pairs_of_rows = gather_pairs(tokens, staged, COST[0])
     mix_row = mix_gain.reshape(1, -1)
     projections = (query_weight, forget_weight, value_weight, gate_weight)
-    early = call(
-        early_project_kernel,
-        shape((rows, 4 * heads * chan), f32),
-        (pairs_of_rows[0], pairs_of_rows[2], mix_row, *projections),
-        COST[9],
-        14 * MIB,
+    early = early_parts(
+        early_project_kernel, pairs_of_rows, (mix_row, *projections), 4 * heads * chan, COST[9]
     )
     near, mid, far, swap = call(
         functools.partial(project_kernel, kv),
@@ -446,15 +493,22 @@
         14 * MIB,
         [pltpu.VMEM((kv, pairs, 4 * chan), f32)],
     )
+    next_state = call(
+        state_kernel,
+        pltpu.VMEM(recurrent_state.shape, f32),
+        (key_rows, value_rows, recurrent_state),
+        COST[3],
+        4 * MIB,
+    )
     next_state = pl.pallas_call(
-        state_kernel,
+        copy_out_kernel,
         out_shape=shape(recurrent_state.shape, f32),
-        in_specs=[whole] * 3,
+        in_specs=[whole],
         out_specs=pl.BlockSpec(memory_space=pl.ANY),
-        scratch_shapes=[pltpu.VMEM((pairs, keys, values), f32), pltpu.SemaphoreType.DMA((pairs,))],
-        compiler_params=pltpu.CompilerParams(vmem_limit_bytes=6 * MIB),
+        scratch_shapes=[pltpu.SemaphoreType.DMA],
+        compiler_params=pltpu.CompilerParams(vmem_limit_bytes=MIB),
         cost_estimate=pl.CostEstimate(flops=COST[3], bytes_accessed=0, transcendentals=0),
-    )(key_rows, value_rows, recurrent_state)
+    )(next_state)
     residual = call(
         functools.partial(out_kernel, kv, heads),
         shape((rows, width), bf16),
@@ -465,12 +519,8 @@
     )
     pairs_of_rows = gather_pairs(residual, residual, COST[4])
     mlp_row = mlp_gain.reshape(1, -1)
-    early = call(
-        early_up_kernel,
-        shape((rows, up_weight.shape[1]), f32),
-        (pairs_of_rows[0], pairs_of_rows[2], mlp_row, up_weight),
-        COST[10],
-        14 * MIB,
+    early = early_parts(
+        early_up_kernel, pairs_of_rows, (mlp_row, up_weight, down_weight), up_weight.shape[1], COST[10]
     )
     hidden, mate_part = call(
         functools.partial(mixer_kernel, kv),

time: 48 us -> 47.7 us (level)
  starting transfers between devices: 22.7 us -> 21.2 us
  waiting for transfers between devices: 13.2 us -> 13.9 us
    ppermute x20, starting transfers between devices: 22.7 us -> 21.2 us  [permute(): return lax.ppermute(block, group, hops)]
    pallas_call x14 -> x17, Pallas kernels: 8.85 us -> 9.67 us  [call(): pl.pallas_call(body, out_shape=outs, in_specs=[whole] * len(arrays), out_...]
    ppermute x20, waiting for transfers between devices: 13.2 us -> 13.9 us  [permute(): return lax.ppermute(block, group, hops)]
  transfers between devices with their start and end apart: 20 -> 20, of which waited for: 12 -> 12; matrix products, arithmetic and copies ran while one was open for 0% -> 0% of each run, Pallas kernels for 10% -> 11%
where the time goes in v5:
time: 47.7 us; the launch traced here: 47.4 us
  starting transfers between devices  21.2 us (44%)
  waiting for transfers between devices  13.9 us (29%)
  Pallas kernels  10.6 us (22%)
  between operations  0.93 us (2%)
  local copies, waits for them, and re-layouts  0.81 us (2%)
    ppermute x20, starting transfers between devices, permute(): return lax.ppermute(block, group, hops)  21.2 us
    ppermute x20, waiting for transfers between devices, permute(): return lax.ppermute(block, group, hops)  13.9 us
    pallas_call x17, Pallas kernels, call(): pl.pallas_call(body, out_shape=outs, in_specs=[whole] * len(arrays), out_...  9.67 us
    pallas_call x1, Pallas kernels, tiled_local(): pl.pallas_call(copy_out_kernel, out_shape=shape(recurrent_state.shape, f3...  0.98 us
  transfers between devices with their start and end apart: 20, of which 12 were waited for; matrix products, arithmetic and copies ran while one was open for 0% of the time, Pallas kernels for 11%

profile of v5, /device:TPU:0, one launch (start us, length us, event | category | flops | bytes accessed | tf_op | source)
XLA Modules:
  0.0 47.4 jit_solution(6870595468623483206)
XLA Ops:
  2.2 2.9 %collective-permute-start.2 = (bf16[2,8,512]{2,1,0:T(8,128)(2,1)S(1)}, bf16[2,8,512]{2,1,0:T(8,128)(2,1)S(1)}, u32[]{:S(2)}, u32[]{:S(2)}) collective-permute-start(bf16[2,8,512]{2,1,0:T(8,128)(2,1)S(1)} %shard_map.141.pair_ref.refs_0_), channel_id=1, source_target_pairs={{0,2},{1,7},{2,0},{3,5},{4,6},{5,3},{6,4},{7,1},{8,10},{9,15},{10,... | collective-permute-start | bytes 49160 | tf_op jit(solution)/shard_map/ppermute | solution.py:442
  5.1 2.6 %collective-permute-start.1 = (bf16[2,8,512]{2,1,0:T(8,128)(2,1)S(1)}, bf16[2,8,512]{2,1,0:T(8,128)(2,1)S(1)}, u32[]{:S(2)}, u32[]{:S(2)}) collective-permute-start(bf16[2,8,512]{2,1,0:T(8,128)(2,1)S(1)} %shard_map.141.pair_ref.refs_0_), channel_id=1, source_target_pairs={{0,4},{1,5},{2,6},{3,7},{4,0},{5,1},{6,2},{7,3},{8,12},{9,13},{10,... | collective-permute-start | bytes 49160 | tf_op jit(solution)/shard_map/ppermute | solution.py:442
  9.9 1.2 %shard_map.144 = (f32[16,128]{1,0:T(8,128)S(1)}, f32[16,128]{1,0:T(8,128)S(1)}, f32[16,128]{1,0:T(8,128)S(1)}, f32[16,128]{1,0:T(8,128)S(1)}) custom-call(bf16[2,8,512]{2,1,0:T(8,128)(2,1)S(1)} %shard_map.141.pair_ref.refs_0_, bf16[2,8,512]{2,1,0:T(8,128)(2,1)S(1)} %collective-permute-done.1.refs_1_, ...), custom_call_target="tpu_custom_call" | custom-call | flops 99999997952 | tf_op jit(solution)/shard_map/pallas_call | solution.py:102
  11.9 0.8 %collective-permute-done.5.mate_ref = f32[16,128]{1,0:T(8,128)S(1)} collective-permute-done((f32[16,128]{1,0:T(8,128)S(1)}, f32[16,128]{1,0:T(8,128)S(1)}, u32[]{:S(2)}, u32[]{:S(2)}) %collective-permute-start.5) | collective-permute-done | bytes 8224 | tf_op jit(solution)/shard_map/ppermute | solution.py:442
  12.7 3.7 %collective-permute-done.6.refs_2_ = f32[2,16,128]{2,1,0:T(8,128)S(1)} collective-permute-done((f32[2,16,128]{2,1,0:T(8,128)S(1)}, f32[2,16,128]{2,1,0:T(8,128)S(1)}, u32[]{:S(2)}, u32[]{:S(2)}) %collective-permute-start.6) | collective-permute-done | bytes 16416 | tf_op jit(solution)/shard_map/ppermute | solution.py:442
  16.4 1.0 %collective-permute-start.7 = (f32[2,16,128]{2,1,0:T(8,128)S(1)}, f32[2,16,128]{2,1,0:T(8,128)S(1)}, u32[]{:S(2)}, u32[]{:S(2)}) collective-permute-start(f32[2,16,128]{2,1,0:T(8,128)S(1)} %collective-permute-done.6.refs_2_), channel_id=1, source_target_pairs={{0,1},{1,0},{2,3},{3,2},{4,5},{5,4},{6,7},{7,6},{8,9},{9,8},{10,11... | collective-permute-start | bytes 49160 | tf_op jit(solution)/shard_map/ppermute | solution.py:442
  17.4 1.2 %collective-permute-start.4 = (f32[16,128]{1,0:T(8,128)S(1)}, f32[16,128]{1,0:T(8,128)S(1)}, u32[]{:S(2)}, u32[]{:S(2)}) collective-permute-start(f32[16,128]{1,0:T(8,128)S(1)} %get-tuple-element.15), channel_id=1, source_target_pairs={{0,4},{1,5},{2,6},{3,7},{4,0},{5,1},{6,2},{7,3},{8,12},{9,13},{10,... | collective-permute-start | bytes 24584 | tf_op jit(solution)/shard_map/ppermute | solution.py:442
  18.6 3.4 %collective-permute-done.4.refs_1_ = f32[16,128]{1,0:T(8,128)S(1)} collective-permute-done((f32[16,128]{1,0:T(8,128)S(1)}, f32[16,128]{1,0:T(8,128)S(1)}, u32[]{:S(2)}, u32[]{:S(2)}) %collective-permute-start.4) | collective-permute-done | bytes 8224 | tf_op jit(solution)/shard_map/ppermute | solution.py:442
  22.0 0.7 %shard_map.146 = (f32[16,128]{1,0:T(8,128)S(1)}, f32[16,128]{1,0:T(8,128)S(1)}, f32[16,128]{1,0:T(8,128)S(1)}) custom-call(f32[16,128]{1,0:T(8,128)S(1)} %get-tuple-element.14.refs_0_, f32[16,128]{1,0:T(8,128)S(1)} %collective-permute-done.4.refs_1_, f32[2,16,128]{2,1,0:T(8,128)S(1)} %collective-permute-done.6.refs_2_, ...), custom_call_target="tpu_custom_call" | custom-call | flops 1000000000 | tf_op jit(solution)/shard_map/pallas_call | solution.py:102
  22.8 1.2 %collective-permute-done.8.mate_ref = f32[16,128]{1,0:T(8,128)S(1)} collective-permute-done((f32[16,128]{1,0:T(8,128)S(1)}, f32[16,128]{1,0:T(8,128)S(1)}, u32[]{:S(2)}, u32[]{:S(2)}) %collective-permute-start.8) | collective-permute-done | bytes 8224 | tf_op jit(solution)/shard_map/ppermute | solution.py:442
  24.0 2.9 %collective-permute-start.9 = (f32[2,16,128]{2,1,0:T(8,128)S(1)}, f32[2,16,128]{2,1,0:T(8,128)S(1)}, u32[]{:S(2)}, u32[]{:S(2)}) collective-permute-start(f32[2,16,128]{2,1,0:T(8,128)S(1)} %shard_map.147.refs_0_), channel_id=1, source_target_pairs={{0,4},{1,5},{2,6},{3,7},{4,0},{5,1},{6,2},{7,3},{8,12},{9,13},{10,... | collective-permute-start | bytes 49160 | tf_op jit(solution)/shard_map/ppermute | solution.py:442
  26.9 0.8 %collective-permute-done.10.refs_2_ = f32[2,16,128]{2,1,0:T(8,128)S(1)} collective-permute-done((f32[2,16,128]{2,1,0:T(8,128)S(1)}, f32[2,16,128]{2,1,0:T(8,128)S(1)}, u32[]{:S(2)}, u32[]{:S(2)}) %collective-permute-start.10) | collective-permute-done | bytes 16416 | tf_op jit(solution)/shard_map/ppermute | solution.py:442
  27.7 0.9 %collective-permute-start.11 = (f32[2,16,128]{2,1,0:T(8,128)S(1)}, f32[2,16,128]{2,1,0:T(8,128)S(1)}, u32[]{:S(2)}, u32[]{:S(2)}) collective-permute-start(f32[2,16,128]{2,1,0:T(8,128)S(1)} %collective-permute-done.10.refs_2_), channel_id=1, source_target_pairs={{0,1},{1,0},{2,3},{3,2},{4,5},{5,4},{6,7},{7,6},{8,9},{9,8},{10,11... | collective-permute-start | bytes 49160 | tf_op jit(solution)/shard_map/ppermute | solution.py:442
  28.6 0.8 %collective-permute-done.11.refs_3_ = f32[2,16,128]{2,1,0:T(8,128)S(1)} collective-permute-done((f32[2,16,128]{2,1,0:T(8,128)S(1)}, f32[2,16,128]{2,1,0:T(8,128)S(1)}, u32[]{:S(2)}, u32[]{:S(2)}) %collective-permute-start.11) | collective-permute-done | bytes 16416 | tf_op jit(solution)/shard_map/ppermute | solution.py:442
  30.3 0.8 %collective-permute-done.12.mate_ref = bf16[8,512]{1,0:T(8,128)(2,1)S(1)} collective-permute-done((bf16[8,512]{1,0:T(8,128)(2,1)S(1)}, bf16[8,512]{1,0:T(8,128)(2,1)S(1)}, u32[]{:S(2)}, u32[]{:S(2)}) %collective-permute-start.12) | collective-permute-done | bytes 8224 | tf_op jit(solution)/shard_map/ppermute | solution.py:442
  31.1 1.2 %collective-permute-start.14 = (bf16[2,8,512]{2,1,0:T(8,128)(2,1)S(1)}, bf16[2,8,512]{2,1,0:T(8,128)(2,1)S(1)}, u32[]{:S(2)}, u32[]{:S(2)}) collective-permute-start(bf16[2,8,512]{2,1,0:T(8,128)(2,1)S(1)} %shard_map.149.pair_ref.refs_0_), channel_id=1, source_target_pairs={{0,2},{1,7},{2,0},{3,5},{4,6},{5,3},{6,4},{7,1},{8,10},{9,15},{10,... | collective-permute-start | bytes 49160 | tf_op jit(solution)/shard_map/ppermute | solution.py:442
  32.3 1.6 %collective-permute-start.13 = (bf16[2,8,512]{2,1,0:T(8,128)(2,1)S(1)}, bf16[2,8,512]{2,1,0:T(8,128)(2,1)S(1)}, u32[]{:S(2)}, u32[]{:S(2)}) collective-permute-start(bf16[2,8,512]{2,1,0:T(8,128)(2,1)S(1)} %shard_map.149.pair_ref.refs_0_), channel_id=1, source_target_pairs={{0,4},{1,5},{2,6},{3,7},{4,0},{5,1},{6,2},{7,3},{8,12},{9,13},{10,... | collective-permute-start | bytes 49160 | tf_op jit(solution)/shard_map/ppermute | solution.py:442
  33.9 0.9 %collective-permute-done.14.pair_ref.refs_2_ = bf16[2,8,512]{2,1,0:T(8,128)(2,1)S(1)} collective-permute-done((bf16[2,8,512]{2,1,0:T(8,128)(2,1)S(1)}, bf16[2,8,512]{2,1,0:T(8,128)(2,1)S(1)}, u32[]{:S(2)}, u32[]{:S(2)}) %collective-permute-start.14) | collective-permute-done | bytes 16416 | tf_op jit(solution)/shard_map/ppermute | solution.py:442
  34.8 1.0 %collective-permute-start.15 = (bf16[2,8,512]{2,1,0:T(8,128)(2,1)S(1)}, bf16[2,8,512]{2,1,0:T(8,128)(2,1)S(1)}, u32[]{:S(2)}, u32[]{:S(2)}) collective-permute-start(bf16[2,8,512]{2,1,0:T(8,128)(2,1)S(1)} %collective-permute-done.14.pair_ref.refs_2_), channel_id=1, source_target_pairs={{0,1},{1,0},{2,3},{3,2},{4,5},{5,4},{6,7},{7,6},{8,9},{9,8},{10,11... | collective-permute-start | bytes 49160 | tf_op jit(solution)/shard_map/ppermute | solution.py:442
  37.3 2.4 %shard_map.152 = (bf16[8,2048]{1,0:T(8,128)(2,1)S(1)}, f32[4,8,512]{2,1,0:T(8,128)S(1)}) custom-call(bf16[2,8,512]{2,1,0:T(8,128)(2,1)S(1)} %shard_map.149.pair_ref.refs_0_, bf16[2,8,512]{2,1,0:T(8,128)(2,1)S(1)} %collective-permute-done.13.refs_1_, bf16[2,8,512]{2,1,0:T(8,128)(2,1)S(1)} %collective-permute-done.14.pair_ref.refs_2_, ...), custom_call_target="tpu_custom_call" | custom-call | flops 1000000 | tf_op jit(solution)/shard_map/pallas_call | solution.py:102
  39.6 1.2 %shard_map.153.own_ref = f32[4,8,512]{2,1,0:T(8,128)S(1)} custom-call(bf16[8,2048]{1,0:T(8,128)(2,1)S(1)} %get-tuple-element.19.hidden_ref, bf16[2048,4096]{1,0:T(8,128)(2,1)S(1)} %bitcast.3), custom_call_target="tpu_custom_call" | custom-call | flops 1000000000 | tf_op jit(solution)/shard_map/pallas_call | solution.py:102
  42.1 2.2 %collective-permute-start.17 = (bf16[8,512]{1,0:T(8,128)(2,1)S(1)}, bf16[8,512]{1,0:T(8,128)(2,1)S(1)}, u32[]{:S(2)}, u32[]{:S(2)}) collective-permute-start(bf16[8,512]{1,0:T(8,128)(2,1)S(1)} %get-tuple-element.22), channel_id=1, source_target_pairs={{0,4},{1,5},{2,6},{3,7},{4,0},{5,1},{6,2},{7,3},{8,12},{9,13},{10,... | collective-permute-start | bytes 24584 | tf_op jit(solution)/shard_map/ppermute | solution.py:442
  44.7 1.1 %collective-permute-start.19 = (bf16[2,8,512]{2,1,0:T(8,128)(2,1)S(1)}, bf16[2,8,512]{2,1,0:T(8,128)(2,1)S(1)}, u32[]{:S(2)}, u32[]{:S(2)}) collective-permute-start(bf16[2,8,512]{2,1,0:T(8,128)(2,1)S(1)} %collective-permute-done.18.far_ref), channel_id=1, source_target_pairs={{0,1},{1,0},{2,3},{3,2},{4,5},{5,4},{6,7},{7,6},{8,9},{9,8},{10,11... | collective-permute-start | bytes 49160 | tf_op jit(solution)/shard_map/ppermute | solution.py:442
  45.8 1.0 %shard_map.157 = f32[2,8,128,128]{3,2,1,0:T(8,128)} custom-call(f32[2,8,128,128]{3,2,1,0:T(8,128)S(1)} %shard_map.156.made_ref), custom_call_target="tpu_custom_call" | custom-call | flops 1000000000 | tf_op jit(solution)/shard_map/pallas_call | solution.py:503
  (76 shorter events, 8.9 us)
Async XLA Ops:
  0.6 1.6 %collective-permute-start = (bf16[8,512]{1,0:T(8,128)(2,1)}, bf16[8,512]{1,0:T(8,128)(2,1)S(1)}, u32[]{:S(2)}, u32[]{:S(2)}) collective-permute-start(bf16[8,512]{1,0:T(8,128)(2,1)} %refs_4_.3), channel_id=1, source_target_pairs={{0,1},{1,0},{2,3},{3,2},{4,5},{5,4},{6,7},{7,6},{8,9},{9,8},{10,11... | collective-permute-start | bytes 24584 | tf_op jit(solution)/shard_map/ppermute | solution.py:442
  2.2 6.2 %collective-permute-start.2 = (bf16[2,8,512]{2,1,0:T(8,128)(2,1)S(1)}, bf16[2,8,512]{2,1,0:T(8,128)(2,1)S(1)}, u32[]{:S(2)}, u32[]{:S(2)}) collective-permute-start(bf16[2,8,512]{2,1,0:T(8,128)(2,1)S(1)} %shard_map.141.pair_ref.refs_0_), channel_id=1, source_target_pairs={{0,2},{1,7},{2,0},{3,5},{4,6},{5,3},{6,4},{7,1},{8,10},{9,15},{10,... | collective-permute-start | bytes 49160 | tf_op jit(solution)/shard_map/ppermute | solution.py:442
  5.1 4.7 %collective-permute-start.1 = (bf16[2,8,512]{2,1,0:T(8,128)(2,1)S(1)}, bf16[2,8,512]{2,1,0:T(8,128)(2,1)S(1)}, u32[]{:S(2)}, u32[]{:S(2)}) collective-permute-start(bf16[2,8,512]{2,1,0:T(8,128)(2,1)S(1)} %shard_map.141.pair_ref.refs_0_), channel_id=1, source_target_pairs={{0,4},{1,5},{2,6},{3,7},{4,0},{5,1},{6,2},{7,3},{8,12},{9,13},{10,... | collective-permute-start | bytes 49160 | tf_op jit(solution)/shard_map/ppermute | solution.py:442
  8.4 1.5 %collective-permute-start.3 = (bf16[2,8,512]{2,1,0:T(8,128)(2,1)S(1)}, bf16[2,8,512]{2,1,0:T(8,128)(2,1)S(1)}, u32[]{:S(2)}, u32[]{:S(2)}) collective-permute-start(bf16[2,8,512]{2,1,0:T(8,128)(2,1)S(1)} %collective-permute-done.2.pair_ref.refs_2_), channel_id=1, source_target_pairs={{0,1},{1,0},{2,3},{3,2},{4,5},{5,4},{6,7},{7,6},{8,9},{9,8},{10,11... | collective-permute-start | bytes 49160 | tf_op jit(solution)/shard_map/ppermute | solution.py:442
  8.4 27.4 %slice-start = ((s8[16777216]{0:T(1024)(128)(4,1)}), s8[4194304]{0:T(1024)(128)(4,1)S(1)}, s32[]{:S(2)}) async-start(s8[16777216]{0:T(1024)(128)(4,1)} %bitcast.2), calls=%async_computation | async-start | bytes 8388608
  8.4 27.4 %slice-start.4 = ((s8[16777216]{0:T(1024)(128)(4,1)}), s8[4194304]{0:T(1024)(128)(4,1)S(1)}, s32[]{:S(2)}) async-start(s8[16777216]{0:T(1024)(128)(4,1)} %bitcast.4), calls=%async_computation.4 | async-start | bytes 8388608
  9.2 26.7 %slice-start.1 = ((s8[16777216]{0:T(1024)(128)(4,1)}), s8[4194304]{0:T(1024)(128)(4,1)S(1)}, s32[]{:S(2)}) async-start(s8[16777216]{0:T(1024)(128)(4,1)} %bitcast.2), calls=%async_computation.1 | async-start | bytes 8388608
  9.2 26.7 %slice-start.2 = ((s8[16777216]{0:T(1024)(128)(4,1)}), s8[4194304]{0:T(1024)(128)(4,1)S(1)}, s32[]{:S(2)}) async-start(s8[16777216]{0:T(1024)(128)(4,1)} %bitcast.2), calls=%async_computation.2 | async-start | bytes 8388608
  11.2 1.6 %collective-permute-start.5 = (f32[16,128]{1,0:T(8,128)S(1)}, f32[16,128]{1,0:T(8,128)S(1)}, u32[]{:S(2)}, u32[]{:S(2)}) collective-permute-start(f32[16,128]{1,0:T(8,128)S(1)} %get-tuple-element.17), channel_id=1, source_target_pairs={{0,1},{1,0},{2,3},{3,2},{4,5},{5,4},{6,7},{7,6},{8,9},{9,8},{10,11... | collective-permute-start | bytes 24584 | tf_op jit(solution)/shard_map/ppermute | solution.py:442
  12.7 3.7 %collective-permute-start.6 = (f32[2,16,128]{2,1,0:T(8,128)S(1)}, f32[2,16,128]{2,1,0:T(8,128)S(1)}, u32[]{:S(2)}, u32[]{:S(2)}) collective-permute-start(f32[2,16,128]{2,1,0:T(8,128)S(1)} %shard_map.145), channel_id=1, source_target_pairs={{0,2},{1,7},{2,0},{3,5},{4,6},{5,3},{6,4},{7,1},{8,10},{9,15},{10,... | collective-permute-start | bytes 49160 | tf_op jit(solution)/shard_map/ppermute | solution.py:442
  16.4 5.5 %collective-permute-start.7 = (f32[2,16,128]{2,1,0:T(8,128)S(1)}, f32[2,16,128]{2,1,0:T(8,128)S(1)}, u32[]{:S(2)}, u32[]{:S(2)}) collective-permute-start(f32[2,16,128]{2,1,0:T(8,128)S(1)} %collective-permute-done.6.refs_2_), channel_id=1, source_target_pairs={{0,1},{1,0},{2,3},{3,2},{4,5},{5,4},{6,7},{7,6},{8,9},{9,8},{10,11... | collective-permute-start | bytes 49160 | tf_op jit(solution)/shard_map/ppermute | solution.py:442
  17.4 4.5 %collective-permute-start.4 = (f32[16,128]{1,0:T(8,128)S(1)}, f32[16,128]{1,0:T(8,128)S(1)}, u32[]{:S(2)}, u32[]{:S(2)}) collective-permute-start(f32[16,128]{1,0:T(8,128)S(1)} %get-tuple-element.15), channel_id=1, source_target_pairs={{0,4},{1,5},{2,6},{3,7},{4,0},{5,1},{6,2},{7,3},{8,12},{9,13},{10,... | collective-permute-start | bytes 24584 | tf_op jit(solution)/shard_map/ppermute | solution.py:442
  22.8 1.2 %collective-permute-start.8 = (f32[16,128]{1,0:T(8,128)S(1)}, f32[16,128]{1,0:T(8,128)S(1)}, u32[]{:S(2)}, u32[]{:S(2)}) collective-permute-start(f32[16,128]{1,0:T(8,128)S(1)} %get-tuple-element.18.own_ref), channel_id=1, source_target_pairs={{0,1},{1,0},{2,3},{3,2},{4,5},{5,4},{6,7},{7,6},{8,9},{9,8},{10,11... | collective-permute-start | bytes 24584 | tf_op jit(solution)/shard_map/ppermute | solution.py:442
  24.0 3.7 %collective-permute-start.10 = (f32[2,16,128]{2,1,0:T(8,128)S(1)}, f32[2,16,128]{2,1,0:T(8,128)S(1)}, u32[]{:S(2)}, u32[]{:S(2)}) collective-permute-start(f32[2,16,128]{2,1,0:T(8,128)S(1)} %shard_map.147.refs_0_), channel_id=1, source_target_pairs={{0,2},{1,7},{2,0},{3,5},{4,6},{5,3},{6,4},{7,1},{8,10},{9,15},{10,... | collective-permute-start | bytes 49160 | tf_op jit(solution)/shard_map/ppermute | solution.py:442
  24.0 4.6 %collective-permute-start.9 = (f32[2,16,128]{2,1,0:T(8,128)S(1)}, f32[2,16,128]{2,1,0:T(8,128)S(1)}, u32[]{:S(2)}, u32[]{:S(2)}) collective-permute-start(f32[2,16,128]{2,1,0:T(8,128)S(1)} %shard_map.147.refs_0_), channel_id=1, source_target_pairs={{0,4},{1,5},{2,6},{3,7},{4,0},{5,1},{6,2},{7,3},{8,12},{9,13},{10,... | collective-permute-start | bytes 49160 | tf_op jit(solution)/shard_map/ppermute | solution.py:442
  27.7 1.7 %collective-permute-start.11 = (f32[2,16,128]{2,1,0:T(8,128)S(1)}, f32[2,16,128]{2,1,0:T(8,128)S(1)}, u32[]{:S(2)}, u32[]{:S(2)}) collective-permute-start(f32[2,16,128]{2,1,0:T(8,128)S(1)} %collective-permute-done.10.refs_2_), channel_id=1, source_target_pairs={{0,1},{1,0},{2,3},{3,2},{4,5},{5,4},{6,7},{7,6},{8,9},{9,8},{10,11... | collective-permute-start | bytes 49160 | tf_op jit(solution)/shard_map/ppermute | solution.py:442
  29.8 1.2 %collective-permute-start.12 = (bf16[8,512]{1,0:T(8,128)(2,1)S(1)}, bf16[8,512]{1,0:T(8,128)(2,1)S(1)}, u32[]{:S(2)}, u32[]{:S(2)}) collective-permute-start(bf16[8,512]{1,0:T(8,128)(2,1)S(1)} %shard_map.148.own_ref.residual_ref), channel_id=1, source_target_pairs={{0,1},{1,0},{2,3},{3,2},{4,5},{5,4},{6,7},{7,6},{8,9},{9,8},{10,11... | collective-permute-start | bytes 24584 | tf_op jit(solution)/shard_map/ppermute | solution.py:442
  31.1 3.7 %collective-permute-start.14 = (bf16[2,8,512]{2,1,0:T(8,128)(2,1)S(1)}, bf16[2,8,512]{2,1,0:T(8,128)(2,1)S(1)}, u32[]{:S(2)}, u32[]{:S(2)}) collective-permute-start(bf16[2,8,512]{2,1,0:T(8,128)(2,1)S(1)} %shard_map.149.pair_ref.refs_0_), channel_id=1, source_target_pairs={{0,2},{1,7},{2,0},{3,5},{4,6},{5,3},{6,4},{7,1},{8,10},{9,15},{10,... | collective-permute-start | bytes 49160 | tf_op jit(solution)/shard_map/ppermute | solution.py:442
  32.3 5.0 %collective-permute-start.13 = (bf16[2,8,512]{2,1,0:T(8,128)(2,1)S(1)}, bf16[2,8,512]{2,1,0:T(8,128)(2,1)S(1)}, u32[]{:S(2)}, u32[]{:S(2)}) collective-permute-start(bf16[2,8,512]{2,1,0:T(8,128)(2,1)S(1)} %shard_map.149.pair_ref.refs_0_), channel_id=1, source_target_pairs={{0,4},{1,5},{2,6},{3,7},{4,0},{5,1},{6,2},{7,3},{8,12},{9,13},{10,... | collective-permute-start | bytes 49160 | tf_op jit(solution)/shard_map/ppermute | solution.py:442
  34.8 2.4 %collective-permute-start.15 = (bf16[2,8,512]{2,1,0:T(8,128)(2,1)S(1)}, bf16[2,8,512]{2,1,0:T(8,128)(2,1)S(1)}, u32[]{:S(2)}, u32[]{:S(2)}) collective-permute-start(bf16[2,8,512]{2,1,0:T(8,128)(2,1)S(1)} %collective-permute-done.14.pair_ref.refs_2_), channel_id=1, source_target_pairs={{0,1},{1,0},{2,3},{3,2},{4,5},{5,4},{6,7},{7,6},{8,9},{9,8},{10,11... | collective-permute-start | bytes 49160 | tf_op jit(solution)/shard_map/ppermute | solution.py:442
  39.6 1.3 %collective-permute-start.16 = (f32[4,8,512]{2,1,0:T(8,128)S(1)}, f32[4,8,512]{2,1,0:T(8,128)S(1)}, u32[]{:S(2)}, u32[]{:S(2)}) collective-permute-start(f32[4,8,512]{2,1,0:T(8,128)S(1)} %get-tuple-element.20), channel_id=1, source_target_pairs={{0,1},{1,0},{2,3},{3,2},{4,5},{5,4},{6,7},{7,6},{8,9},{9,8},{10,11... | collective-permute-start | bytes 196616 | tf_op jit(solution)/shard_map/ppermute | solution.py:442
  40.9 3.8 %collective-permute-start.18 = (bf16[2,8,512]{2,1,0:T(8,128)(2,1)S(1)}, bf16[2,8,512]{2,1,0:T(8,128)(2,1)S(1)}, u32[]{:S(2)}, u32[]{:S(2)}) collective-permute-start(bf16[2,8,512]{2,1,0:T(8,128)(2,1)S(1)} %get-tuple-element.23), channel_id=1, source_target_pairs={{0,2},{1,7},{2,0},{3,5},{4,6},{5,3},{6,4},{7,1},{8,10},{9,15},{10,... | collective-permute-start | bytes 49160 | tf_op jit(solution)/shard_map/ppermute | solution.py:442
  42.1 4.7 %collective-permute-start.17 = (bf16[8,512]{1,0:T(8,128)(2,1)S(1)}, bf16[8,512]{1,0:T(8,128)(2,1)S(1)}, u32[]{:S(2)}, u32[]{:S(2)}) collective-permute-start(bf16[8,512]{1,0:T(8,128)(2,1)S(1)} %get-tuple-element.22), channel_id=1, source_target_pairs={{0,4},{1,5},{2,6},{3,7},{4,0},{5,1},{6,2},{7,3},{8,12},{9,13},{10,... | collective-permute-start | bytes 24584 | tf_op jit(solution)/shard_map/ppermute | solution.py:442
  44.7 2.1 %collective-permute-start.19 = (bf16[2,8,512]{2,1,0:T(8,128)(2,1)S(1)}, bf16[2,8,512]{2,1,0:T(8,128)(2,1)S(1)}, u32[]{:S(2)}, u32[]{:S(2)}) collective-permute-start(bf16[2,8,512]{2,1,0:T(8,128)(2,1)S(1)} %collective-permute-done.18.far_ref), channel_id=1, source_target_pairs={{0,1},{1,0},{2,3},{3,2},{4,5},{5,4},{6,7},{7,6},{8,9},{9,8},{10,11... | collective-permute-start | bytes 49160 | tf_op jit(solution)/shard_map/ppermute | solution.py:442
  (16 other events, 225.6 us)

commit v6 on v5

--- a/solution.py
+++ b/solution.py
@@ -238,18 +238,19 @@
     project_blocks(normed_blocks(late_steps(pair_refs), gain_ref, inv_root), weight_refs, finish)
     heads, chan, _ = weight_refs[0].shape
     rows, lanes = total_ref.shape[0], 4 * chan
-    product = total_ref[...].astype(jnp.bfloat16).astype(jnp.float32)
+    product = total_ref[...]
     for head in range(heads):
         made_ref[pl.ds(head, rows, stride=heads), :] = product[:, head * lanes : (head + 1) * lanes]
     chip = lax.axis_index("kv")
     pairs = rows * heads // chips
     for step, sent_ref in placed_blocks(core, near_ref, mid_ref, far_ref, swap_ref):
         first = pl.multiple_of(lax.bitwise_xor(chip, step) * pairs, pairs)
-        sent_ref[...] = made_ref[pl.ds(first, pairs), :]
+        sent_ref[...] = made_ref[pl.ds(first, pairs), :].astype(jnp.bfloat16)
 
 
 def sigmoid(x):
-    return 1.0 / (1.0 + jnp.exp(-x))
+    small = jnp.exp(-jnp.abs(x))
+    return jnp.where(x >= 0.0, 1.0, small) / (1.0 + small)
 
 
 def readout_kernel(chips, *refs):
@@ -260,7 +261,7 @@
     chip, core = lax.axis_index("kv"), lax.axis_index("tp")
     for step, got_ref in placed_blocks(core, *got_refs):
         block = got_ref[...] if len(got_ref.shape) == 2 else got_ref[core]
-        placed_ref[lax.bitwise_xor(chip, step)] = block
+        placed_ref[lax.bitwise_xor(chip, step)] = block.astype(jnp.float32)
 
     def channels(kind):
         return jnp.concatenate(
@@ -285,7 +286,7 @@
     readout = jnp.concatenate(old_parts, axis=0) + new_part
     inv_head = lax.rsqrt(jnp.mean(readout * readout, axis=1, keepdims=True) + epsilon)
     mixed = readout * inv_head * gain * (pre_gate * sigmoid(pre_gate))
-    mixed_ref[...] = mixed.astype(jnp.bfloat16).astype(jnp.float32)
+    mixed_ref[...] = mixed.astype(jnp.bfloat16)
     key_ref[...] = key_rows
     value_ref[...] = value_rows
 
@@ -319,7 +320,9 @@
     chip = lax.axis_index("kv")
     for step, pair_ref in placed_blocks(lax.axis_index("tp"), *pair_refs):
         first = pl.multiple_of(lax.bitwise_xor(chip, step) * (cores * pairs), cores * pairs)
-        placed_ref[pl.ds(first, cores * pairs), :] = pair_ref[...].reshape(-1, values)
+        placed_ref[pl.ds(first, cores * pairs), :] = (
+            pair_ref[...].astype(jnp.float32).reshape(-1, values)
+        )
     blocks = []
     for core in range(cores):
         for head in range(heads):
@@ -478,7 +481,7 @@
     )
     near, mid, far, swap = call(
         functools.partial(project_kernel, kv),
-        [shape((pairs, 4 * chan), f32)] * kv,
+        [shape((pairs, 4 * chan), bf16)] * kv,
         (*pairs_of_rows, early, mix_row, *projections),
         COST[1],
         14 * MIB,
@@ -487,7 +490,7 @@
     got = (near,) + crossed(paired(far, other_core(swap), COST[4]), mid)
     mixed, key_rows, value_rows = call(
         functools.partial(readout_kernel, kv),
-        [shape((pairs, values), f32), shape((pairs, keys), f32), shape((pairs, values), f32)],
+        [shape((pairs, values), bf16), shape((pairs, keys), f32), shape((pairs, values), f32)],
         (*got, lower_bound, recurrent_state, head_gain),
         COST[2],
         14 * MIB,

time: 47.7 us -> 47.4 us (level)
  transfers between devices with their start and end apart: 20 -> 20, of which waited for: 12 -> 13; matrix products, arithmetic and copies ran while one was open for 0% -> 0% of each run, Pallas kernels for 11% -> 11%
where the time goes in v6:
time: 47.4 us; the launch traced here: 47.1 us
  starting transfers between devices  21.2 us (45%)
  waiting for transfers between devices  13.5 us (28%)
  Pallas kernels  10.7 us (23%)
  between operations  0.92 us (2%)
  local copies, waits for them, and re-layouts  0.82 us (2%)
    ppermute x20, starting transfers between devices, permute(): return lax.ppermute(block, group, hops)  21.2 us
    ppermute x20, waiting for transfers between devices, permute(): return lax.ppermute(block, group, hops)  13.5 us
    pallas_call x17, Pallas kernels, call(): pl.pallas_call(body, out_shape=outs, in_specs=[whole] * len(arrays), out_...  9.67 us
    pallas_call x1, Pallas kernels, tiled_local(): pl.pallas_call(copy_out_kernel, out_shape=shape(recurrent_state.shape, f3...  0.98 us
  transfers between devices with their start and end apart: 20, of which 13 were waited for; matrix products, arithmetic and copies ran while one was open for 0% of the time, Pallas kernels for 11%

profile of v6, /device:TPU:0, one launch (start us, length us, event | category | flops | bytes accessed | tf_op | source)
XLA Modules:
  0.0 47.1 jit_solution(1331280233232437584)
XLA Ops:
  2.2 2.9 %collective-permute-start.2 = (bf16[2,8,512]{2,1,0:T(8,128)(2,1)S(1)}, bf16[2,8,512]{2,1,0:T(8,128)(2,1)S(1)}, u32[]{:S(2)}, u32[]{:S(2)}) collective-permute-start(bf16[2,8,512]{2,1,0:T(8,128)(2,1)S(1)} %shard_map.141.pair_ref.refs_0_), channel_id=1, source_target_pairs={{0,2},{1,7},{2,0},{3,5},{4,6},{5,3},{6,4},{7,1},{8,10},{9,15},{10,... | collective-permute-start | bytes 49160 | tf_op jit(solution)/shard_map/ppermute | solution.py:445
  5.1 2.6 %collective-permute-start.1 = (bf16[2,8,512]{2,1,0:T(8,128)(2,1)S(1)}, bf16[2,8,512]{2,1,0:T(8,128)(2,1)S(1)}, u32[]{:S(2)}, u32[]{:S(2)}) collective-permute-start(bf16[2,8,512]{2,1,0:T(8,128)(2,1)S(1)} %shard_map.141.pair_ref.refs_0_), channel_id=1, source_target_pairs={{0,4},{1,5},{2,6},{3,7},{4,0},{5,1},{6,2},{7,3},{8,12},{9,13},{10,... | collective-permute-start | bytes 49160 | tf_op jit(solution)/shard_map/ppermute | solution.py:445
  9.9 1.2 %shard_map.144 = (bf16[16,128]{1,0:T(8,128)(2,1)S(1)}, bf16[16,128]{1,0:T(8,128)(2,1)S(1)}, bf16[16,128]{1,0:T(8,128)(2,1)S(1)}, bf16[16,128]{1,0:T(8,128)(2,1)S(1)}) custom-call(bf16[2,8,512]{2,1,0:T(8,128)(2,1)S(1)} %shard_map.141.pair_ref.refs_0_, bf16[2,8,512]{2,1,0:T(8,128)(2,1)S(1)} %collective-permute-done.1.refs_1_, ...), custom_call_target="tpu_custom_call" | custom-call | flops 99999997952 | tf_op jit(solution)/shard_map/pallas_call | solution.py:102
  11.9 0.8 %collective-permute-done.5.mate_ref = bf16[16,128]{1,0:T(8,128)(2,1)S(1)} collective-permute-done((bf16[16,128]{1,0:T(8,128)(2,1)S(1)}, bf16[16,128]{1,0:T(8,128)(2,1)S(1)}, u32[]{:S(2)}, u32[]{:S(2)}) %collective-permute-start.5) | collective-permute-done | bytes 4128 | tf_op jit(solution)/shard_map/ppermute | solution.py:445
  12.7 3.6 %collective-permute-done.6.refs_2_ = bf16[2,16,128]{2,1,0:T(8,128)(2,1)S(1)} collective-permute-done((bf16[2,16,128]{2,1,0:T(8,128)(2,1)S(1)}, bf16[2,16,128]{2,1,0:T(8,128)(2,1)S(1)}, u32[]{:S(2)}, u32[]{:S(2)}) %collective-permute-start.6) | collective-permute-done | bytes 8224 | tf_op jit(solution)/shard_map/ppermute | solution.py:445
  16.4 1.0 %collective-permute-start.7 = (bf16[2,16,128]{2,1,0:T(8,128)(2,1)S(1)}, bf16[2,16,128]{2,1,0:T(8,128)(2,1)S(1)}, u32[]{:S(2)}, u32[]{:S(2)}) collective-permute-start(bf16[2,16,128]{2,1,0:T(8,128)(2,1)S(1)} %collective-permute-done.6.refs_2_), channel_id=1, source_target_pairs={{0,1},{1,0},{2,3},{3,2},{4,5},{5,4},{6,7},{7,6},{8,9},{9,8},{10,11... | collective-permute-start | bytes 24584 | tf_op jit(solution)/shard_map/ppermute | solution.py:445
  17.3 1.2 %collective-permute-start.4 = (bf16[16,128]{1,0:T(8,128)(2,1)S(1)}, bf16[16,128]{1,0:T(8,128)(2,1)S(1)}, u32[]{:S(2)}, u32[]{:S(2)}) collective-permute-start(bf16[16,128]{1,0:T(8,128)(2,1)S(1)} %get-tuple-element.15), channel_id=1, source_target_pairs={{0,4},{1,5},{2,6},{3,7},{4,0},{5,1},{6,2},{7,3},{8,12},{9,13},{10,... | collective-permute-start | bytes 12296 | tf_op jit(solution)/shard_map/ppermute | solution.py:445
  18.5 3.3 %collective-permute-done.4.refs_1_ = bf16[16,128]{1,0:T(8,128)(2,1)S(1)} collective-permute-done((bf16[16,128]{1,0:T(8,128)(2,1)S(1)}, bf16[16,128]{1,0:T(8,128)(2,1)S(1)}, u32[]{:S(2)}, u32[]{:S(2)}) %collective-permute-start.4) | collective-permute-done | bytes 4128 | tf_op jit(solution)/shard_map/ppermute | solution.py:445
  21.9 0.7 %shard_map.146 = (bf16[16,128]{1,0:T(8,128)(2,1)S(1)}, f32[16,128]{1,0:T(8,128)S(1)}, f32[16,128]{1,0:T(8,128)S(1)}) custom-call(bf16[16,128]{1,0:T(8,128)(2,1)S(1)} %get-tuple-element.14.refs_0_, bf16[16,128]{1,0:T(8,128)(2,1)S(1)} %collective-permute-done.4.refs_1_, bf16[2,16,128]{2,1,0:T(8,128)(2,1)S(1)} %collective-permute-done.6.refs_2_, ...), custom_call_target="tpu_custom_call" | custom-call | flops 1000000000 | tf_op jit(solution)/shard_map/pallas_call | solution.py:102
  22.7 1.2 %collective-permute-done.8.mate_ref = bf16[16,128]{1,0:T(8,128)(2,1)S(1)} collective-permute-done((bf16[16,128]{1,0:T(8,128)(2,1)S(1)}, bf16[16,128]{1,0:T(8,128)(2,1)S(1)}, u32[]{:S(2)}, u32[]{:S(2)}) %collective-permute-start.8) | collective-permute-done | bytes 4128 | tf_op jit(solution)/shard_map/ppermute | solution.py:445
  23.8 2.9 %collective-permute-start.9 = (bf16[2,16,128]{2,1,0:T(8,128)(2,1)S(1)}, bf16[2,16,128]{2,1,0:T(8,128)(2,1)S(1)}, u32[]{:S(2)}, u32[]{:S(2)}) collective-permute-start(bf16[2,16,128]{2,1,0:T(8,128)(2,1)S(1)} %shard_map.147.refs_0_), channel_id=1, source_target_pairs={{0,4},{1,5},{2,6},{3,7},{4,0},{5,1},{6,2},{7,3},{8,12},{9,13},{10,... | collective-permute-start | bytes 24584 | tf_op jit(solution)/shard_map/ppermute | solution.py:445
  27.5 0.8 %collective-permute-start.11 = (bf16[2,16,128]{2,1,0:T(8,128)(2,1)S(1)}, bf16[2,16,128]{2,1,0:T(8,128)(2,1)S(1)}, u32[]{:S(2)}, u32[]{:S(2)}) collective-permute-start(bf16[2,16,128]{2,1,0:T(8,128)(2,1)S(1)} %collective-permute-done.10.refs_2_), channel_id=1, source_target_pairs={{0,1},{1,0},{2,3},{3,2},{4,5},{5,4},{6,7},{7,6},{8,9},{9,8},{10,11... | collective-permute-start | bytes 24584 | tf_op jit(solution)/shard_map/ppermute | solution.py:445
  28.4 0.7 %collective-permute-done.11.refs_3_ = bf16[2,16,128]{2,1,0:T(8,128)(2,1)S(1)} collective-permute-done((bf16[2,16,128]{2,1,0:T(8,128)(2,1)S(1)}, bf16[2,16,128]{2,1,0:T(8,128)(2,1)S(1)}, u32[]{:S(2)}, u32[]{:S(2)}) %collective-permute-start.11) | collective-permute-done | bytes 8224 | tf_op jit(solution)/shard_map/ppermute | solution.py:445
  29.9 0.8 %collective-permute-done.12.mate_ref = bf16[8,512]{1,0:T(8,128)(2,1)S(1)} collective-permute-done((bf16[8,512]{1,0:T(8,128)(2,1)S(1)}, bf16[8,512]{1,0:T(8,128)(2,1)S(1)}, u32[]{:S(2)}, u32[]{:S(2)}) %collective-permute-start.12) | collective-permute-done | bytes 8224 | tf_op jit(solution)/shard_map/ppermute | solution.py:445
  30.8 1.3 %collective-permute-start.14 = (bf16[2,8,512]{2,1,0:T(8,128)(2,1)S(1)}, bf16[2,8,512]{2,1,0:T(8,128)(2,1)S(1)}, u32[]{:S(2)}, u32[]{:S(2)}) collective-permute-start(bf16[2,8,512]{2,1,0:T(8,128)(2,1)S(1)} %shard_map.149.pair_ref.refs_0_), channel_id=1, source_target_pairs={{0,2},{1,7},{2,0},{3,5},{4,6},{5,3},{6,4},{7,1},{8,10},{9,15},{10,... | collective-permute-start | bytes 49160 | tf_op jit(solution)/shard_map/ppermute | solution.py:445
  32.1 1.6 %collective-permute-start.13 = (bf16[2,8,512]{2,1,0:T(8,128)(2,1)S(1)}, bf16[2,8,512]{2,1,0:T(8,128)(2,1)S(1)}, u32[]{:S(2)}, u32[]{:S(2)}) collective-permute-start(bf16[2,8,512]{2,1,0:T(8,128)(2,1)S(1)} %shard_map.149.pair_ref.refs_0_), channel_id=1, source_target_pairs={{0,4},{1,5},{2,6},{3,7},{4,0},{5,1},{6,2},{7,3},{8,12},{9,13},{10,... | collective-permute-start | bytes 49160 | tf_op jit(solution)/shard_map/ppermute | solution.py:445
  33.7 0.8 %collective-permute-done.14.pair_ref.refs_2_ = bf16[2,8,512]{2,1,0:T(8,128)(2,1)S(1)} collective-permute-done((bf16[2,8,512]{2,1,0:T(8,128)(2,1)S(1)}, bf16[2,8,512]{2,1,0:T(8,128)(2,1)S(1)}, u32[]{:S(2)}, u32[]{:S(2)}) %collective-permute-start.14) | collective-permute-done | bytes 16416 | tf_op jit(solution)/shard_map/ppermute | solution.py:445
  34.5 1.0 %collective-permute-start.15 = (bf16[2,8,512]{2,1,0:T(8,128)(2,1)S(1)}, bf16[2,8,512]{2,1,0:T(8,128)(2,1)S(1)}, u32[]{:S(2)}, u32[]{:S(2)}) collective-permute-start(bf16[2,8,512]{2,1,0:T(8,128)(2,1)S(1)} %collective-permute-done.14.pair_ref.refs_2_), channel_id=1, source_target_pairs={{0,1},{1,0},{2,3},{3,2},{4,5},{5,4},{6,7},{7,6},{8,9},{9,8},{10,11... | collective-permute-start | bytes 49160 | tf_op jit(solution)/shard_map/ppermute | solution.py:445
  36.9 2.4 %shard_map.152 = (bf16[8,2048]{1,0:T(8,128)(2,1)S(1)}, f32[4,8,512]{2,1,0:T(8,128)S(1)}) custom-call(bf16[2,8,512]{2,1,0:T(8,128)(2,1)S(1)} %shard_map.149.pair_ref.refs_0_, bf16[2,8,512]{2,1,0:T(8,128)(2,1)S(1)} %collective-permute-done.13.refs_1_, bf16[2,8,512]{2,1,0:T(8,128)(2,1)S(1)} %collective-permute-done.14.pair_ref.refs_2_, ...), custom_call_target="tpu_custom_call" | custom-call | flops 1000000 | tf_op jit(solution)/shard_map/pallas_call | solution.py:102
  39.3 1.2 %shard_map.153.own_ref = f32[4,8,512]{2,1,0:T(8,128)S(1)} custom-call(bf16[8,2048]{1,0:T(8,128)(2,1)S(1)} %get-tuple-element.19.hidden_ref, bf16[2048,4096]{1,0:T(8,128)(2,1)S(1)} %bitcast.3), custom_call_target="tpu_custom_call" | custom-call | flops 1000000000 | tf_op jit(solution)/shard_map/pallas_call | solution.py:102
  40.6 0.8 %collective-permute-start.18 = (bf16[2,8,512]{2,1,0:T(8,128)(2,1)S(1)}, bf16[2,8,512]{2,1,0:T(8,128)(2,1)S(1)}, u32[]{:S(2)}, u32[]{:S(2)}) collective-permute-start(bf16[2,8,512]{2,1,0:T(8,128)(2,1)S(1)} %get-tuple-element.23), channel_id=1, source_target_pairs={{0,2},{1,7},{2,0},{3,5},{4,6},{5,3},{6,4},{7,1},{8,10},{9,15},{10,... | collective-permute-start | bytes 49160 | tf_op jit(solution)/shard_map/ppermute | solution.py:445
  41.9 2.2 %collective-permute-start.17 = (bf16[8,512]{1,0:T(8,128)(2,1)S(1)}, bf16[8,512]{1,0:T(8,128)(2,1)S(1)}, u32[]{:S(2)}, u32[]{:S(2)}) collective-permute-start(bf16[8,512]{1,0:T(8,128)(2,1)S(1)} %get-tuple-element.22), channel_id=1, source_target_pairs={{0,4},{1,5},{2,6},{3,7},{4,0},{5,1},{6,2},{7,3},{8,12},{9,13},{10,... | collective-permute-start | bytes 24584 | tf_op jit(solution)/shard_map/ppermute | solution.py:445
  44.4 1.1 %collective-permute-start.19 = (bf16[2,8,512]{2,1,0:T(8,128)(2,1)S(1)}, bf16[2,8,512]{2,1,0:T(8,128)(2,1)S(1)}, u32[]{:S(2)}, u32[]{:S(2)}) collective-permute-start(bf16[2,8,512]{2,1,0:T(8,128)(2,1)S(1)} %collective-permute-done.18.far_ref), channel_id=1, source_target_pairs={{0,1},{1,0},{2,3},{3,2},{4,5},{5,4},{6,7},{7,6},{8,9},{9,8},{10,11... | collective-permute-start | bytes 49160 | tf_op jit(solution)/shard_map/ppermute | solution.py:445
  45.5 1.0 %shard_map.157 = f32[2,8,128,128]{3,2,1,0:T(8,128)} custom-call(f32[2,8,128,128]{3,2,1,0:T(8,128)S(1)} %shard_map.156.made_ref), custom_call_target="tpu_custom_call" | custom-call | flops 1000000000 | tf_op jit(solution)/shard_map/pallas_call | solution.py:506
  (76 shorter events, 8.9 us)
Async XLA Ops:
  0.6 1.6 %collective-permute-start = (bf16[8,512]{1,0:T(8,128)(2,1)}, bf16[8,512]{1,0:T(8,128)(2,1)S(1)}, u32[]{:S(2)}, u32[]{:S(2)}) collective-permute-start(bf16[8,512]{1,0:T(8,128)(2,1)} %refs_4_.3), channel_id=1, source_target_pairs={{0,1},{1,0},{2,3},{3,2},{4,5},{5,4},{6,7},{7,6},{8,9},{9,8},{10,11... | collective-permute-start | bytes 24584 | tf_op jit(solution)/shard_map/ppermute | solution.py:445
  2.2 6.2 %collective-permute-start.2 = (bf16[2,8,512]{2,1,0:T(8,128)(2,1)S(1)}, bf16[2,8,512]{2,1,0:T(8,128)(2,1)S(1)}, u32[]{:S(2)}, u32[]{:S(2)}) collective-permute-start(bf16[2,8,512]{2,1,0:T(8,128)(2,1)S(1)} %shard_map.141.pair_ref.refs_0_), channel_id=1, source_target_pairs={{0,2},{1,7},{2,0},{3,5},{4,6},{5,3},{6,4},{7,1},{8,10},{9,15},{10,... | collective-permute-start | bytes 49160 | tf_op jit(solution)/shard_map/ppermute | solution.py:445
  5.1 4.7 %collective-permute-start.1 = (bf16[2,8,512]{2,1,0:T(8,128)(2,1)S(1)}, bf16[2,8,512]{2,1,0:T(8,128)(2,1)S(1)}, u32[]{:S(2)}, u32[]{:S(2)}) collective-permute-start(bf16[2,8,512]{2,1,0:T(8,128)(2,1)S(1)} %shard_map.141.pair_ref.refs_0_), channel_id=1, source_target_pairs={{0,4},{1,5},{2,6},{3,7},{4,0},{5,1},{6,2},{7,3},{8,12},{9,13},{10,... | collective-permute-start | bytes 49160 | tf_op jit(solution)/shard_map/ppermute | solution.py:445
  8.4 1.5 %collective-permute-start.3 = (bf16[2,8,512]{2,1,0:T(8,128)(2,1)S(1)}, bf16[2,8,512]{2,1,0:T(8,128)(2,1)S(1)}, u32[]{:S(2)}, u32[]{:S(2)}) collective-permute-start(bf16[2,8,512]{2,1,0:T(8,128)(2,1)S(1)} %collective-permute-done.2.pair_ref.refs_2_), channel_id=1, source_target_pairs={{0,1},{1,0},{2,3},{3,2},{4,5},{5,4},{6,7},{7,6},{8,9},{9,8},{10,11... | collective-permute-start | bytes 49160 | tf_op jit(solution)/shard_map/ppermute | solution.py:445
  8.4 27.1 %slice-start = ((s8[16777216]{0:T(1024)(128)(4,1)}), s8[4194304]{0:T(1024)(128)(4,1)S(1)}, s32[]{:S(2)}) async-start(s8[16777216]{0:T(1024)(128)(4,1)} %bitcast.2), calls=%async_computation | async-start | bytes 8388608
  8.4 27.1 %slice-start.4 = ((s8[16777216]{0:T(1024)(128)(4,1)}), s8[4194304]{0:T(1024)(128)(4,1)S(1)}, s32[]{:S(2)}) async-start(s8[16777216]{0:T(1024)(128)(4,1)} %bitcast.4), calls=%async_computation.4 | async-start | bytes 8388608
  9.2 26.4 %slice-start.1 = ((s8[16777216]{0:T(1024)(128)(4,1)}), s8[4194304]{0:T(1024)(128)(4,1)S(1)}, s32[]{:S(2)}) async-start(s8[16777216]{0:T(1024)(128)(4,1)} %bitcast.2), calls=%async_computation.1 | async-start | bytes 8388608
  9.2 26.4 %slice-start.2 = ((s8[16777216]{0:T(1024)(128)(4,1)}), s8[4194304]{0:T(1024)(128)(4,1)S(1)}, s32[]{:S(2)}) async-start(s8[16777216]{0:T(1024)(128)(4,1)} %bitcast.2), calls=%async_computation.2 | async-start | bytes 8388608
  11.2 1.5 %collective-permute-start.5 = (bf16[16,128]{1,0:T(8,128)(2,1)S(1)}, bf16[16,128]{1,0:T(8,128)(2,1)S(1)}, u32[]{:S(2)}, u32[]{:S(2)}) collective-permute-start(bf16[16,128]{1,0:T(8,128)(2,1)S(1)} %get-tuple-element.17), channel_id=1, source_target_pairs={{0,1},{1,0},{2,3},{3,2},{4,5},{5,4},{6,7},{7,6},{8,9},{9,8},{10,11... | collective-permute-start | bytes 12296 | tf_op jit(solution)/shard_map/ppermute | solution.py:445
  12.7 3.7 %collective-permute-start.6 = (bf16[2,16,128]{2,1,0:T(8,128)(2,1)S(1)}, bf16[2,16,128]{2,1,0:T(8,128)(2,1)S(1)}, u32[]{:S(2)}, u32[]{:S(2)}) collective-permute-start(bf16[2,16,128]{2,1,0:T(8,128)(2,1)S(1)} %shard_map.145), channel_id=1, source_target_pairs={{0,2},{1,7},{2,0},{3,5},{4,6},{5,3},{6,4},{7,1},{8,10},{9,15},{10,... | collective-permute-start | bytes 24584 | tf_op jit(solution)/shard_map/ppermute | solution.py:445
  16.4 5.5 %collective-permute-start.7 = (bf16[2,16,128]{2,1,0:T(8,128)(2,1)S(1)}, bf16[2,16,128]{2,1,0:T(8,128)(2,1)S(1)}, u32[]{:S(2)}, u32[]{:S(2)}) collective-permute-start(bf16[2,16,128]{2,1,0:T(8,128)(2,1)S(1)} %collective-permute-done.6.refs_2_), channel_id=1, source_target_pairs={{0,1},{1,0},{2,3},{3,2},{4,5},{5,4},{6,7},{7,6},{8,9},{9,8},{10,11... | collective-permute-start | bytes 24584 | tf_op jit(solution)/shard_map/ppermute | solution.py:445
  17.3 4.5 %collective-permute-start.4 = (bf16[16,128]{1,0:T(8,128)(2,1)S(1)}, bf16[16,128]{1,0:T(8,128)(2,1)S(1)}, u32[]{:S(2)}, u32[]{:S(2)}) collective-permute-start(bf16[16,128]{1,0:T(8,128)(2,1)S(1)} %get-tuple-element.15), channel_id=1, source_target_pairs={{0,4},{1,5},{2,6},{3,7},{4,0},{5,1},{6,2},{7,3},{8,12},{9,13},{10,... | collective-permute-start | bytes 12296 | tf_op jit(solution)/shard_map/ppermute | solution.py:445
  22.6 1.2 %collective-permute-start.8 = (bf16[16,128]{1,0:T(8,128)(2,1)S(1)}, bf16[16,128]{1,0:T(8,128)(2,1)S(1)}, u32[]{:S(2)}, u32[]{:S(2)}) collective-permute-start(bf16[16,128]{1,0:T(8,128)(2,1)S(1)} %get-tuple-element.18.own_ref), channel_id=1, source_target_pairs={{0,1},{1,0},{2,3},{3,2},{4,5},{5,4},{6,7},{7,6},{8,9},{9,8},{10,11... | collective-permute-start | bytes 12296 | tf_op jit(solution)/shard_map/ppermute | solution.py:445
  23.8 3.7 %collective-permute-start.10 = (bf16[2,16,128]{2,1,0:T(8,128)(2,1)S(1)}, bf16[2,16,128]{2,1,0:T(8,128)(2,1)S(1)}, u32[]{:S(2)}, u32[]{:S(2)}) collective-permute-start(bf16[2,16,128]{2,1,0:T(8,128)(2,1)S(1)} %shard_map.147.refs_0_), channel_id=1, source_target_pairs={{0,2},{1,7},{2,0},{3,5},{4,6},{5,3},{6,4},{7,1},{8,10},{9,15},{10,... | collective-permute-start | bytes 24584 | tf_op jit(solution)/shard_map/ppermute | solution.py:445
  23.8 4.6 %collective-permute-start.9 = (bf16[2,16,128]{2,1,0:T(8,128)(2,1)S(1)}, bf16[2,16,128]{2,1,0:T(8,128)(2,1)S(1)}, u32[]{:S(2)}, u32[]{:S(2)}) collective-permute-start(bf16[2,16,128]{2,1,0:T(8,128)(2,1)S(1)} %shard_map.147.refs_0_), channel_id=1, source_target_pairs={{0,4},{1,5},{2,6},{3,7},{4,0},{5,1},{6,2},{7,3},{8,12},{9,13},{10,... | collective-permute-start | bytes 24584 | tf_op jit(solution)/shard_map/ppermute | solution.py:445
  27.5 1.6 %collective-permute-start.11 = (bf16[2,16,128]{2,1,0:T(8,128)(2,1)S(1)}, bf16[2,16,128]{2,1,0:T(8,128)(2,1)S(1)}, u32[]{:S(2)}, u32[]{:S(2)}) collective-permute-start(bf16[2,16,128]{2,1,0:T(8,128)(2,1)S(1)} %collective-permute-done.10.refs_2_), channel_id=1, source_target_pairs={{0,1},{1,0},{2,3},{3,2},{4,5},{5,4},{6,7},{7,6},{8,9},{9,8},{10,11... | collective-permute-start | bytes 24584 | tf_op jit(solution)/shard_map/ppermute | solution.py:445
  29.5 1.3 %collective-permute-start.12 = (bf16[8,512]{1,0:T(8,128)(2,1)S(1)}, bf16[8,512]{1,0:T(8,128)(2,1)S(1)}, u32[]{:S(2)}, u32[]{:S(2)}) collective-permute-start(bf16[8,512]{1,0:T(8,128)(2,1)S(1)} %shard_map.148.own_ref.residual_ref), channel_id=1, source_target_pairs={{0,1},{1,0},{2,3},{3,2},{4,5},{5,4},{6,7},{7,6},{8,9},{9,8},{10,11... | collective-permute-start | bytes 24584 | tf_op jit(solution)/shard_map/ppermute | solution.py:445
  30.8 3.7 %collective-permute-start.14 = (bf16[2,8,512]{2,1,0:T(8,128)(2,1)S(1)}, bf16[2,8,512]{2,1,0:T(8,128)(2,1)S(1)}, u32[]{:S(2)}, u32[]{:S(2)}) collective-permute-start(bf16[2,8,512]{2,1,0:T(8,128)(2,1)S(1)} %shard_map.149.pair_ref.refs_0_), channel_id=1, source_target_pairs={{0,2},{1,7},{2,0},{3,5},{4,6},{5,3},{6,4},{7,1},{8,10},{9,15},{10,... | collective-permute-start | bytes 49160 | tf_op jit(solution)/shard_map/ppermute | solution.py:445
  32.1 4.9 %collective-permute-start.13 = (bf16[2,8,512]{2,1,0:T(8,128)(2,1)S(1)}, bf16[2,8,512]{2,1,0:T(8,128)(2,1)S(1)}, u32[]{:S(2)}, u32[]{:S(2)}) collective-permute-start(bf16[2,8,512]{2,1,0:T(8,128)(2,1)S(1)} %shard_map.149.pair_ref.refs_0_), channel_id=1, source_target_pairs={{0,4},{1,5},{2,6},{3,7},{4,0},{5,1},{6,2},{7,3},{8,12},{9,13},{10,... | collective-permute-start | bytes 49160 | tf_op jit(solution)/shard_map/ppermute | solution.py:445
  34.5 2.4 %collective-permute-start.15 = (bf16[2,8,512]{2,1,0:T(8,128)(2,1)S(1)}, bf16[2,8,512]{2,1,0:T(8,128)(2,1)S(1)}, u32[]{:S(2)}, u32[]{:S(2)}) collective-permute-start(bf16[2,8,512]{2,1,0:T(8,128)(2,1)S(1)} %collective-permute-done.14.pair_ref.refs_2_), channel_id=1, source_target_pairs={{0,1},{1,0},{2,3},{3,2},{4,5},{5,4},{6,7},{7,6},{8,9},{9,8},{10,11... | collective-permute-start | bytes 49160 | tf_op jit(solution)/shard_map/ppermute | solution.py:445
  39.3 1.3 %collective-permute-start.16 = (f32[4,8,512]{2,1,0:T(8,128)S(1)}, f32[4,8,512]{2,1,0:T(8,128)S(1)}, u32[]{:S(2)}, u32[]{:S(2)}) collective-permute-start(f32[4,8,512]{2,1,0:T(8,128)S(1)} %get-tuple-element.20), channel_id=1, source_target_pairs={{0,1},{1,0},{2,3},{3,2},{4,5},{5,4},{6,7},{7,6},{8,9},{9,8},{10,11... | collective-permute-start | bytes 196616 | tf_op jit(solution)/shard_map/ppermute | solution.py:445
  40.6 3.8 %collective-permute-start.18 = (bf16[2,8,512]{2,1,0:T(8,128)(2,1)S(1)}, bf16[2,8,512]{2,1,0:T(8,128)(2,1)S(1)}, u32[]{:S(2)}, u32[]{:S(2)}) collective-permute-start(bf16[2,8,512]{2,1,0:T(8,128)(2,1)S(1)} %get-tuple-element.23), channel_id=1, source_target_pairs={{0,2},{1,7},{2,0},{3,5},{4,6},{5,3},{6,4},{7,1},{8,10},{9,15},{10,... | collective-permute-start | bytes 49160 | tf_op jit(solution)/shard_map/ppermute | solution.py:445
  41.9 4.6 %collective-permute-start.17 = (bf16[8,512]{1,0:T(8,128)(2,1)S(1)}, bf16[8,512]{1,0:T(8,128)(2,1)S(1)}, u32[]{:S(2)}, u32[]{:S(2)}) collective-permute-start(bf16[8,512]{1,0:T(8,128)(2,1)S(1)} %get-tuple-element.22), channel_id=1, source_target_pairs={{0,4},{1,5},{2,6},{3,7},{4,0},{5,1},{6,2},{7,3},{8,12},{9,13},{10,... | collective-permute-start | bytes 24584 | tf_op jit(solution)/shard_map/ppermute | solution.py:445
  44.4 2.1 %collective-permute-start.19 = (bf16[2,8,512]{2,1,0:T(8,128)(2,1)S(1)}, bf16[2,8,512]{2,1,0:T(8,128)(2,1)S(1)}, u32[]{:S(2)}, u32[]{:S(2)}) collective-permute-start(bf16[2,8,512]{2,1,0:T(8,128)(2,1)S(1)} %collective-permute-done.18.far_ref), channel_id=1, source_target_pairs={{0,1},{1,0},{2,3},{3,2},{4,5},{5,4},{6,7},{7,6},{8,9},{9,8},{10,11... | collective-permute-start | bytes 49160 | tf_op jit(solution)/shard_map/ppermute | solution.py:445
  (16 other events, 223.1 us)

commit v7 on v6

--- a/solution.py
+++ b/solution.py
@@ -111,13 +111,13 @@
 
 
 def far_step(core):
-    return 1 + 2 * core
+    return 1 + core
 
 
 def placed_blocks(core, near_ref, mid_ref, far_ref, swapped_ref):
     return (
         (0, near_ref),
-        (2, mid_ref),
+        (3, mid_ref),
         (far_step(core), far_ref),
         (far_step(1 - core), swapped_ref),
     )
@@ -184,8 +184,12 @@
     return far_step(lax.axis_index("tp"))
 
 
+def swapped_step():
+    return far_step(1 - lax.axis_index("tp"))
+
+
 def late_steps(pair_refs):
-    return ((2, pair_refs[1]), (far_step(1 - lax.axis_index("tp")), pair_refs[3]))
+    return ((3, pair_refs[1]),)
 
 
 def split_blocks(steps, gain_ref):
@@ -353,7 +357,7 @@
     width = partial_ref.shape[2]
     chip = lax.axis_index("kv")
     far = lax.bitwise_xor(chip, far_step(core))
-    columns = (2 * far, 2 * far + 1, 2 * lax.bitwise_xor(chip, 2) + core, 2 * chip + core)
+    columns = (2 * far, 2 * far + 1, 2 * lax.bitwise_xor(chip, 3) + core, 2 * chip + core)
     for slot, column in enumerate(columns):
         partial_ref[slot] = jnp.dot(
             hidden,
@@ -451,8 +455,8 @@
         return call(pair_kernel, shape((tp,) + block.shape, block.dtype), (block, mate), cost, MIB)
 
     def crossed(far, mid):
-        got_far = permute(far, (1, 3))
-        got_mid = permute(mid, (2, 2))
+        got_far = permute(far, (1, 2))
+        got_mid = permute(mid, (3, 3))
         return got_mid, got_far, permute(got_far, (0, 0), True)
 
     def gather_pairs(block, staged, cost):
@@ -461,7 +465,7 @@
 
     def early_parts(kernel, got, operands, columns, cost):
         total = ()
-        for place, step in ((0, near_step), (2, other_step)):
+        for place, step in ((0, near_step), (2, other_step), (3, swapped_step)):
             part = call(
                 functools.partial(kernel, step),
                 shape((rows, columns), f32),

time: 47.4 us -> 50.1 us (1.057)
  waiting for transfers between devices: 13.5 us -> 20.9 us
  starting transfers between devices: 21.2 us -> 16.4 us
    ppermute x20, waiting for transfers between devices: 13.5 us -> 20.9 us  [permute(): return lax.ppermute(block, group, hops)]
    ppermute x20, starting transfers between devices: 21.2 us -> 16.4 us  [permute(): return lax.ppermute(block, group, hops)]
    pallas_call x17 -> x19, Pallas kernels: 9.67 us -> 9.9 us  [call(): pl.pallas_call(body, out_shape=outs, in_specs=[whole] * len(arrays), out_...]
  transfers between devices with their start and end apart: 20 -> 20, of which waited for: 13 -> 15; matrix products, arithmetic and copies ran while one was open for 0% -> 0% of each run, Pallas kernels for 11% -> 13%
where the time goes in v7:
time: 50.1 us; the launch traced here: 49.9 us
  waiting for transfers between devices  20.9 us (42%)
  starting transfers between devices  16.4 us (33%)
  Pallas kernels  10.9 us (22%)
  between operations  0.91 us (2%)
  local copies, waits for them, and re-layouts  0.81 us (2%)
    ppermute x20, waiting for transfers between devices, permute(): return lax.ppermute(block, group, hops)  20.9 us
    ppermute x20, starting transfers between devices, permute(): return lax.ppermute(block, group, hops)  16.4 us
    pallas_call x19, Pallas kernels, call(): pl.pallas_call(body, out_shape=outs, in_specs=[whole] * len(arrays), out_...  9.9 us
  transfers between devices with their start and end apart: 20, of which 15 were waited for; matrix products, arithmetic and copies ran while one was open for 0% of the time, Pallas kernels for 13%

profile of v7, /device:TPU:0, one launch (start us, length us, event | category | flops | bytes accessed | tf_op | source)
XLA Modules:
  0.0 49.9 jit_solution(16734899347881064644)
XLA Ops:
  1.2 0.7 %copy-done.7 = bf16[8,512]{1,0:T(8,128)(2,1)S(1)} copy-done((bf16[8,512]{1,0:T(8,128)(2,1)S(1)}, bf16[8,512]{1,0:T(8,128)(2,1)}, u32[]{:S(2)}) %copy-start.7) | copy-done | bytes 8216
  2.2 2.9 %collective-permute-start.2 = (bf16[2,8,512]{2,1,0:T(8,128)(2,1)S(1)}, bf16[2,8,512]{2,1,0:T(8,128)(2,1)S(1)}, u32[]{:S(2)}, u32[]{:S(2)}) collective-permute-start(bf16[2,8,512]{2,1,0:T(8,128)(2,1)S(1)} %shard_map.141.pair_ref.refs_0_), channel_id=1, source_target_pairs={{0,2},{1,5},{2,0},{3,7},{4,6},{5,1},{6,4},{7,3},{8,10},{9,13},{10,... | collective-permute-start | bytes 49160 | tf_op jit(solution)/shard_map/ppermute | solution.py:449
  5.1 2.5 %collective-permute-start.1 = (bf16[2,8,512]{2,1,0:T(8,128)(2,1)S(1)}, bf16[2,8,512]{2,1,0:T(8,128)(2,1)S(1)}, u32[]{:S(2)}, u32[]{:S(2)}) collective-permute-start(bf16[2,8,512]{2,1,0:T(8,128)(2,1)S(1)} %shard_map.141.pair_ref.refs_0_), channel_id=1, source_target_pairs={{0,6},{1,7},{2,4},{3,5},{4,2},{5,3},{6,0},{7,1},{8,14},{9,15},{10,... | collective-permute-start | bytes 49160 | tf_op jit(solution)/shard_map/ppermute | solution.py:449
  10.8 0.7 %shard_map.145 = (bf16[16,128]{1,0:T(8,128)(2,1)S(1)}, bf16[16,128]{1,0:T(8,128)(2,1)S(1)}, bf16[16,128]{1,0:T(8,128)(2,1)S(1)}, bf16[16,128]{1,0:T(8,128)(2,1)S(1)}) custom-call(bf16[2,8,512]{2,1,0:T(8,128)(2,1)S(1)} %shard_map.141.pair_ref.refs_0_, bf16[2,8,512]{2,1,0:T(8,128)(2,1)S(1)} %collective-permute-done.1.refs_1_, ...), custom_call_target="tpu_custom_call" | custom-call | flops 99999997952 | tf_op jit(solution)/shard_map/pallas_call | solution.py:102
  11.6 1.1 %collective-permute-done.5.mate_ref = bf16[16,128]{1,0:T(8,128)(2,1)S(1)} collective-permute-done((bf16[16,128]{1,0:T(8,128)(2,1)S(1)}, bf16[16,128]{1,0:T(8,128)(2,1)S(1)}, u32[]{:S(2)}, u32[]{:S(2)}) %collective-permute-start.5) | collective-permute-done | bytes 4128 | tf_op jit(solution)/shard_map/ppermute | solution.py:449
  12.9 3.5 %collective-permute-done.6.refs_2_ = bf16[2,16,128]{2,1,0:T(8,128)(2,1)S(1)} collective-permute-done((bf16[2,16,128]{2,1,0:T(8,128)(2,1)S(1)}, bf16[2,16,128]{2,1,0:T(8,128)(2,1)S(1)}, u32[]{:S(2)}, u32[]{:S(2)}) %collective-permute-start.6) | collective-permute-done | bytes 8224 | tf_op jit(solution)/shard_map/ppermute | solution.py:449
  16.4 2.4 %collective-permute-start.4 = (bf16[16,128]{1,0:T(8,128)(2,1)S(1)}, bf16[16,128]{1,0:T(8,128)(2,1)S(1)}, u32[]{:S(2)}, u32[]{:S(2)}) collective-permute-start(bf16[16,128]{1,0:T(8,128)(2,1)S(1)} %get-tuple-element.15), channel_id=1, source_target_pairs={{0,6},{1,7},{2,4},{3,5},{4,2},{5,3},{6,0},{7,1},{8,14},{9,15},{10,... | collective-permute-start | bytes 12296 | tf_op jit(solution)/shard_map/ppermute | solution.py:449
  18.8 3.0 %collective-permute-done.4.refs_1_ = bf16[16,128]{1,0:T(8,128)(2,1)S(1)} collective-permute-done((bf16[16,128]{1,0:T(8,128)(2,1)S(1)}, bf16[16,128]{1,0:T(8,128)(2,1)S(1)}, u32[]{:S(2)}, u32[]{:S(2)}) %collective-permute-start.4) | collective-permute-done | bytes 4128 | tf_op jit(solution)/shard_map/ppermute | solution.py:449
  21.8 0.7 %shard_map.147 = (bf16[16,128]{1,0:T(8,128)(2,1)S(1)}, f32[16,128]{1,0:T(8,128)S(1)}, f32[16,128]{1,0:T(8,128)S(1)}) custom-call(bf16[16,128]{1,0:T(8,128)(2,1)S(1)} %get-tuple-element.14.refs_0_, bf16[16,128]{1,0:T(8,128)(2,1)S(1)} %collective-permute-done.4.refs_1_, bf16[2,16,128]{2,1,0:T(8,128)(2,1)S(1)} %collective-permute-done.6.refs_2_, ...), custom_call_target="tpu_custom_call" | custom-call | flops 1000000000 | tf_op jit(solution)/shard_map/pallas_call | solution.py:102
  22.6 1.2 %collective-permute-done.8.mate_ref = bf16[16,128]{1,0:T(8,128)(2,1)S(1)} collective-permute-done((bf16[16,128]{1,0:T(8,128)(2,1)S(1)}, bf16[16,128]{1,0:T(8,128)(2,1)S(1)}, u32[]{:S(2)}, u32[]{:S(2)}) %collective-permute-start.8) | collective-permute-done | bytes 4128 | tf_op jit(solution)/shard_map/ppermute | solution.py:449
  23.8 2.4 %collective-permute-start.9 = (bf16[2,16,128]{2,1,0:T(8,128)(2,1)S(1)}, bf16[2,16,128]{2,1,0:T(8,128)(2,1)S(1)}, u32[]{:S(2)}, u32[]{:S(2)}) collective-permute-start(bf16[2,16,128]{2,1,0:T(8,128)(2,1)S(1)} %shard_map.148.refs_0_), channel_id=1, source_target_pairs={{0,6},{1,7},{2,4},{3,5},{4,2},{5,3},{6,0},{7,1},{8,14},{9,15},{10,... | collective-permute-start | bytes 24584 | tf_op jit(solution)/shard_map/ppermute | solution.py:449
  26.1 1.3 %collective-permute-done.10.refs_2_ = bf16[2,16,128]{2,1,0:T(8,128)(2,1)S(1)} collective-permute-done((bf16[2,16,128]{2,1,0:T(8,128)(2,1)S(1)}, bf16[2,16,128]{2,1,0:T(8,128)(2,1)S(1)}, u32[]{:S(2)}, u32[]{:S(2)}) %collective-permute-start.10) | collective-permute-done | bytes 8224 | tf_op jit(solution)/shard_map/ppermute | solution.py:449
  27.4 1.8 %collective-permute-done.9.refs_1_ = bf16[2,16,128]{2,1,0:T(8,128)(2,1)S(1)} collective-permute-done((bf16[2,16,128]{2,1,0:T(8,128)(2,1)S(1)}, bf16[2,16,128]{2,1,0:T(8,128)(2,1)S(1)}, u32[]{:S(2)}, u32[]{:S(2)}) %collective-permute-start.9) | collective-permute-done | bytes 8224 | tf_op jit(solution)/shard_map/ppermute | solution.py:449
  29.7 1.2 %collective-permute-done.12.mate_ref = bf16[8,512]{1,0:T(8,128)(2,1)S(1)} collective-permute-done((bf16[8,512]{1,0:T(8,128)(2,1)S(1)}, bf16[8,512]{1,0:T(8,128)(2,1)S(1)}, u32[]{:S(2)}, u32[]{:S(2)}) %collective-permute-start.12) | collective-permute-done | bytes 8224 | tf_op jit(solution)/shard_map/ppermute | solution.py:449
  31.1 3.5 %collective-permute-done.14.pair_ref.refs_2_ = bf16[2,8,512]{2,1,0:T(8,128)(2,1)S(1)} collective-permute-done((bf16[2,8,512]{2,1,0:T(8,128)(2,1)S(1)}, bf16[2,8,512]{2,1,0:T(8,128)(2,1)S(1)}, u32[]{:S(2)}, u32[]{:S(2)}) %collective-permute-start.14) | collective-permute-done | bytes 16416 | tf_op jit(solution)/shard_map/ppermute | solution.py:449
  34.6 2.4 %collective-permute-start.13 = (bf16[2,8,512]{2,1,0:T(8,128)(2,1)S(1)}, bf16[2,8,512]{2,1,0:T(8,128)(2,1)S(1)}, u32[]{:S(2)}, u32[]{:S(2)}) collective-permute-start(bf16[2,8,512]{2,1,0:T(8,128)(2,1)S(1)} %shard_map.150.pair_ref.refs_0_), channel_id=1, source_target_pairs={{0,6},{1,7},{2,4},{3,5},{4,2},{5,3},{6,0},{7,1},{8,14},{9,15},{10,... | collective-permute-start | bytes 49160 | tf_op jit(solution)/shard_map/ppermute | solution.py:449
  38.4 0.7 %shard_map.153.refs_4_ = f32[8,2048]{1,0:T(8,128)S(1)} custom-call(bf16[2,8,512]{2,1,0:T(8,128)(2,1)S(1)} %collective-permute-done.15.pair_ref.refs_3_, f32[1,4096]{1,0:T(1,128)S(1)} %bitcast.8, bf16[4096,2048]{1,0:T(8,128)(2,1)S(1)} %bitcast.5, bf16[2048,4096]{1,0:T(8,128)(2,1)S(1)} %bitcast.3, f32[8,2048]{1,0:T(8,128)S(1)} %shard_map.152.refs_0_), custom_call_target="tpu_custom_call" | custom-call | flops 1000000 | tf_op jit(solution)/shard_map/pallas_call | solution.py:102
  39.1 1.1 %collective-permute-done.13.refs_1_ = bf16[2,8,512]{2,1,0:T(8,128)(2,1)S(1)} collective-permute-done((bf16[2,8,512]{2,1,0:T(8,128)(2,1)S(1)}, bf16[2,8,512]{2,1,0:T(8,128)(2,1)S(1)}, u32[]{:S(2)}, u32[]{:S(2)}) %collective-permute-start.13) | collective-permute-done | bytes 16416 | tf_op jit(solution)/shard_map/ppermute | solution.py:449
  40.2 1.8 %shard_map.154 = (bf16[8,2048]{1,0:T(8,128)(2,1)S(1)}, f32[4,8,512]{2,1,0:T(8,128)S(1)}) custom-call(bf16[2,8,512]{2,1,0:T(8,128)(2,1)S(1)} %shard_map.150.pair_ref.refs_0_, bf16[2,8,512]{2,1,0:T(8,128)(2,1)S(1)} %collective-permute-done.13.refs_1_, bf16[2,8,512]{2,1,0:T(8,128)(2,1)S(1)} %collective-permute-done.14.pair_ref.refs_2_, ...), custom_call_target="tpu_custom_call" | custom-call | flops 1000000 | tf_op jit(solution)/shard_map/pallas_call | solution.py:102
  42.0 1.2 %shard_map.155.own_ref = f32[4,8,512]{2,1,0:T(8,128)S(1)} custom-call(bf16[8,2048]{1,0:T(8,128)(2,1)S(1)} %get-tuple-element.19.hidden_ref, bf16[2048,4096]{1,0:T(8,128)(2,1)S(1)} %bitcast.3), custom_call_target="tpu_custom_call" | custom-call | flops 1000000000 | tf_op jit(solution)/shard_map/pallas_call | solution.py:102
  43.8 2.4 %collective-permute-start.17 = (bf16[8,512]{1,0:T(8,128)(2,1)S(1)}, bf16[8,512]{1,0:T(8,128)(2,1)S(1)}, u32[]{:S(2)}, u32[]{:S(2)}) collective-permute-start(bf16[8,512]{1,0:T(8,128)(2,1)S(1)} %get-tuple-element.22), channel_id=1, source_target_pairs={{0,6},{1,7},{2,4},{3,5},{4,2},{5,3},{6,0},{7,1},{8,14},{9,15},{10,... | collective-permute-start | bytes 24584 | tf_op jit(solution)/shard_map/ppermute | solution.py:449
  46.2 0.8 %collective-permute-done.18.far_ref = bf16[2,8,512]{2,1,0:T(8,128)(2,1)S(1)} collective-permute-done((bf16[2,8,512]{2,1,0:T(8,128)(2,1)S(1)}, bf16[2,8,512]{2,1,0:T(8,128)(2,1)S(1)}, u32[]{:S(2)}, u32[]{:S(2)}) %collective-permute-start.18) | collective-permute-done | bytes 16416 | tf_op jit(solution)/shard_map/ppermute | solution.py:449
  47.3 1.0 %shard_map.159 = f32[2,8,128,128]{3,2,1,0:T(8,128)} custom-call(f32[2,8,128,128]{3,2,1,0:T(8,128)S(1)} %shard_map.158.made_ref), custom_call_target="tpu_custom_call" | custom-call | flops 1000000000 | tf_op jit(solution)/shard_map/pallas_call | solution.py:510
  48.3 1.1 %collective-permute-done.17.mid_ref = bf16[8,512]{1,0:T(8,128)(2,1)S(1)} collective-permute-done((bf16[8,512]{1,0:T(8,128)(2,1)S(1)}, bf16[8,512]{1,0:T(8,128)(2,1)S(1)}, u32[]{:S(2)}, u32[]{:S(2)}) %collective-permute-start.17) | collective-permute-done | bytes 8224 | tf_op jit(solution)/shard_map/ppermute | solution.py:449
  (78 shorter events, 7.8 us)
Async XLA Ops:
  0.6 1.6 %collective-permute-start = (bf16[8,512]{1,0:T(8,128)(2,1)}, bf16[8,512]{1,0:T(8,128)(2,1)S(1)}, u32[]{:S(2)}, u32[]{:S(2)}) collective-permute-start(bf16[8,512]{1,0:T(8,128)(2,1)} %refs_4_.3), channel_id=1, source_target_pairs={{0,1},{1,0},{2,3},{3,2},{4,5},{5,4},{6,7},{7,6},{8,9},{9,8},{10,11... | collective-permute-start | bytes 24584 | tf_op jit(solution)/shard_map/ppermute | solution.py:449
  2.2 6.1 %collective-permute-start.2 = (bf16[2,8,512]{2,1,0:T(8,128)(2,1)S(1)}, bf16[2,8,512]{2,1,0:T(8,128)(2,1)S(1)}, u32[]{:S(2)}, u32[]{:S(2)}) collective-permute-start(bf16[2,8,512]{2,1,0:T(8,128)(2,1)S(1)} %shard_map.141.pair_ref.refs_0_), channel_id=1, source_target_pairs={{0,2},{1,5},{2,0},{3,7},{4,6},{5,1},{6,4},{7,3},{8,10},{9,13},{10,... | collective-permute-start | bytes 49160 | tf_op jit(solution)/shard_map/ppermute | solution.py:449
  5.1 5.6 %collective-permute-start.1 = (bf16[2,8,512]{2,1,0:T(8,128)(2,1)S(1)}, bf16[2,8,512]{2,1,0:T(8,128)(2,1)S(1)}, u32[]{:S(2)}, u32[]{:S(2)}) collective-permute-start(bf16[2,8,512]{2,1,0:T(8,128)(2,1)S(1)} %shard_map.141.pair_ref.refs_0_), channel_id=1, source_target_pairs={{0,6},{1,7},{2,4},{3,5},{4,2},{5,3},{6,0},{7,1},{8,14},{9,15},{10,... | collective-permute-start | bytes 49160 | tf_op jit(solution)/shard_map/ppermute | solution.py:449
  8.3 1.2 %collective-permute-start.3 = (bf16[2,8,512]{2,1,0:T(8,128)(2,1)S(1)}, bf16[2,8,512]{2,1,0:T(8,128)(2,1)S(1)}, u32[]{:S(2)}, u32[]{:S(2)}) collective-permute-start(bf16[2,8,512]{2,1,0:T(8,128)(2,1)S(1)} %collective-permute-done.2.pair_ref.refs_2_), channel_id=1, source_target_pairs={{0,1},{1,0},{2,3},{3,2},{4,5},{5,4},{6,7},{7,6},{8,9},{9,8},{10,11... | collective-permute-start | bytes 49160 | tf_op jit(solution)/shard_map/ppermute | solution.py:449
  9.5 27.5 %slice-start = ((s8[16777216]{0:T(1024)(128)(4,1)}), s8[4194304]{0:T(1024)(128)(4,1)S(1)}, s32[]{:S(2)}) async-start(s8[16777216]{0:T(1024)(128)(4,1)} %bitcast.2), calls=%async_computation | async-start | bytes 8388608
  9.5 27.5 %slice-start.4 = ((s8[16777216]{0:T(1024)(128)(4,1)}), s8[4194304]{0:T(1024)(128)(4,1)S(1)}, s32[]{:S(2)}) async-start(s8[16777216]{0:T(1024)(128)(4,1)} %bitcast.4), calls=%async_computation.4 | async-start | bytes 8388608
  10.2 26.8 %slice-start.1 = ((s8[16777216]{0:T(1024)(128)(4,1)}), s8[4194304]{0:T(1024)(128)(4,1)S(1)}, s32[]{:S(2)}) async-start(s8[16777216]{0:T(1024)(128)(4,1)} %bitcast.2), calls=%async_computation.1 | async-start | bytes 8388608
  10.2 26.8 %slice-start.2 = ((s8[16777216]{0:T(1024)(128)(4,1)}), s8[4194304]{0:T(1024)(128)(4,1)S(1)}, s32[]{:S(2)}) async-start(s8[16777216]{0:T(1024)(128)(4,1)} %bitcast.2), calls=%async_computation.2 | async-start | bytes 8388608
  11.5 1.2 %collective-permute-start.5 = (bf16[16,128]{1,0:T(8,128)(2,1)S(1)}, bf16[16,128]{1,0:T(8,128)(2,1)S(1)}, u32[]{:S(2)}, u32[]{:S(2)}) collective-permute-start(bf16[16,128]{1,0:T(8,128)(2,1)S(1)} %get-tuple-element.17), channel_id=1, source_target_pairs={{0,1},{1,0},{2,3},{3,2},{4,5},{5,4},{6,7},{7,6},{8,9},{9,8},{10,11... | collective-permute-start | bytes 12296 | tf_op jit(solution)/shard_map/ppermute | solution.py:449
  12.7 3.7 %collective-permute-start.6 = (bf16[2,16,128]{2,1,0:T(8,128)(2,1)S(1)}, bf16[2,16,128]{2,1,0:T(8,128)(2,1)S(1)}, u32[]{:S(2)}, u32[]{:S(2)}) collective-permute-start(bf16[2,16,128]{2,1,0:T(8,128)(2,1)S(1)} %shard_map.146), channel_id=1, source_target_pairs={{0,2},{1,5},{2,0},{3,7},{4,6},{5,1},{6,4},{7,3},{8,10},{9,13},{10,... | collective-permute-start | bytes 24584 | tf_op jit(solution)/shard_map/ppermute | solution.py:449
  16.4 5.4 %collective-permute-start.7 = (bf16[2,16,128]{2,1,0:T(8,128)(2,1)S(1)}, bf16[2,16,128]{2,1,0:T(8,128)(2,1)S(1)}, u32[]{:S(2)}, u32[]{:S(2)}) collective-permute-start(bf16[2,16,128]{2,1,0:T(8,128)(2,1)S(1)} %collective-permute-done.6.refs_2_), channel_id=1, source_target_pairs={{0,1},{1,0},{2,3},{3,2},{4,5},{5,4},{6,7},{7,6},{8,9},{9,8},{10,11... | collective-permute-start | bytes 24584 | tf_op jit(solution)/shard_map/ppermute | solution.py:449
  16.4 5.4 %collective-permute-start.4 = (bf16[16,128]{1,0:T(8,128)(2,1)S(1)}, bf16[16,128]{1,0:T(8,128)(2,1)S(1)}, u32[]{:S(2)}, u32[]{:S(2)}) collective-permute-start(bf16[16,128]{1,0:T(8,128)(2,1)S(1)} %get-tuple-element.15), channel_id=1, source_target_pairs={{0,6},{1,7},{2,4},{3,5},{4,2},{5,3},{6,0},{7,1},{8,14},{9,15},{10,... | collective-permute-start | bytes 12296 | tf_op jit(solution)/shard_map/ppermute | solution.py:449
  22.6 1.2 %collective-permute-start.8 = (bf16[16,128]{1,0:T(8,128)(2,1)S(1)}, bf16[16,128]{1,0:T(8,128)(2,1)S(1)}, u32[]{:S(2)}, u32[]{:S(2)}) collective-permute-start(bf16[16,128]{1,0:T(8,128)(2,1)S(1)} %get-tuple-element.18.own_ref), channel_id=1, source_target_pairs={{0,1},{1,0},{2,3},{3,2},{4,5},{5,4},{6,7},{7,6},{8,9},{9,8},{10,11... | collective-permute-start | bytes 12296 | tf_op jit(solution)/shard_map/ppermute | solution.py:449
  23.8 3.7 %collective-permute-start.10 = (bf16[2,16,128]{2,1,0:T(8,128)(2,1)S(1)}, bf16[2,16,128]{2,1,0:T(8,128)(2,1)S(1)}, u32[]{:S(2)}, u32[]{:S(2)}) collective-permute-start(bf16[2,16,128]{2,1,0:T(8,128)(2,1)S(1)} %shard_map.148.refs_0_), channel_id=1, source_target_pairs={{0,2},{1,5},{2,0},{3,7},{4,6},{5,1},{6,4},{7,3},{8,10},{9,13},{10,... | collective-permute-start | bytes 24584 | tf_op jit(solution)/shard_map/ppermute | solution.py:449
  23.8 5.4 %collective-permute-start.9 = (bf16[2,16,128]{2,1,0:T(8,128)(2,1)S(1)}, bf16[2,16,128]{2,1,0:T(8,128)(2,1)S(1)}, u32[]{:S(2)}, u32[]{:S(2)}) collective-permute-start(bf16[2,16,128]{2,1,0:T(8,128)(2,1)S(1)} %shard_map.148.refs_0_), channel_id=1, source_target_pairs={{0,6},{1,7},{2,4},{3,5},{4,2},{5,3},{6,0},{7,1},{8,14},{9,15},{10,... | collective-permute-start | bytes 24584 | tf_op jit(solution)/shard_map/ppermute | solution.py:449
  27.4 1.8 %collective-permute-start.11 = (bf16[2,16,128]{2,1,0:T(8,128)(2,1)S(1)}, bf16[2,16,128]{2,1,0:T(8,128)(2,1)S(1)}, u32[]{:S(2)}, u32[]{:S(2)}) collective-permute-start(bf16[2,16,128]{2,1,0:T(8,128)(2,1)S(1)} %collective-permute-done.10.refs_2_), channel_id=1, source_target_pairs={{0,1},{1,0},{2,3},{3,2},{4,5},{5,4},{6,7},{7,6},{8,9},{9,8},{10,11... | collective-permute-start | bytes 24584 | tf_op jit(solution)/shard_map/ppermute | solution.py:449
  29.6 1.2 %collective-permute-start.12 = (bf16[8,512]{1,0:T(8,128)(2,1)S(1)}, bf16[8,512]{1,0:T(8,128)(2,1)S(1)}, u32[]{:S(2)}, u32[]{:S(2)}) collective-permute-start(bf16[8,512]{1,0:T(8,128)(2,1)S(1)} %shard_map.149.own_ref.residual_ref), channel_id=1, source_target_pairs={{0,1},{1,0},{2,3},{3,2},{4,5},{5,4},{6,7},{7,6},{8,9},{9,8},{10,11... | collective-permute-start | bytes 24584 | tf_op jit(solution)/shard_map/ppermute | solution.py:449
  30.9 3.8 %collective-permute-start.14 = (bf16[2,8,512]{2,1,0:T(8,128)(2,1)S(1)}, bf16[2,8,512]{2,1,0:T(8,128)(2,1)S(1)}, u32[]{:S(2)}, u32[]{:S(2)}) collective-permute-start(bf16[2,8,512]{2,1,0:T(8,128)(2,1)S(1)} %shard_map.150.pair_ref.refs_0_), channel_id=1, source_target_pairs={{0,2},{1,5},{2,0},{3,7},{4,6},{5,1},{6,4},{7,3},{8,10},{9,13},{10,... | collective-permute-start | bytes 49160 | tf_op jit(solution)/shard_map/ppermute | solution.py:449
  34.6 3.8 %collective-permute-start.15 = (bf16[2,8,512]{2,1,0:T(8,128)(2,1)S(1)}, bf16[2,8,512]{2,1,0:T(8,128)(2,1)S(1)}, u32[]{:S(2)}, u32[]{:S(2)}) collective-permute-start(bf16[2,8,512]{2,1,0:T(8,128)(2,1)S(1)} %collective-permute-done.14.pair_ref.refs_2_), channel_id=1, source_target_pairs={{0,1},{1,0},{2,3},{3,2},{4,5},{5,4},{6,7},{7,6},{8,9},{9,8},{10,11... | collective-permute-start | bytes 49160 | tf_op jit(solution)/shard_map/ppermute | solution.py:449
  34.6 5.5 %collective-permute-start.13 = (bf16[2,8,512]{2,1,0:T(8,128)(2,1)S(1)}, bf16[2,8,512]{2,1,0:T(8,128)(2,1)S(1)}, u32[]{:S(2)}, u32[]{:S(2)}) collective-permute-start(bf16[2,8,512]{2,1,0:T(8,128)(2,1)S(1)} %shard_map.150.pair_ref.refs_0_), channel_id=1, source_target_pairs={{0,6},{1,7},{2,4},{3,5},{4,2},{5,3},{6,0},{7,1},{8,14},{9,15},{10,... | collective-permute-start | bytes 49160 | tf_op jit(solution)/shard_map/ppermute | solution.py:449
  42.0 1.3 %collective-permute-start.16 = (f32[4,8,512]{2,1,0:T(8,128)S(1)}, f32[4,8,512]{2,1,0:T(8,128)S(1)}, u32[]{:S(2)}, u32[]{:S(2)}) collective-permute-start(f32[4,8,512]{2,1,0:T(8,128)S(1)} %get-tuple-element.20), channel_id=1, source_target_pairs={{0,1},{1,0},{2,3},{3,2},{4,5},{5,4},{6,7},{7,6},{8,9},{9,8},{10,11... | collective-permute-start | bytes 196616 | tf_op jit(solution)/shard_map/ppermute | solution.py:449
  43.3 3.8 %collective-permute-start.18 = (bf16[2,8,512]{2,1,0:T(8,128)(2,1)S(1)}, bf16[2,8,512]{2,1,0:T(8,128)(2,1)S(1)}, u32[]{:S(2)}, u32[]{:S(2)}) collective-permute-start(bf16[2,8,512]{2,1,0:T(8,128)(2,1)S(1)} %get-tuple-element.23), channel_id=1, source_target_pairs={{0,2},{1,5},{2,0},{3,7},{4,6},{5,1},{6,4},{7,3},{8,10},{9,13},{10,... | collective-permute-start | bytes 49160 | tf_op jit(solution)/shard_map/ppermute | solution.py:449
  43.8 5.5 %collective-permute-start.17 = (bf16[8,512]{1,0:T(8,128)(2,1)S(1)}, bf16[8,512]{1,0:T(8,128)(2,1)S(1)}, u32[]{:S(2)}, u32[]{:S(2)}) collective-permute-start(bf16[8,512]{1,0:T(8,128)(2,1)S(1)} %get-tuple-element.22), channel_id=1, source_target_pairs={{0,6},{1,7},{2,4},{3,5},{4,2},{5,3},{6,0},{7,1},{8,14},{9,15},{10,... | collective-permute-start | bytes 24584 | tf_op jit(solution)/shard_map/ppermute | solution.py:449
  47.1 2.3 %collective-permute-start.19 = (bf16[2,8,512]{2,1,0:T(8,128)(2,1)S(1)}, bf16[2,8,512]{2,1,0:T(8,128)(2,1)S(1)}, u32[]{:S(2)}, u32[]{:S(2)}) collective-permute-start(bf16[2,8,512]{2,1,0:T(8,128)(2,1)S(1)} %collective-permute-done.18.far_ref), channel_id=1, source_target_pairs={{0,1},{1,0},{2,3},{3,2},{4,5},{5,4},{6,7},{7,6},{8,9},{9,8},{10,11... | collective-permute-start | bytes 49160 | tf_op jit(solution)/shard_map/ppermute | solution.py:449
  (16 other events, 222.2 us)

commit v8 on v7

--- a/solution.py
+++ b/solution.py
@@ -358,7 +358,7 @@
     chip = lax.axis_index("kv")
     far = lax.bitwise_xor(chip, far_step(core))
     columns = (2 * far, 2 * far + 1, 2 * lax.bitwise_xor(chip, 3) + core, 2 * chip + core)
-    for slot, column in enumerate(columns):
+    for slot, column in enumerate(columns[: partial_ref.shape[0]]):
         partial_ref[slot] = jnp.dot(
             hidden,
             down_ref[:, pl.ds(pl.multiple_of(column * width, width), width)],
@@ -397,16 +397,26 @@
     down_part(hidden_ref[...], down_ref, lax.axis_index("tp"), partial_ref)
 
 
+def mate_kept_kernel(hidden_ref, down_ref, kept_ref):
+    width = kept_ref.shape[1]
+    column = 2 * lax.axis_index("kv") + 1 - lax.axis_index("tp")
+    kept_ref[...] = jnp.dot(
+        hidden_ref[...],
+        down_ref[:, pl.ds(pl.multiple_of(column * width, width), width)],
+        preferred_element_type=jnp.float32,
+    )
+
+
 def chip_sum_kernel(own_ref, mate_ref, far_ref, mid_ref, kept_ref):
     for core in range(2):
         far_ref[core] = (own_ref[core] + mate_ref[core]).astype(jnp.bfloat16)
     mid_ref[...] = (own_ref[2] + mate_ref[2]).astype(jnp.bfloat16)
-    kept_ref[...] = own_ref[3] + mate_ref[3]
-
-
-def last_kernel(residual_ref, kept_ref, mid_ref, far_ref, swapped_ref, output_ref):
+    kept_ref[...] = own_ref[3]
+
+
+def last_kernel(residual_ref, kept_ref, mid_ref, far_ref, swapped_ref, mate_ref, output_ref):
     core = lax.axis_index("tp")
-    total = kept_ref[...]
+    total = kept_ref[...] + mate_ref[...]
     for block in (mid_ref[...], far_ref[core], swapped_ref[core]):
         total = total + block.astype(jnp.float32)
     output_ref[...] = (residual_ref[...].astype(jnp.float32) + total).astype(jnp.bfloat16)
@@ -531,7 +541,7 @@
     )
     hidden, mate_part = call(
         functools.partial(mixer_kernel, kv),
-        [shape((rows, up_weight.shape[1]), bf16), shape((kv, rows, width), f32)],
+        [shape((rows, up_weight.shape[1]), bf16), shape((kv - 1, rows, width), f32)],
         (*pairs_of_rows, early, mlp_row, up_weight, down_weight),
         COST[5],
         14 * MIB,
@@ -547,8 +557,12 @@
         MIB,
     )
     sums = crossed(far, mid)
+    mate_kept = call(
+        mate_kept_kernel, shape((rows, width), f32), (hidden, down_weight), COST[7], 14 * MIB
+    )
+    mate_kept = other_core(mate_kept)
     layer_output = call(
-        last_kernel, shape((rows, width), bf16), (residual, kept, *sums), COST[8], MIB
+        last_kernel, shape((rows, width), bf16), (residual, kept, *sums, mate_kept), COST[8], MIB
     )
     return (layer_output, next_state)
 

time: 50.1 us -> 50.7 us (1.012)
    ppermute x20 -> x21, starting transfers between devices: 16.4 us -> 16.8 us  [permute(): return lax.ppermute(block, group, hops)]
    pallas_call x19 -> x20, Pallas kernels: 9.9 us -> 10 us  [call(): pl.pallas_call(body, out_shape=outs, in_specs=[whole] * len(arrays), out_...]
    ppermute x20 -> x21, waiting for transfers between devices: 20.9 us -> 20.9 us  [permute(): return lax.ppermute(block, group, hops)]
  transfers between devices with their start and end apart: 20 -> 21, of which waited for: 15 -> 13; matrix products, arithmetic and copies ran while one was open for 0% -> 0% of each run, Pallas kernels for 13% -> 14%
where the time goes in v8:
time: 50.7 us; the launch traced here: 50.5 us
  waiting for transfers between devices  20.9 us (41%)
  starting transfers between devices  16.8 us (33%)
  Pallas kernels  11 us (22%)
  between operations  0.92 us (2%)
  local copies, waits for them, and re-layouts  0.81 us (2%)
    ppermute x21, waiting for transfers between devices, permute(): return lax.ppermute(block, group, hops)  20.9 us
    ppermute x21, starting transfers between devices, permute(): return lax.ppermute(block, group, hops)  16.8 us
    pallas_call x20, Pallas kernels, call(): pl.pallas_call(body, out_shape=outs, in_specs=[whole] * len(arrays), out_...  10 us
  transfers between devices with their start and end apart: 21, of which 13 were waited for; matrix products, arithmetic and copies ran while one was open for 0% of the time, Pallas kernels for 14%

profile of v8, /device:TPU:0, one launch (start us, length us, event | category | flops | bytes accessed | tf_op | source)
XLA Modules:
  0.0 50.5 jit_solution(6255516432233302471)
XLA Ops:
  1.2 0.7 %copy-done.7 = bf16[8,512]{1,0:T(8,128)(2,1)S(1)} copy-done((bf16[8,512]{1,0:T(8,128)(2,1)S(1)}, bf16[8,512]{1,0:T(8,128)(2,1)}, u32[]{:S(2)}) %copy-start.7) | copy-done | bytes 8216
  2.2 2.9 %collective-permute-start.2 = (bf16[2,8,512]{2,1,0:T(8,128)(2,1)S(1)}, bf16[2,8,512]{2,1,0:T(8,128)(2,1)S(1)}, u32[]{:S(2)}, u32[]{:S(2)}) collective-permute-start(bf16[2,8,512]{2,1,0:T(8,128)(2,1)S(1)} %shard_map.141.pair_ref.refs_0_), channel_id=1, source_target_pairs={{0,2},{1,5},{2,0},{3,7},{4,6},{5,1},{6,4},{7,3},{8,10},{9,13},{10,... | collective-permute-start | bytes 49160 | tf_op jit(solution)/shard_map/ppermute | solution.py:459
  5.1 2.5 %collective-permute-start.1 = (bf16[2,8,512]{2,1,0:T(8,128)(2,1)S(1)}, bf16[2,8,512]{2,1,0:T(8,128)(2,1)S(1)}, u32[]{:S(2)}, u32[]{:S(2)}) collective-permute-start(bf16[2,8,512]{2,1,0:T(8,128)(2,1)S(1)} %shard_map.141.pair_ref.refs_0_), channel_id=1, source_target_pairs={{0,6},{1,7},{2,4},{3,5},{4,2},{5,3},{6,0},{7,1},{8,14},{9,15},{10,... | collective-permute-start | bytes 49160 | tf_op jit(solution)/shard_map/ppermute | solution.py:459
  10.8 0.7 %shard_map.145 = (bf16[16,128]{1,0:T(8,128)(2,1)S(1)}, bf16[16,128]{1,0:T(8,128)(2,1)S(1)}, bf16[16,128]{1,0:T(8,128)(2,1)S(1)}, bf16[16,128]{1,0:T(8,128)(2,1)S(1)}) custom-call(bf16[2,8,512]{2,1,0:T(8,128)(2,1)S(1)} %shard_map.141.pair_ref.refs_0_, bf16[2,8,512]{2,1,0:T(8,128)(2,1)S(1)} %collective-permute-done.1.refs_1_, ...), custom_call_target="tpu_custom_call" | custom-call | flops 99999997952 | tf_op jit(solution)/shard_map/pallas_call | solution.py:102
  11.6 1.1 %collective-permute-done.5.mate_ref = bf16[16,128]{1,0:T(8,128)(2,1)S(1)} collective-permute-done((bf16[16,128]{1,0:T(8,128)(2,1)S(1)}, bf16[16,128]{1,0:T(8,128)(2,1)S(1)}, u32[]{:S(2)}, u32[]{:S(2)}) %collective-permute-start.5) | collective-permute-done | bytes 4128 | tf_op jit(solution)/shard_map/ppermute | solution.py:459
  12.9 3.5 %collective-permute-done.6.refs_2_ = bf16[2,16,128]{2,1,0:T(8,128)(2,1)S(1)} collective-permute-done((bf16[2,16,128]{2,1,0:T(8,128)(2,1)S(1)}, bf16[2,16,128]{2,1,0:T(8,128)(2,1)S(1)}, u32[]{:S(2)}, u32[]{:S(2)}) %collective-permute-start.6) | collective-permute-done | bytes 8224 | tf_op jit(solution)/shard_map/ppermute | solution.py:459
  16.4 2.4 %collective-permute-start.4 = (bf16[16,128]{1,0:T(8,128)(2,1)S(1)}, bf16[16,128]{1,0:T(8,128)(2,1)S(1)}, u32[]{:S(2)}, u32[]{:S(2)}) collective-permute-start(bf16[16,128]{1,0:T(8,128)(2,1)S(1)} %get-tuple-element.15), channel_id=1, source_target_pairs={{0,6},{1,7},{2,4},{3,5},{4,2},{5,3},{6,0},{7,1},{8,14},{9,15},{10,... | collective-permute-start | bytes 12296 | tf_op jit(solution)/shard_map/ppermute | solution.py:459
  18.8 3.0 %collective-permute-done.4.refs_1_ = bf16[16,128]{1,0:T(8,128)(2,1)S(1)} collective-permute-done((bf16[16,128]{1,0:T(8,128)(2,1)S(1)}, bf16[16,128]{1,0:T(8,128)(2,1)S(1)}, u32[]{:S(2)}, u32[]{:S(2)}) %collective-permute-start.4) | collective-permute-done | bytes 4128 | tf_op jit(solution)/shard_map/ppermute | solution.py:459
  21.8 0.7 %shard_map.147 = (bf16[16,128]{1,0:T(8,128)(2,1)S(1)}, f32[16,128]{1,0:T(8,128)S(1)}, f32[16,128]{1,0:T(8,128)S(1)}) custom-call(bf16[16,128]{1,0:T(8,128)(2,1)S(1)} %get-tuple-element.14.refs_0_, bf16[16,128]{1,0:T(8,128)(2,1)S(1)} %collective-permute-done.4.refs_1_, bf16[2,16,128]{2,1,0:T(8,128)(2,1)S(1)} %collective-permute-done.6.refs_2_, ...), custom_call_target="tpu_custom_call" | custom-call | flops 1000000000 | tf_op jit(solution)/shard_map/pallas_call | solution.py:102
  22.6 1.2 %collective-permute-done.8.mate_ref = bf16[16,128]{1,0:T(8,128)(2,1)S(1)} collective-permute-done((bf16[16,128]{1,0:T(8,128)(2,1)S(1)}, bf16[16,128]{1,0:T(8,128)(2,1)S(1)}, u32[]{:S(2)}, u32[]{:S(2)}) %collective-permute-start.8) | collective-permute-done | bytes 4128 | tf_op jit(solution)/shard_map/ppermute | solution.py:459
  23.8 2.4 %collective-permute-start.9 = (bf16[2,16,128]{2,1,0:T(8,128)(2,1)S(1)}, bf16[2,16,128]{2,1,0:T(8,128)(2,1)S(1)}, u32[]{:S(2)}, u32[]{:S(2)}) collective-permute-start(bf16[2,16,128]{2,1,0:T(8,128)(2,1)S(1)} %shard_map.148.refs_0_), channel_id=1, source_target_pairs={{0,6},{1,7},{2,4},{3,5},{4,2},{5,3},{6,0},{7,1},{8,14},{9,15},{10,... | collective-permute-start | bytes 24584 | tf_op jit(solution)/shard_map/ppermute | solution.py:459
  26.1 1.3 %collective-permute-done.10.refs_2_ = bf16[2,16,128]{2,1,0:T(8,128)(2,1)S(1)} collective-permute-done((bf16[2,16,128]{2,1,0:T(8,128)(2,1)S(1)}, bf16[2,16,128]{2,1,0:T(8,128)(2,1)S(1)}, u32[]{:S(2)}, u32[]{:S(2)}) %collective-permute-start.10) | collective-permute-done | bytes 8224 | tf_op jit(solution)/shard_map/ppermute | solution.py:459
  27.4 1.8 %collective-permute-done.9.refs_1_ = bf16[2,16,128]{2,1,0:T(8,128)(2,1)S(1)} collective-permute-done((bf16[2,16,128]{2,1,0:T(8,128)(2,1)S(1)}, bf16[2,16,128]{2,1,0:T(8,128)(2,1)S(1)}, u32[]{:S(2)}, u32[]{:S(2)}) %collective-permute-start.9) | collective-permute-done | bytes 8224 | tf_op jit(solution)/shard_map/ppermute | solution.py:459
  29.7 1.2 %collective-permute-done.12.mate_ref = bf16[8,512]{1,0:T(8,128)(2,1)S(1)} collective-permute-done((bf16[8,512]{1,0:T(8,128)(2,1)S(1)}, bf16[8,512]{1,0:T(8,128)(2,1)S(1)}, u32[]{:S(2)}, u32[]{:S(2)}) %collective-permute-start.12) | collective-permute-done | bytes 8224 | tf_op jit(solution)/shard_map/ppermute | solution.py:459
  31.1 3.5 %collective-permute-done.14.pair_ref.refs_2_ = bf16[2,8,512]{2,1,0:T(8,128)(2,1)S(1)} collective-permute-done((bf16[2,8,512]{2,1,0:T(8,128)(2,1)S(1)}, bf16[2,8,512]{2,1,0:T(8,128)(2,1)S(1)}, u32[]{:S(2)}, u32[]{:S(2)}) %collective-permute-start.14) | collective-permute-done | bytes 16416 | tf_op jit(solution)/shard_map/ppermute | solution.py:459
  34.6 2.4 %collective-permute-start.13 = (bf16[2,8,512]{2,1,0:T(8,128)(2,1)S(1)}, bf16[2,8,512]{2,1,0:T(8,128)(2,1)S(1)}, u32[]{:S(2)}, u32[]{:S(2)}) collective-permute-start(bf16[2,8,512]{2,1,0:T(8,128)(2,1)S(1)} %shard_map.150.pair_ref.refs_0_), channel_id=1, source_target_pairs={{0,6},{1,7},{2,4},{3,5},{4,2},{5,3},{6,0},{7,1},{8,14},{9,15},{10,... | collective-permute-start | bytes 49160 | tf_op jit(solution)/shard_map/ppermute | solution.py:459
  37.7 0.7 %shard_map.152.refs_0_ = f32[8,2048]{1,0:T(8,128)S(1)} custom-call(bf16[2,8,512]{2,1,0:T(8,128)(2,1)S(1)} %collective-permute-done.14.pair_ref.refs_2_, f32[1,4096]{1,0:T(1,128)S(1)} %bitcast.7, bf16[4096,2048]{1,0:T(8,128)(2,1)S(1)} %bitcast.5, bf16[2048,4096]{1,0:T(8,128)(2,1)S(1)} %bitcast.3, f32[8,2048]{1,0:T(8,128)S(1)} %shard_map.151.refs_0_), custom_call_target="tpu_custom_call" | custom-call | flops 1000000 | tf_op jit(solution)/shard_map/pallas_call | solution.py:102
  38.4 0.7 %shard_map.153.refs_4_ = f32[8,2048]{1,0:T(8,128)S(1)} custom-call(bf16[2,8,512]{2,1,0:T(8,128)(2,1)S(1)} %collective-permute-done.15.pair_ref.refs_3_, f32[1,4096]{1,0:T(1,128)S(1)} %bitcast.8, bf16[4096,2048]{1,0:T(8,128)(2,1)S(1)} %bitcast.5, bf16[2048,4096]{1,0:T(8,128)(2,1)S(1)} %bitcast.3, f32[8,2048]{1,0:T(8,128)S(1)} %shard_map.152.refs_0_), custom_call_target="tpu_custom_call" | custom-call | flops 1000000 | tf_op jit(solution)/shard_map/pallas_call | solution.py:102
  39.1 1.1 %collective-permute-done.13.refs_1_ = bf16[2,8,512]{2,1,0:T(8,128)(2,1)S(1)} collective-permute-done((bf16[2,8,512]{2,1,0:T(8,128)(2,1)S(1)}, bf16[2,8,512]{2,1,0:T(8,128)(2,1)S(1)}, u32[]{:S(2)}, u32[]{:S(2)}) %collective-permute-start.13) | collective-permute-done | bytes 16416 | tf_op jit(solution)/shard_map/ppermute | solution.py:459
  40.2 1.5 %shard_map.154 = (bf16[8,2048]{1,0:T(8,128)(2,1)S(1)}, f32[3,8,512]{2,1,0:T(8,128)S(1)}) custom-call(bf16[2,8,512]{2,1,0:T(8,128)(2,1)S(1)} %shard_map.150.pair_ref.refs_0_, bf16[2,8,512]{2,1,0:T(8,128)(2,1)S(1)} %collective-permute-done.13.refs_1_, bf16[2,8,512]{2,1,0:T(8,128)(2,1)S(1)} %collective-permute-done.14.pair_ref.refs_2_, ...), custom_call_target="tpu_custom_call" | custom-call | flops 1000000 | tf_op jit(solution)/shard_map/pallas_call | solution.py:102
  41.7 1.2 %shard_map.155.own_ref = f32[4,8,512]{2,1,0:T(8,128)S(1)} custom-call(bf16[8,2048]{1,0:T(8,128)(2,1)S(1)} %get-tuple-element.19.hidden_ref, bf16[2048,4096]{1,0:T(8,128)(2,1)S(1)} %bitcast.3), custom_call_target="tpu_custom_call" | custom-call | flops 1000000000 | tf_op jit(solution)/shard_map/pallas_call | solution.py:102
  44.4 2.4 %collective-permute-start.17 = (bf16[8,512]{1,0:T(8,128)(2,1)S(1)}, bf16[8,512]{1,0:T(8,128)(2,1)S(1)}, u32[]{:S(2)}, u32[]{:S(2)}) collective-permute-start(bf16[8,512]{1,0:T(8,128)(2,1)S(1)} %get-tuple-element.22), channel_id=1, source_target_pairs={{0,6},{1,7},{2,4},{3,5},{4,2},{5,3},{6,0},{7,1},{8,14},{9,15},{10,... | collective-permute-start | bytes 24584 | tf_op jit(solution)/shard_map/ppermute | solution.py:459
  47.0 1.0 %shard_map.160 = f32[2,8,128,128]{3,2,1,0:T(8,128)} custom-call(f32[2,8,128,128]{3,2,1,0:T(8,128)S(1)} %shard_map.159.made_ref), custom_call_target="tpu_custom_call" | custom-call | flops 1000000000 | tf_op jit(solution)/shard_map/pallas_call | solution.py:520
  48.0 1.9 %collective-permute-done.17.mid_ref = bf16[8,512]{1,0:T(8,128)(2,1)S(1)} collective-permute-done((bf16[8,512]{1,0:T(8,128)(2,1)S(1)}, bf16[8,512]{1,0:T(8,128)(2,1)S(1)}, u32[]{:S(2)}, u32[]{:S(2)}) %collective-permute-start.17) | collective-permute-done | bytes 8224 | tf_op jit(solution)/shard_map/ppermute | solution.py:459
  (81 shorter events, 8.0 us)
Async XLA Ops:
  0.6 1.6 %collective-permute-start = (bf16[8,512]{1,0:T(8,128)(2,1)}, bf16[8,512]{1,0:T(8,128)(2,1)S(1)}, u32[]{:S(2)}, u32[]{:S(2)}) collective-permute-start(bf16[8,512]{1,0:T(8,128)(2,1)} %refs_4_.3), channel_id=1, source_target_pairs={{0,1},{1,0},{2,3},{3,2},{4,5},{5,4},{6,7},{7,6},{8,9},{9,8},{10,11... | collective-permute-start | bytes 24584 | tf_op jit(solution)/shard_map/ppermute | solution.py:459
  2.2 6.1 %collective-permute-start.2 = (bf16[2,8,512]{2,1,0:T(8,128)(2,1)S(1)}, bf16[2,8,512]{2,1,0:T(8,128)(2,1)S(1)}, u32[]{:S(2)}, u32[]{:S(2)}) collective-permute-start(bf16[2,8,512]{2,1,0:T(8,128)(2,1)S(1)} %shard_map.141.pair_ref.refs_0_), channel_id=1, source_target_pairs={{0,2},{1,5},{2,0},{3,7},{4,6},{5,1},{6,4},{7,3},{8,10},{9,13},{10,... | collective-permute-start | bytes 49160 | tf_op jit(solution)/shard_map/ppermute | solution.py:459
  5.1 5.6 %collective-permute-start.1 = (bf16[2,8,512]{2,1,0:T(8,128)(2,1)S(1)}, bf16[2,8,512]{2,1,0:T(8,128)(2,1)S(1)}, u32[]{:S(2)}, u32[]{:S(2)}) collective-permute-start(bf16[2,8,512]{2,1,0:T(8,128)(2,1)S(1)} %shard_map.141.pair_ref.refs_0_), channel_id=1, source_target_pairs={{0,6},{1,7},{2,4},{3,5},{4,2},{5,3},{6,0},{7,1},{8,14},{9,15},{10,... | collective-permute-start | bytes 49160 | tf_op jit(solution)/shard_map/ppermute | solution.py:459
  8.3 1.2 %collective-permute-start.3 = (bf16[2,8,512]{2,1,0:T(8,128)(2,1)S(1)}, bf16[2,8,512]{2,1,0:T(8,128)(2,1)S(1)}, u32[]{:S(2)}, u32[]{:S(2)}) collective-permute-start(bf16[2,8,512]{2,1,0:T(8,128)(2,1)S(1)} %collective-permute-done.2.pair_ref.refs_2_), channel_id=1, source_target_pairs={{0,1},{1,0},{2,3},{3,2},{4,5},{5,4},{6,7},{7,6},{8,9},{9,8},{10,11... | collective-permute-start | bytes 49160 | tf_op jit(solution)/shard_map/ppermute | solution.py:459
  9.5 27.5 %slice-start = ((s8[16777216]{0:T(1024)(128)(4,1)}), s8[4194304]{0:T(1024)(128)(4,1)S(1)}, s32[]{:S(2)}) async-start(s8[16777216]{0:T(1024)(128)(4,1)} %bitcast.2), calls=%async_computation | async-start | bytes 8388608
  9.5 27.5 %slice-start.4 = ((s8[16777216]{0:T(1024)(128)(4,1)}), s8[4194304]{0:T(1024)(128)(4,1)S(1)}, s32[]{:S(2)}) async-start(s8[16777216]{0:T(1024)(128)(4,1)} %bitcast.4), calls=%async_computation.4 | async-start | bytes 8388608
  10.2 26.8 %slice-start.1 = ((s8[16777216]{0:T(1024)(128)(4,1)}), s8[4194304]{0:T(1024)(128)(4,1)S(1)}, s32[]{:S(2)}) async-start(s8[16777216]{0:T(1024)(128)(4,1)} %bitcast.2), calls=%async_computation.1 | async-start | bytes 8388608
  11.5 1.2 %collective-permute-start.5 = (bf16[16,128]{1,0:T(8,128)(2,1)S(1)}, bf16[16,128]{1,0:T(8,128)(2,1)S(1)}, u32[]{:S(2)}, u32[]{:S(2)}) collective-permute-start(bf16[16,128]{1,0:T(8,128)(2,1)S(1)} %get-tuple-element.17), channel_id=1, source_target_pairs={{0,1},{1,0},{2,3},{3,2},{4,5},{5,4},{6,7},{7,6},{8,9},{9,8},{10,11... | collective-permute-start | bytes 12296 | tf_op jit(solution)/shard_map/ppermute | solution.py:459
  12.7 3.7 %collective-permute-start.6 = (bf16[2,16,128]{2,1,0:T(8,128)(2,1)S(1)}, bf16[2,16,128]{2,1,0:T(8,128)(2,1)S(1)}, u32[]{:S(2)}, u32[]{:S(2)}) collective-permute-start(bf16[2,16,128]{2,1,0:T(8,128)(2,1)S(1)} %shard_map.146), channel_id=1, source_target_pairs={{0,2},{1,5},{2,0},{3,7},{4,6},{5,1},{6,4},{7,3},{8,10},{9,13},{10,... | collective-permute-start | bytes 24584 | tf_op jit(solution)/shard_map/ppermute | solution.py:459
  16.4 5.4 %collective-permute-start.7 = (bf16[2,16,128]{2,1,0:T(8,128)(2,1)S(1)}, bf16[2,16,128]{2,1,0:T(8,128)(2,1)S(1)}, u32[]{:S(2)}, u32[]{:S(2)}) collective-permute-start(bf16[2,16,128]{2,1,0:T(8,128)(2,1)S(1)} %collective-permute-done.6.refs_2_), channel_id=1, source_target_pairs={{0,1},{1,0},{2,3},{3,2},{4,5},{5,4},{6,7},{7,6},{8,9},{9,8},{10,11... | collective-permute-start | bytes 24584 | tf_op jit(solution)/shard_map/ppermute | solution.py:459
  16.4 5.4 %collective-permute-start.4 = (bf16[16,128]{1,0:T(8,128)(2,1)S(1)}, bf16[16,128]{1,0:T(8,128)(2,1)S(1)}, u32[]{:S(2)}, u32[]{:S(2)}) collective-permute-start(bf16[16,128]{1,0:T(8,128)(2,1)S(1)} %get-tuple-element.15), channel_id=1, source_target_pairs={{0,6},{1,7},{2,4},{3,5},{4,2},{5,3},{6,0},{7,1},{8,14},{9,15},{10,... | collective-permute-start | bytes 12296 | tf_op jit(solution)/shard_map/ppermute | solution.py:459
  22.6 1.2 %collective-permute-start.8 = (bf16[16,128]{1,0:T(8,128)(2,1)S(1)}, bf16[16,128]{1,0:T(8,128)(2,1)S(1)}, u32[]{:S(2)}, u32[]{:S(2)}) collective-permute-start(bf16[16,128]{1,0:T(8,128)(2,1)S(1)} %get-tuple-element.18.own_ref), channel_id=1, source_target_pairs={{0,1},{1,0},{2,3},{3,2},{4,5},{5,4},{6,7},{7,6},{8,9},{9,8},{10,11... | collective-permute-start | bytes 12296 | tf_op jit(solution)/shard_map/ppermute | solution.py:459
  23.8 3.7 %collective-permute-start.10 = (bf16[2,16,128]{2,1,0:T(8,128)(2,1)S(1)}, bf16[2,16,128]{2,1,0:T(8,128)(2,1)S(1)}, u32[]{:S(2)}, u32[]{:S(2)}) collective-permute-start(bf16[2,16,128]{2,1,0:T(8,128)(2,1)S(1)} %shard_map.148.refs_0_), channel_id=1, source_target_pairs={{0,2},{1,5},{2,0},{3,7},{4,6},{5,1},{6,4},{7,3},{8,10},{9,13},{10,... | collective-permute-start | bytes 24584 | tf_op jit(solution)/shard_map/ppermute | solution.py:459
  23.8 5.4 %collective-permute-start.9 = (bf16[2,16,128]{2,1,0:T(8,128)(2,1)S(1)}, bf16[2,16,128]{2,1,0:T(8,128)(2,1)S(1)}, u32[]{:S(2)}, u32[]{:S(2)}) collective-permute-start(bf16[2,16,128]{2,1,0:T(8,128)(2,1)S(1)} %shard_map.148.refs_0_), channel_id=1, source_target_pairs={{0,6},{1,7},{2,4},{3,5},{4,2},{5,3},{6,0},{7,1},{8,14},{9,15},{10,... | collective-permute-start | bytes 24584 | tf_op jit(solution)/shard_map/ppermute | solution.py:459
  27.4 1.8 %collective-permute-start.11 = (bf16[2,16,128]{2,1,0:T(8,128)(2,1)S(1)}, bf16[2,16,128]{2,1,0:T(8,128)(2,1)S(1)}, u32[]{:S(2)}, u32[]{:S(2)}) collective-permute-start(bf16[2,16,128]{2,1,0:T(8,128)(2,1)S(1)} %collective-permute-done.10.refs_2_), channel_id=1, source_target_pairs={{0,1},{1,0},{2,3},{3,2},{4,5},{5,4},{6,7},{7,6},{8,9},{9,8},{10,11... | collective-permute-start | bytes 24584 | tf_op jit(solution)/shard_map/ppermute | solution.py:459
  29.6 1.2 %collective-permute-start.12 = (bf16[8,512]{1,0:T(8,128)(2,1)S(1)}, bf16[8,512]{1,0:T(8,128)(2,1)S(1)}, u32[]{:S(2)}, u32[]{:S(2)}) collective-permute-start(bf16[8,512]{1,0:T(8,128)(2,1)S(1)} %shard_map.149.own_ref.residual_ref), channel_id=1, source_target_pairs={{0,1},{1,0},{2,3},{3,2},{4,5},{5,4},{6,7},{7,6},{8,9},{9,8},{10,11... | collective-permute-start | bytes 24584 | tf_op jit(solution)/shard_map/ppermute | solution.py:459
  30.9 3.8 %collective-permute-start.14 = (bf16[2,8,512]{2,1,0:T(8,128)(2,1)S(1)}, bf16[2,8,512]{2,1,0:T(8,128)(2,1)S(1)}, u32[]{:S(2)}, u32[]{:S(2)}) collective-permute-start(bf16[2,8,512]{2,1,0:T(8,128)(2,1)S(1)} %shard_map.150.pair_ref.refs_0_), channel_id=1, source_target_pairs={{0,2},{1,5},{2,0},{3,7},{4,6},{5,1},{6,4},{7,3},{8,10},{9,13},{10,... | collective-permute-start | bytes 49160 | tf_op jit(solution)/shard_map/ppermute | solution.py:459
  34.6 3.8 %collective-permute-start.15 = (bf16[2,8,512]{2,1,0:T(8,128)(2,1)S(1)}, bf16[2,8,512]{2,1,0:T(8,128)(2,1)S(1)}, u32[]{:S(2)}, u32[]{:S(2)}) collective-permute-start(bf16[2,8,512]{2,1,0:T(8,128)(2,1)S(1)} %collective-permute-done.14.pair_ref.refs_2_), channel_id=1, source_target_pairs={{0,1},{1,0},{2,3},{3,2},{4,5},{5,4},{6,7},{7,6},{8,9},{9,8},{10,11... | collective-permute-start | bytes 49160 | tf_op jit(solution)/shard_map/ppermute | solution.py:459
  34.6 5.5 %collective-permute-start.13 = (bf16[2,8,512]{2,1,0:T(8,128)(2,1)S(1)}, bf16[2,8,512]{2,1,0:T(8,128)(2,1)S(1)}, u32[]{:S(2)}, u32[]{:S(2)}) collective-permute-start(bf16[2,8,512]{2,1,0:T(8,128)(2,1)S(1)} %shard_map.150.pair_ref.refs_0_), channel_id=1, source_target_pairs={{0,6},{1,7},{2,4},{3,5},{4,2},{5,3},{6,0},{7,1},{8,14},{9,15},{10,... | collective-permute-start | bytes 49160 | tf_op jit(solution)/shard_map/ppermute | solution.py:459
  41.7 1.2 %collective-permute-start.16 = (f32[3,8,512]{2,1,0:T(8,128)S(1)}, f32[3,8,512]{2,1,0:T(8,128)S(1)}, u32[]{:S(2)}, u32[]{:S(2)}) collective-permute-start(f32[3,8,512]{2,1,0:T(8,128)S(1)} %get-tuple-element.20), channel_id=1, source_target_pairs={{0,1},{1,0},{2,3},{3,2},{4,5},{5,4},{6,7},{7,6},{8,9},{9,8},{10,11... | collective-permute-start | bytes 147464 | tf_op jit(solution)/shard_map/ppermute | solution.py:459
  43.0 3.8 %collective-permute-start.18 = (bf16[2,8,512]{2,1,0:T(8,128)(2,1)S(1)}, bf16[2,8,512]{2,1,0:T(8,128)(2,1)S(1)}, u32[]{:S(2)}, u32[]{:S(2)}) collective-permute-start(bf16[2,8,512]{2,1,0:T(8,128)(2,1)S(1)} %get-tuple-element.23), channel_id=1, source_target_pairs={{0,2},{1,5},{2,0},{3,7},{4,6},{5,1},{6,4},{7,3},{8,10},{9,13},{10,... | collective-permute-start | bytes 49160 | tf_op jit(solution)/shard_map/ppermute | solution.py:459
  43.9 4.1 %collective-permute-start.20 = (f32[8,512]{1,0:T(8,128)S(1)}, f32[8,512]{1,0:T(8,128)S(1)}, u32[]{:S(2)}, u32[]{:S(2)}) collective-permute-start(f32[8,512]{1,0:T(8,128)S(1)} %shard_map.157), channel_id=1, source_target_pairs={{0,1},{1,0},{2,3},{3,2},{4,5},{5,4},{6,7},{7,6},{8,9},{9,8},{10,11... | collective-permute-start | bytes 49160 | tf_op jit(solution)/shard_map/ppermute | solution.py:459
  44.4 5.4 %collective-permute-start.17 = (bf16[8,512]{1,0:T(8,128)(2,1)S(1)}, bf16[8,512]{1,0:T(8,128)(2,1)S(1)}, u32[]{:S(2)}, u32[]{:S(2)}) collective-permute-start(bf16[8,512]{1,0:T(8,128)(2,1)S(1)} %get-tuple-element.22), channel_id=1, source_target_pairs={{0,6},{1,7},{2,4},{3,5},{4,2},{5,3},{6,0},{7,1},{8,14},{9,15},{10,... | collective-permute-start | bytes 24584 | tf_op jit(solution)/shard_map/ppermute | solution.py:459
  46.8 3.1 %collective-permute-start.19 = (bf16[2,8,512]{2,1,0:T(8,128)(2,1)S(1)}, bf16[2,8,512]{2,1,0:T(8,128)(2,1)S(1)}, u32[]{:S(2)}, u32[]{:S(2)}) collective-permute-start(bf16[2,8,512]{2,1,0:T(8,128)(2,1)S(1)} %collective-permute-done.18.far_ref), channel_id=1, source_target_pairs={{0,1},{1,0},{2,3},{3,2},{4,5},{5,4},{6,7},{7,6},{8,9},{9,8},{10,11... | collective-permute-start | bytes 49160 | tf_op jit(solution)/shard_map/ppermute | solution.py:459
  (17 other events, 249.0 us)
